TPU v7x, 32 devices: a whole 2x2x4 slice. The times are simulated.
32 devices in a mesh: sp: 32 (over z, y, x, core), tp: 1.
Axes of the slice: x: 2, y: 2, z: 4, core: 2. Of those that a mesh axis runs over, the one named last changes fastest.
Arguments:
- stream: bfloat16 [8192, 2048], P(('sp', 'tp')), may hold values from -6 to 6
- query_one: bfloat16 [8192, 512], P('sp', 'tp'), may hold values from -280 to 280
- key_one: bfloat16 [8192, 512], P('sp', 'tp'), may hold values from -6 to 6
- query_two: bfloat16 [8192, 512], P('sp', 'tp'), may hold values from -280 to 280
- key_two: bfloat16 [8192, 512], P('sp', 'tp'), may hold values from -6 to 6
- values: bfloat16 [8192, 1024], P('sp', 'tp'), may hold values from -6 to 6
- lambdas: float32 [8], P('tp'), may hold values from 0.3 to 0.8
- head_gain: float32 [128], replicated, may hold values from 0.1 to 1.9
- out_weight: bfloat16 [1024, 2048], replicated, may hold values from -0.1875 to 0.1875
- norm_gain: float32 [2048], replicated, may hold values from 0.1 to 1.9
- gate_weight: bfloat16 [2048, 2816], P('sp', 'tp'), may hold values from -0.125 to 0.125
- up_weight: bfloat16 [2048, 2816], P('sp', 'tp'), may hold values from -0.125 to 0.125
- down_weight: bfloat16 [2816, 2048], P('tp', 'sp'), may hold values from -0.3125 to 0.3125
Outputs:
- result: bfloat16 [8192, 2048], P(('sp', 'tp'))
All inputs are finite; a program needn't handle non-finite values.
Results may differ from a plain program's by a relative error of at most 0.014.
Values may be sent and summed in bfloat16 or wider, within the bound.
No kernel may reach another device: no remote copies, remote signals or barrier semaphores. Data moves between devices by JAX's collectives and lax.ppermute only.
A program may use at most 192 MiB of HBM per device.

v0:
```python
import math

import jax
import jax.numpy as jnp
from jax import lax
from jax.sharding import PartitionSpec as P

HEAD_DIM = 64


ALPHA = 1.4142135623730951
EPSILON = 1e-05


def update(carried, queries, keys, value_rows, factor):
    maxima, totals, weighted = carried
    scores = jnp.einsum("qhd,khd->hqk", queries, keys, preferred_element_type=jnp.float32) * factor
    new_maxima = jnp.maximum(maxima, jnp.max(scores, axis=-1))
    rescale = jnp.exp(maxima - new_maxima)
    weights = jnp.exp(scores - new_maxima[:, :, None])
    totals = totals * rescale + jnp.sum(weights, axis=-1)
    weighted = weighted * jnp.transpose(rescale)[:, :, None] + jnp.einsum(
        "hqk,khe->qhe", weights.astype(jnp.bfloat16), value_rows, preferred_element_type=jnp.float32
    )
    return (new_maxima, totals, weighted)


def finish(carried):
    maxima, totals, weighted = carried
    return weighted / jnp.transpose(totals)[:, :, None]


def layer_normed(heads_rows, residual_rows, out_weight, norm_gain):
    branch = jnp.dot(heads_rows, out_weight, preferred_element_type=jnp.float32)
    mixed_in = ALPHA * residual_rows.astype(jnp.float32) + branch
    row_mean = jnp.mean(mixed_in, axis=-1, keepdims=True)
    centered = mixed_in - row_mean
    row_var = jnp.mean(centered * centered, axis=-1, keepdims=True)
    return (centered * lax.rsqrt(row_var + EPSILON) * norm_gain).astype(jnp.bfloat16)


def sectioned_length(shard_len, group):
    return shard_len * math.gcd(128 // shard_len, group)


def sectioned_absorb(state, pieces, offset, along, block_len, work):
    running, sectioning, filled = state
    length = pieces[0].shape[along]
    sectioning = tuple((piece for piece in pieces))
    block_starts = jnp.arange(filled.shape[0], dtype=jnp.int32) * block_len
    covered = jnp.minimum(offset + length, block_starts + block_len) - jnp.maximum(
        offset, block_starts
    )
    covered = jnp.clip(covered, 0, block_len)
    before = filled
    filled = covered
    completed = (filled == block_len) & (before < block_len)

    def visit_block(block_index, totals):
        begin_at = block_index * block_len

        def compute(inner):
            slices = tuple(
                (
                    lax.dynamic_slice_in_dim(holder, begin_at, block_len, along)
                    for holder in sectioning
                )
            )
            return work(inner, slices, begin_at)

        def unchanged(inner):
            return inner

        return lax.cond(completed[block_index], compute, unchanged, totals)

    running = lax.fori_loop(0, filled.shape[0], visit_block, running)
    return (running, sectioning, filled)


def on_device(
    stream,
    query_one,
    key_one,
    query_two,
    key_two,
    values,
    lambdas,
    head_gain,
    out_weight,
    norm_gain,
    gate_weight,
    up_weight,
    down_weight,
):
    local_heads = lambdas.shape[0]
    head_width = query_one.shape[1] // local_heads
    value_width = values.shape[1] // local_heads
    tokens = query_one.shape[0]
    group = lax.axis_size("sp")
    factor = HEAD_DIM ** (-0.5)
    gate_full, up_full = (
        lax.all_gather(gate_weight, "sp", axis=0, tiled=True),
        lax.all_gather(up_weight, "sp", axis=0, tiled=True),
    )
    queries_first = query_one.reshape(tokens, local_heads, head_width)
    queries_second = query_two.reshape(tokens, local_heads, head_width)
    initial = (
        jnp.full((local_heads, tokens), -1e30, jnp.float32),
        jnp.zeros((local_heads, tokens), jnp.float32),
        jnp.zeros((tokens, local_heads, value_width), jnp.float32),
    )
    first_keys = lax.all_gather(key_one, "sp", axis=0, tiled=True)
    second_keys = lax.all_gather(key_two, "sp", axis=0, tiled=True)
    value_rows = lax.all_gather(values, "sp", axis=0, tiled=True)
    length = first_keys.shape[0]
    block_len = length
    while block_len > 2048 and block_len % 2 == 0:
        block_len = block_len // 2
    first_keys = first_keys.reshape(length, local_heads, head_width)
    second_keys = second_keys.reshape(length, local_heads, head_width)
    value_rows = value_rows.reshape(length, local_heads, value_width)

    def advance(block_index, partial_value):
        begin_row = block_index * block_len
        keys_first = lax.dynamic_slice_in_dim(first_keys, begin_row, block_len, 0)
        keys_second = lax.dynamic_slice_in_dim(second_keys, begin_row, block_len, 0)
        block_values = lax.dynamic_slice_in_dim(value_rows, begin_row, block_len, 0)
        return (
            update(partial_value[0], queries_first, keys_first, block_values, factor),
            update(partial_value[1], queries_second, keys_second, block_values, factor),
        )

    first_state, second_state = lax.fori_loop(0, length // block_len, advance, (initial, initial))
    differ = finish(first_state) - lambdas[None, :, None] * finish(second_state)
    inverse_rms = lax.rsqrt(jnp.mean(differ * differ, axis=-1, keepdims=True) + EPSILON)
    attended = (
        (differ * inverse_rms * head_gain * 0.8)
        .astype(jnp.bfloat16)
        .reshape(tokens, local_heads * value_width)
    )
    by_rows = lax.all_to_all(attended, "tp", split_axis=0, concat_axis=1, tiled=True)
    own_normed = layer_normed(by_rows, stream, out_weight, norm_gain)
    normed_all = lax.all_gather(own_normed, "tp", axis=0, tiled=True)
    row_count = normed_all.shape[0]
    gate_out = jnp.dot(normed_all, gate_full, preferred_element_type=jnp.float32)
    upward = jnp.dot(normed_all, up_full, preferred_element_type=jnp.float32)
    hidden = (jax.nn.silu(gate_out) * upward).astype(jnp.bfloat16)
    column_width = down_weight.shape[1]
    columns_block = sectioned_length(column_width, group)

    def project_block(outputs, slices, begin_at):
        product = jnp.dot(hidden, slices[0], preferred_element_type=jnp.float32)
        return lax.dynamic_update_slice_in_dim(outputs, product, begin_at, 1)

    project_start = (
        jnp.zeros((row_count, column_width * group), jnp.float32),
        (jnp.zeros((down_weight.shape[0], column_width * group), jnp.bfloat16),),
        jnp.zeros((column_width * group // columns_block,), jnp.int32),
    )
    project_state = sectioned_absorb(
        project_start,
        (lax.all_gather(down_weight, "sp", axis=1, tiled=True),),
        jnp.int32(0),
        1,
        columns_block,
        project_block,
    )
    partial_terms = project_state[0]
    mixer_out = lax.psum_scatter(
        partial_terms.astype(jnp.bfloat16), "tp", scatter_dimension=0, tiled=True
    ).astype(jnp.float32)
    return (ALPHA * own_normed.astype(jnp.float32) + 0.5 * mixer_out).astype(jnp.bfloat16)


def solution(mesh):
    return jax.shard_map(
        on_device,
        mesh=mesh,
        in_specs=(
            P(("sp", "tp"), None),
            P("sp", "tp"),
            P("sp", "tp"),
            P("sp", "tp"),
            P("sp", "tp"),
            P("sp", "tp"),
            P("tp"),
            P(),
            P(),
            P(),
            P("sp", "tp"),
            P("sp", "tp"),
            P("tp", "sp"),
        ),
        out_specs=P(("sp", "tp"), None),
        check_vma=False,
    )
```

profile of v0, /device:TPU:0, one launch (start us, length us, event | category | flops | bytes accessed | tf_op | source)
XLA Modules:
  0.0 724.0 jit_solution(6272200042016041110)
XLA Ops:
  13.2 76.8 %all-gather.7.cloned.1.call-done = bf16[8192,512]{1,0:T(8,128)(2,1)} async-done(((bf16[256,512]{1,0:T(8,128)(2,1)}), bf16[8192,512]{1,0:T(8,128)(2,1)}) %all-gather.7.cloned.1.call-update) | async-done | bytes 8388624 | tf_op jit(solution)/shard_map/all_gather | solution.py:112
  90.0 11.9 %copy.25 = bf16[8192,512]{0,1:T(8,128)(2,1)} copy(bf16[8192,512]{1,0:T(8,128)(2,1)} %all-gather.7.cloned.1.call-done) | data formatting | bytes 16777216 | tf_op jit(solution)/shard_map/all_gather | solution.py:112
  101.9 66.6 %all-gather.11.cloned.1.call-done = bf16[8192,512]{1,0:T(8,128)(2,1)} async-done(((bf16[256,512]{1,0:T(8,128)(2,1)}), bf16[8192,512]{1,0:T(8,128)(2,1)}) %all-gather.11.cloned.1.call-update) | async-done | bytes 8388624 | tf_op jit(solution)/shard_map/all_gather | solution.py:113
  168.6 11.8 %copy.28 = bf16[8192,512]{0,1:T(8,128)(2,1)} copy(bf16[8192,512]{1,0:T(8,128)(2,1)} %all-gather.11.cloned.1.call-done) | data formatting | bytes 16777216 | tf_op jit(solution)/shard_map/all_gather | solution.py:113
  180.3 80.3 %all-gather.13.cloned.1.call-done = bf16[2816,2048]{0,1:T(8,128)(2,1)} async-done(((bf16[2816,64]{0,1:T(8,128)(2,1)}), bf16[2816,2048]{0,1:T(8,128)(2,1)}) %all-gather.13.cloned.1.call-update) | async-done | bytes 11534352 | tf_op jit(solution)/shard_map/all_gather | solution.py:162
  260.6 15.3 %copy.30 = bf16[2816,2048]{1,0:T(8,128)(2,1)} copy(bf16[2816,2048]{0,1:T(8,128)(2,1)} %all-gather.13.cloned.1.call-done) | data formatting | bytes 23068672 | tf_op jit(solution)/shard_map/while | solution.py:76
  275.9 100.4 %all-gather.9.cloned.1.call-done = bf16[8192,1024]{1,0:T(8,128)(2,1)} async-done(((bf16[256,1024]{1,0:T(8,128)(2,1)}), bf16[8192,1024]{1,0:T(8,128)(2,1)}) %all-gather.9.cloned.1.call-update) | async-done | bytes 16777232 | tf_op jit(solution)/shard_map/all_gather | solution.py:114
  376.3 21.3 %copy.27 = bf16[8192,1024]{0,1:T(8,128)(2,1)} copy(bf16[8192,1024]{1,0:T(8,128)(2,1)} %all-gather.9.cloned.1.call-done) | data formatting | bytes 33554432 | tf_op jit(solution)/shard_map/all_gather | solution.py:114
  397.6 225.1 %while.41 = (s32[]{:T(128)}, f32[8,256]{1,0:T(8,128)S(1)}, f32[8,256]{1,0:T(8,128)S(1)}, f32[256,8,128]{0,2,1:T(8,128)S(1)}, f32[8,256]{1,0:T(8,128)S(1)}, /*ind...) while((s32[]{:T(128)}, f32[8,256]{1,0:T(8,128)S(1)}, ...), condition=%wide.region_5.0_spmd.clone, body=%wide.region_0.0_spmd.clone.sunk | while | flops 3289931776 | bytes 118227160 | solution.py:133
  397.6 9.9 %bitcast_reduce_fusion.5 = (f32[8,256]{1,0:T(8,128)S(1)}, f32[8,2048,256]{2,1,0:T(8,128)}) fusion(bf16[256,8,64]{0,2,1:T(8,128)(2,1)S(1)} %get-tuple-element.595, bf16[8192,8,64]{0,2,1:T(8,128)(2,1)} %get-tuple-element.594, s32[]{:T(128)S(6)} %select_n.21), kind=kOutput, calls=%fused_computation.5.clone.1 | convolution fusion | flops 545257472 | bytes 19144708 | tf_op jit(solution)/shard_map/while/body/eval_jaxpr/qhd,khd->hqk/dot_general | solution.py:17
  407.5 9.2 %fusion.90 = f32[256,8,128]{0,2,1:T(8,128)S(1)} fusion(f32[8,2048,256]{2,1,0:T(8,128)} %get-tuple-element.544, f32[8,256]{1,0:T(8,128)S(1)} %get-tuple-element.588, bf16[8192,8,128]{0,2,1:T(8,128)(2,1)} %get-tuple-element.593, s32[]{:T(128)S(6)} %select_n.21, f32[256,8,128]{0,2,1:T(8,128)S(1)} %get-tuple-element.574, ...), kind=kOutput, calls=%fused_computation.28.clone.1 | convolution fusion | flops 1087111168 | bytes 23085060 | tf_op jit(solution)/shard_map/while/body/eval_jaxpr/hqk,khe->qhe/dot_general | solution.py:22
  416.7 9.7 %bitcast_reduce_fusion.4 = (f32[8,256]{1,0:T(8,128)S(1)}, f32[8,2048,256]{2,1,0:T(8,128)}) fusion(bf16[256,8,64]{0,2,1:T(8,128)(2,1)S(1)} %get-tuple-element.592, bf16[8192,8,64]{0,2,1:T(8,128)(2,1)} %get-tuple-element.591, s32[]{:T(128)S(6)} %select_n.21), kind=kOutput, calls=%fused_computation.8.clone.1 | convolution fusion | flops 545257472 | bytes 19144708 | tf_op jit(solution)/shard_map/while/body/eval_jaxpr/qhd,khd->hqk/dot_general | solution.py:17
  426.4 10.7 %fusion.89 = f32[256,8,128]{0,2,1:T(8,128)S(1)} fusion(f32[8,2048,256]{2,1,0:T(8,128)} %get-tuple-element.547, f32[8,256]{1,0:T(8,128)S(1)} %get-tuple-element.585, bf16[8192,8,128]{0,2,1:T(8,128)(2,1)} %get-tuple-element.593, s32[]{:T(128)S(6)} %select_n.21, f32[256,8,128]{0,2,1:T(8,128)S(1)} %get-tuple-element.571, ...), kind=kOutput, calls=%fused_computation.29.clone.1 | convolution fusion | flops 1087111168 | bytes 23085060 | tf_op jit(solution)/shard_map/while/body/eval_jaxpr/hqk,khe->qhe/dot_general | solution.py:22
  445.8 8.6 %fusion.86 = f32[8,256]{1,0:T(8,128)S(1)} fusion(f32[8,2048,256]{2,1,0:T(8,128)} %get-tuple-element.544, f32[8,256]{1,0:T(8,128)S(1)} %get-tuple-element.588), kind=kLoop, calls=%fused_computation.13.clone.1 | loop fusion | flops 12580864 | bytes 16793600 | tf_op jit(solution)/shard_map/while/body/eval_jaxpr/reduce_sum | solution.py:21
  454.5 10.0 %bitcast_reduce_fusion.5 = (f32[8,256]{1,0:T(8,128)S(1)}, f32[8,2048,256]{2,1,0:T(8,128)}) fusion(bf16[256,8,64]{0,2,1:T(8,128)(2,1)S(1)} %get-tuple-element.595, bf16[8192,8,64]{0,2,1:T(8,128)(2,1)} %get-tuple-element.594, s32[]{:T(128)S(6)} %select_n.21), kind=kOutput, calls=%fused_computation.5.clone.1 | convolution fusion | flops 545257472 | bytes 19144708 | tf_op jit(solution)/shard_map/while/body/eval_jaxpr/qhd,khd->hqk/dot_general | solution.py:17
  464.4 9.5 %fusion.90 = f32[256,8,128]{0,2,1:T(8,128)S(1)} fusion(f32[8,2048,256]{2,1,0:T(8,128)} %get-tuple-element.544, f32[8,256]{1,0:T(8,128)S(1)} %get-tuple-element.588, bf16[8192,8,128]{0,2,1:T(8,128)(2,1)} %get-tuple-element.593, s32[]{:T(128)S(6)} %select_n.21, f32[256,8,128]{0,2,1:T(8,128)S(1)} %get-tuple-element.574, ...), kind=kOutput, calls=%fused_computation.28.clone.1 | convolution fusion | flops 1087111168 | bytes 23085060 | tf_op jit(solution)/shard_map/while/body/eval_jaxpr/hqk,khe->qhe/dot_general | solution.py:22
  474.0 9.7 %bitcast_reduce_fusion.4 = (f32[8,256]{1,0:T(8,128)S(1)}, f32[8,2048,256]{2,1,0:T(8,128)}) fusion(bf16[256,8,64]{0,2,1:T(8,128)(2,1)S(1)} %get-tuple-element.592, bf16[8192,8,64]{0,2,1:T(8,128)(2,1)} %get-tuple-element.591, s32[]{:T(128)S(6)} %select_n.21), kind=kOutput, calls=%fused_computation.8.clone.1 | convolution fusion | flops 545257472 | bytes 19144708 | tf_op jit(solution)/shard_map/while/body/eval_jaxpr/qhd,khd->hqk/dot_general | solution.py:17
  483.7 9.2 %fusion.89 = f32[256,8,128]{0,2,1:T(8,128)S(1)} fusion(f32[8,2048,256]{2,1,0:T(8,128)} %get-tuple-element.547, f32[8,256]{1,0:T(8,128)S(1)} %get-tuple-element.585, bf16[8192,8,128]{0,2,1:T(8,128)(2,1)} %get-tuple-element.593, s32[]{:T(128)S(6)} %select_n.21, f32[256,8,128]{0,2,1:T(8,128)S(1)} %get-tuple-element.571, ...), kind=kOutput, calls=%fused_computation.29.clone.1 | convolution fusion | flops 1087111168 | bytes 23085060 | tf_op jit(solution)/shard_map/while/body/eval_jaxpr/hqk,khe->qhe/dot_general | solution.py:22
  492.9 8.8 %fusion.87 = f32[8,256]{1,0:T(8,128)S(1)} fusion(f32[8,2048,256]{2,1,0:T(8,128)} %get-tuple-element.547, f32[8,256]{1,0:T(8,128)S(1)} %get-tuple-element.585), kind=kLoop, calls=%fused_computation.11.clone.1 | loop fusion | flops 12580864 | bytes 16793600 | tf_op jit(solution)/shard_map/while/body/eval_jaxpr/reduce_sum | solution.py:21
  501.7 8.6 %fusion.86 = f32[8,256]{1,0:T(8,128)S(1)} fusion(f32[8,2048,256]{2,1,0:T(8,128)} %get-tuple-element.544, f32[8,256]{1,0:T(8,128)S(1)} %get-tuple-element.588), kind=kLoop, calls=%fused_computation.13.clone.1 | loop fusion | flops 12580864 | bytes 16793600 | tf_op jit(solution)/shard_map/while/body/eval_jaxpr/reduce_sum | solution.py:21
  510.4 9.7 %bitcast_reduce_fusion.5 = (f32[8,256]{1,0:T(8,128)S(1)}, f32[8,2048,256]{2,1,0:T(8,128)}) fusion(bf16[256,8,64]{0,2,1:T(8,128)(2,1)S(1)} %get-tuple-element.595, bf16[8192,8,64]{0,2,1:T(8,128)(2,1)} %get-tuple-element.594, s32[]{:T(128)S(6)} %select_n.21), kind=kOutput, calls=%fused_computation.5.clone.1 | convolution fusion | flops 545257472 | bytes 19144708 | tf_op jit(solution)/shard_map/while/body/eval_jaxpr/qhd,khd->hqk/dot_general | solution.py:17
  520.1 10.8 %fusion.90 = f32[256,8,128]{0,2,1:T(8,128)S(1)} fusion(f32[8,2048,256]{2,1,0:T(8,128)} %get-tuple-element.544, f32[8,256]{1,0:T(8,128)S(1)} %get-tuple-element.588, bf16[8192,8,128]{0,2,1:T(8,128)(2,1)} %get-tuple-element.593, s32[]{:T(128)S(6)} %select_n.21, f32[256,8,128]{0,2,1:T(8,128)S(1)} %get-tuple-element.574, ...), kind=kOutput, calls=%fused_computation.28.clone.1 | convolution fusion | flops 1087111168 | bytes 23085060 | tf_op jit(solution)/shard_map/while/body/eval_jaxpr/hqk,khe->qhe/dot_general | solution.py:22
  530.9 9.7 %bitcast_reduce_fusion.4 = (f32[8,256]{1,0:T(8,128)S(1)}, f32[8,2048,256]{2,1,0:T(8,128)}) fusion(bf16[256,8,64]{0,2,1:T(8,128)(2,1)S(1)} %get-tuple-element.592, bf16[8192,8,64]{0,2,1:T(8,128)(2,1)} %get-tuple-element.591, s32[]{:T(128)S(6)} %select_n.21), kind=kOutput, calls=%fused_computation.8.clone.1 | convolution fusion | flops 545257472 | bytes 19144708 | tf_op jit(solution)/shard_map/while/body/eval_jaxpr/qhd,khd->hqk/dot_general | solution.py:17
  540.6 9.5 %fusion.89 = f32[256,8,128]{0,2,1:T(8,128)S(1)} fusion(f32[8,2048,256]{2,1,0:T(8,128)} %get-tuple-element.547, f32[8,256]{1,0:T(8,128)S(1)} %get-tuple-element.585, bf16[8192,8,128]{0,2,1:T(8,128)(2,1)} %get-tuple-element.593, s32[]{:T(128)S(6)} %select_n.21, f32[256,8,128]{0,2,1:T(8,128)S(1)} %get-tuple-element.571, ...), kind=kOutput, calls=%fused_computation.29.clone.1 | convolution fusion | flops 1087111168 | bytes 23085060 | tf_op jit(solution)/shard_map/while/body/eval_jaxpr/hqk,khe->qhe/dot_general | solution.py:22
  550.1 8.9 %fusion.87 = f32[8,256]{1,0:T(8,128)S(1)} fusion(f32[8,2048,256]{2,1,0:T(8,128)} %get-tuple-element.547, f32[8,256]{1,0:T(8,128)S(1)} %get-tuple-element.585), kind=kLoop, calls=%fused_computation.11.clone.1 | loop fusion | flops 12580864 | bytes 16793600 | tf_op jit(solution)/shard_map/while/body/eval_jaxpr/reduce_sum | solution.py:21
  567.6 9.7 %bitcast_reduce_fusion.5 = (f32[8,256]{1,0:T(8,128)S(1)}, f32[8,2048,256]{2,1,0:T(8,128)}) fusion(bf16[256,8,64]{0,2,1:T(8,128)(2,1)S(1)} %get-tuple-element.595, bf16[8192,8,64]{0,2,1:T(8,128)(2,1)} %get-tuple-element.594, s32[]{:T(128)S(6)} %select_n.21), kind=kOutput, calls=%fused_computation.5.clone.1 | convolution fusion | flops 545257472 | bytes 19144708 | tf_op jit(solution)/shard_map/while/body/eval_jaxpr/qhd,khd->hqk/dot_general | solution.py:17
  577.4 9.2 %fusion.90 = f32[256,8,128]{0,2,1:T(8,128)S(1)} fusion(f32[8,2048,256]{2,1,0:T(8,128)} %get-tuple-element.544, f32[8,256]{1,0:T(8,128)S(1)} %get-tuple-element.588, bf16[8192,8,128]{0,2,1:T(8,128)(2,1)} %get-tuple-element.593, s32[]{:T(128)S(6)} %select_n.21, f32[256,8,128]{0,2,1:T(8,128)S(1)} %get-tuple-element.574, ...), kind=kOutput, calls=%fused_computation.28.clone.1 | convolution fusion | flops 1087111168 | bytes 23085060 | tf_op jit(solution)/shard_map/while/body/eval_jaxpr/hqk,khe->qhe/dot_general | solution.py:22
  586.5 9.7 %bitcast_reduce_fusion.4 = (f32[8,256]{1,0:T(8,128)S(1)}, f32[8,2048,256]{2,1,0:T(8,128)}) fusion(bf16[256,8,64]{0,2,1:T(8,128)(2,1)S(1)} %get-tuple-element.592, bf16[8192,8,64]{0,2,1:T(8,128)(2,1)} %get-tuple-element.591, s32[]{:T(128)S(6)} %select_n.21), kind=kOutput, calls=%fused_computation.8.clone.1 | convolution fusion | flops 545257472 | bytes 19144708 | tf_op jit(solution)/shard_map/while/body/eval_jaxpr/qhd,khd->hqk/dot_general | solution.py:17
  596.2 9.2 %fusion.89 = f32[256,8,128]{0,2,1:T(8,128)S(1)} fusion(f32[8,2048,256]{2,1,0:T(8,128)} %get-tuple-element.547, f32[8,256]{1,0:T(8,128)S(1)} %get-tuple-element.585, bf16[8192,8,128]{0,2,1:T(8,128)(2,1)} %get-tuple-element.593, s32[]{:T(128)S(6)} %select_n.21, f32[256,8,128]{0,2,1:T(8,128)S(1)} %get-tuple-element.571, ...), kind=kOutput, calls=%fused_computation.29.clone.1 | convolution fusion | flops 1087111168 | bytes 23085060 | tf_op jit(solution)/shard_map/while/body/eval_jaxpr/hqk,khe->qhe/dot_general | solution.py:22
  627.9 9.1 %fusion.55 = f32[256,2816]{1,0:T(8,128)} fusion(bf16[2048,2816]{1,0:T(8,128)(2,1)} %all-gather.15.cloned.1.call-done, f32[256,2048]{1,0:T(8,128)S(1)} %get-tuple-element.427, f32[2048]{0:T(1024)S(1)} %copy-done.1, f32[256]{0:T(256)S(1)} %add_rsqrt_fusion.1, f32[256]{0:T(256)S(1)} %broadcast_multiply_fusion), kind=kOutput, calls=%fused_computation.62 | convolution fusion | flops 2954887168 | bytes 16525312 | tf_op jit(solution)/shard_map/dot_general | solution.py:145
  637.0 8.9 %fusion.53 = bf16[256,2816]{1,0:T(8,128)(2,1)S(1)} fusion(bf16[2048,2816]{1,0:T(8,128)(2,1)} %all-gather.17.cloned.1.call-done, f32[256,2816]{1,0:T(8,128)} %fusion.55, f32[256,2048]{1,0:T(8,128)S(1)} %get-tuple-element.427, f32[2048]{0:T(1024)S(1)} %copy-done.1, f32[256]{0:T(256)S(1)} %add_rsqrt_fusion.1, f32[256]{0:T(256)S(1)} %broadcast_multiply_fusion), kind=kOutput, calls=%fused_computation.49 | convolution fusion | flops 2959212544 | bytes 17967104 | tf_op jit(solution)/shard_map/dot_general | solution.py:146
  646.9 67.1 %while.40 = (s32[]{:T(128)}, bf16[256,2048]{0,1:T(8,128)(2,1)}, pred[16]{0:T(512)(128)(4,1)}, bf16[2816,2048]{1,0:T(8,128)(2,1)}, bf16[256,2816]{1,0:T(8,128)(2,1)S(1)}, /*index=5*/s32[]{:T(128)}) while((s32[]{:T(128)}, bf16[256,2048]{0,1:T(8,128)(2,1)}, pred[16]{0:T(512)(128)(4,1)}, bf16[2816,2048]{1,0:T(8,128)(2,1)}, ...), condition=%wide.region_12.13_spmd, body=%wide.region_9.12_spmd.sunk | while | flops 184549376 | bytes 2294950 | solution.py:76
  (113 shorter events, 145.3 us)
Async XLA Ops:
  6.5 83.5 %all-gather.7.cloned.1.call-start = ((), (), s32[]{:S(2)}) async-start(), calls=%async_computation | async-start | bytes 8650752 | tf_op jit(solution)/shard_map/all_gather | solution.py:112
  7.3 161.3 %all-gather.11.cloned.1.call-start = ((), (), s32[]{:S(2)}) async-start(), calls=%async_computation.2 | async-start | bytes 8650752 | tf_op jit(solution)/shard_map/all_gather | solution.py:113
  8.0 252.6 %all-gather.13.cloned.1.call-start = ((), (), s32[]{:S(2)}) async-start(), calls=%async_computation.3 | async-start | bytes 11894784 | tf_op jit(solution)/shard_map/all_gather | solution.py:162
  8.7 367.5 %all-gather.9.cloned.1.call-start = ((), (), s32[]{:S(2)}) async-start(), calls=%async_computation.1 | async-start | bytes 17301504 | tf_op jit(solution)/shard_map/all_gather | solution.py:114
  9.3 618.6 %all-gather.15.cloned.1.call-start = ((), (), s32[]{:S(2)}) async-start(), calls=%async_computation.4 | async-start | bytes 11894784 | tf_op jit(solution)/shard_map/all_gather | solution.py:102
  9.9 627.1 %all-gather.17.cloned.1.call-start = ((), (), s32[]{:S(2)}) async-start(), calls=%async_computation.5 | async-start | bytes 11894784 | tf_op jit(solution)/shard_map/all_gather | solution.py:103
  397.6 225.1 %copy-start.3 = (f32[8]{0:T(128)S(1)}, f32[8]{0:T(128)}, u32[]{:S(2)}) copy-start(f32[8]{0:T(128)} %param.25) | copy-start | bytes 100
  397.6 225.4 %copy-start.2 = (f32[128]{0:T(128)S(1)}, f32[128]{0:T(128)}, u32[]{:S(2)}) copy-start(f32[128]{0:T(128)} %param.26) | copy-start | bytes 1540
  622.7 2.2 copy-start
  624.9 3.0 copy-start.1
Sparse Core Ops, SparseCore 0:
  10.2 79.7 all-gather.6
  92.8 75.6 all-gather.10
  171.4 89.1 all-gather.12
  263.3 112.9 all-gather.8
  379.0 88.7 all-gather.14
  470.5 89.1 all-gather.16
where the time goes:
time: 727 us; the launch traced here: 724 us
  waiting for transfers between devices  328 us (45%)
  matrix products  214 us (29%)
  local copies, waits for them, and re-layouts  85.4 us (12%)
  other arithmetic  72.1 us (10%)
  between operations  13.6 us (2%)
  loops' own time  10.8 us (1%)
    all_gather x1, waiting for transfers between devices, on_device(): value_rows = lax.all_gather(values, 'sp', axis=0, tiled=True)  100 us
    all_gather x1, waiting for transfers between devices, on_device(): lax.all_gather(down_weight, 'sp', axis=1, tiled=True)  80.3 us
    dot_general x8, matrix products, update(): jnp.einsum('qhd,khd->hqk', queries, keys, preferred_element_type=jnp.floa...  78.1 us
    dot_general x8, matrix products, update(): jnp.einsum('hqk,khe->qhe', weights.astype(jnp.bfloat16), value_rows, pref...  77.3 us
    all_gather x1, waiting for transfers between devices, on_device(): first_keys = lax.all_gather(key_one, 'sp', axis=0, tiled=True)  76.8 us
    reduce_sum x8, other arithmetic, update(): totals = totals * rescale + jnp.sum(weights, axis=-1)  69.1 us
    all_gather x1, waiting for transfers between devices, on_device(): second_keys = lax.all_gather(key_two, 'sp', axis=0, tiled=True)  66.6 us
    dot_general x16, matrix products, project_block(): product = jnp.dot(hidden, slices[0], preferred_element_type=jnp.float32)  38.1 us
  transfers between devices with their start and end apart: 6, of which 4 were waited for; matrix products, arithmetic and copies ran while one was open for 41% of the time, Pallas kernels for 0%

commit v1 on v0

v1 whole, which is shorter than its diff:
```python
import functools
import math

import jax
import jax.numpy as jnp
from jax import lax
from jax.experimental import pallas as pl
from jax.experimental.pallas import tpu as pltpu
from jax.sharding import PartitionSpec as P

ALPHA = 1.4142135623730951
EPSILON = 1e-05
LOG2E = 1.4426950408889634
VMEM_LIMIT = 60 * 1024 * 1024


def pack_kernel(q1, q2, k1, k2, v, out, *, heads, hd, vd):
    for h in range(heads):
        cols = slice(h * hd, (h + 1) * hd)
        out[0, h] = jnp.concatenate([q1[:, cols], q2[:, cols]], axis=1)
        out[1, h] = jnp.concatenate([k1[:, cols], k2[:, cols]], axis=1)
        out[2, h] = v[:, h * vd : (h + 1) * vd]


def pack(q1, q2, k1, k2, v, heads):
    rows = q1.shape[0]
    hd, vd = q1.shape[1] // heads, v.shape[1] // heads
    return pl.pallas_call(
        functools.partial(pack_kernel, heads=heads, hd=hd, vd=vd),
        out_shape=jax.ShapeDtypeStruct((3, heads, rows, vd), jnp.bfloat16),
        compiler_params=pltpu.CompilerParams(vmem_limit_bytes=VMEM_LIMIT),
    )(q1, q2, k1, k2, v)


def attend_kernel(*refs, kb, hd, first, last):
    refs = list(refs)
    q_ref, k_ref, v_ref = refs[:3]
    refs = refs[3:]
    if not first:
        m_in, l_in, o_in = refs[:3]
        refs = refs[3:]
    if last:
        lam_ref, gain_ref, out_ref, vt_ref = refs
    else:
        m_out, l_out, o_out, vt_ref = refs
    qb, kc, vd = q_ref.shape[0], k_ref.shape[0], v_ref.shape[1]
    c = LOG2E * hd**-0.5

    @pl.when(pl.program_id(0) == 0)
    def _():
        vt_ref[...] = v_ref[...].T

    qt = q_ref[...].T
    row = lax.broadcasted_iota(jnp.int32, qt.shape, 0)
    zero = jnp.zeros_like(qt)
    queries = (jnp.where(row < hd, qt, zero), jnp.where(row >= hd, qt, zero))
    state = []
    for a in (0, 1):
        cols = slice(a * qb, (a + 1) * qb)
        if first:
            state.append(
                (
                    jnp.full((1, qb), -1e30, jnp.float32),
                    jnp.zeros((1, qb), jnp.float32),
                    jnp.zeros((vd, qb), jnp.float32),
                )
            )
        else:
            state.append((m_in[:, cols], l_in[:, cols], o_in[:, cols]))

    def scores(step):
        j, a = step
        return jnp.dot(
            k_ref[j * kb : (j + 1) * kb, :], queries[a], preferred_element_type=jnp.float32
        )

    steps = [(j, a) for j in range(kc // kb) for a in (0, 1)]
    s = scores(steps[0])
    for t, (j, a) in enumerate(steps):
        s_next = scores(steps[t + 1]) if t + 1 < len(steps) else None
        m, l, o = state[a]
        m_new = jnp.maximum(m, jnp.max(s, axis=0, keepdims=True))
        p = jnp.exp2((s - m_new) * c)
        scale = jnp.exp2((m - m_new) * c)
        l = l * scale + jnp.sum(p, axis=0, keepdims=True)
        o = o * scale + jnp.dot(
            vt_ref[:, j * kb : (j + 1) * kb],
            p.astype(jnp.bfloat16),
            preferred_element_type=jnp.float32,
        )
        state[a] = (m_new, l, o)
        s = s_next
    if last:
        first_map = state[0][2] / state[0][1]
        second_map = state[1][2] / state[1][1]
        differ = first_map - lam_ref[0, 0] * second_map
        inverse = lax.rsqrt(jnp.mean(differ * differ, axis=0, keepdims=True) + EPSILON)
        attended = differ * inverse * gain_ref[...] * 0.8
        out_ref[...] = attended.T.astype(jnp.bfloat16)
    else:
        for a in (0, 1):
            cols = slice(a * qb, (a + 1) * qb)
            m_out[:, cols], l_out[:, cols], o_out[:, cols] = state[a]


def attend(q, k, v, state, final, hd):
    nq, kc, vd = q.shape[0], k.shape[0], v.shape[1]
    qb = math.gcd(nq, 512)
    kb = math.gcd(kc, 1024)
    wide = lambda r: pl.BlockSpec((r, 2 * qb), lambda i: (0, i))
    whole = lambda a: pl.BlockSpec(a.shape, lambda i: (0, 0))
    args = [q, k, v]
    in_specs = [pl.BlockSpec((qb, q.shape[1]), lambda i: (i, 0)), whole(k), whole(v)]
    aliases = {}
    if state is not None:
        args += list(state)
        in_specs += [wide(1), wide(1), wide(vd)]
    if final is not None:
        lam, gain = final
        args += [lam, gain]
        in_specs += [pl.BlockSpec(memory_space=pltpu.SMEM), whole(gain)]
        out_shape = jax.ShapeDtypeStruct((nq, vd), jnp.bfloat16)
        out_specs = pl.BlockSpec((qb, vd), lambda i: (i, 0))
    else:
        out_shape = [jax.ShapeDtypeStruct((r, 2 * nq), jnp.float32) for r in (1, 1, vd)]
        out_specs = [wide(1), wide(1), wide(vd)]
        if state is not None:
            aliases = {3: 0, 4: 1, 5: 2}
    scores = 2 * nq * kc
    return pl.pallas_call(
        functools.partial(
            attend_kernel, kb=kb, hd=hd, first=state is None, last=final is not None
        ),
        grid=(nq // qb,),
        in_specs=in_specs,
        out_specs=out_specs,
        out_shape=out_shape,
        input_output_aliases=aliases,
        scratch_shapes=[pltpu.VMEM((vd, kc), jnp.bfloat16)],
        compiler_params=pltpu.CompilerParams(
            dimension_semantics=("arbitrary",), vmem_limit_bytes=VMEM_LIMIT
        ),
        cost_estimate=pl.CostEstimate(
            flops=2 * scores * (hd + vd), transcendentals=scores, bytes_accessed=4 * nq * vd * 4
        ),
    )(*args)


def layer_normed(heads_rows, residual_rows, out_weight, norm_gain):
    branch = jnp.dot(heads_rows, out_weight, preferred_element_type=jnp.float32)
    mixed_in = ALPHA * residual_rows.astype(jnp.float32) + branch
    row_mean = jnp.mean(mixed_in, axis=-1, keepdims=True)
    centered = mixed_in - row_mean
    row_var = jnp.mean(centered * centered, axis=-1, keepdims=True)
    return (centered * lax.rsqrt(row_var + EPSILON) * norm_gain).astype(jnp.bfloat16)


def attention(query_one, key_one, query_two, key_two, values, lambdas, head_gain):
    heads = lambdas.shape[0]
    tokens = query_one.shape[0]
    hd, vd = query_one.shape[1] // heads, values.shape[1] // heads
    group = lax.axis_size("sp")
    share = group // heads
    part = tokens // share
    packed = pack(query_one, query_two, key_one, key_two, values, heads)
    packed = packed.reshape(3, group, part, vd)
    mine = lax.all_to_all(packed, "sp", split_axis=1, concat_axis=1, tiled=True)
    mine = mine.reshape(3, group * part, vd)
    chunks = {0: mine[1:]}
    for mask in range(1, share):
        low = mask & -mask
        ring = [(i, i ^ low) for i in range(group)]
        chunks[mask] = lax.ppermute(chunks[mask - low], "sp", ring)
    head = lax.axis_index("sp") // share
    lam = lax.dynamic_slice_in_dim(lambdas, head, 1).reshape(1, 1)
    final = (lam, head_gain.reshape(vd, 1))
    order = [0, 1] + list(range(2, share)) if share > 1 else [0]
    state = None
    for n, mask in enumerate(order):
        kv = chunks[mask]
        state = attend(
            mine[0], kv[0], kv[1], state, final if n + 1 == len(order) else None, hd
        )
    back = lax.all_to_all(
        state.reshape(group, part, vd), "sp", split_axis=0, concat_axis=0, tiled=True
    )
    return (
        back.reshape(heads, share, part, vd)
        .transpose(1, 2, 0, 3)
        .reshape(tokens, heads * vd)
    )


def on_device(
    stream,
    query_one,
    key_one,
    query_two,
    key_two,
    values,
    lambdas,
    head_gain,
    out_weight,
    norm_gain,
    gate_weight,
    up_weight,
    down_weight,
):
    gate_full = lax.all_gather(gate_weight, "sp", axis=0, tiled=True)
    up_full = lax.all_gather(up_weight, "sp", axis=0, tiled=True)
    down_full = lax.all_gather(down_weight.T, "sp", axis=0, tiled=True)
    attended = attention(
        query_one, key_one, query_two, key_two, values, lambdas, head_gain
    )
    by_rows = lax.all_to_all(attended, "tp", split_axis=0, concat_axis=1, tiled=True)
    own_normed = layer_normed(by_rows, stream, out_weight, norm_gain)
    normed_all = lax.all_gather(own_normed, "tp", axis=0, tiled=True)
    gate_out = jnp.dot(normed_all, gate_full, preferred_element_type=jnp.float32)
    upward = jnp.dot(normed_all, up_full, preferred_element_type=jnp.float32)
    hidden = (jax.nn.silu(gate_out) * upward).astype(jnp.bfloat16)
    partial_terms = lax.dot_general(
        hidden, down_full, (((1,), (1,)), ((), ())), preferred_element_type=jnp.float32
    )
    mixer_out = lax.psum_scatter(
        partial_terms.astype(jnp.bfloat16), "tp", scatter_dimension=0, tiled=True
    ).astype(jnp.float32)
    return (ALPHA * own_normed.astype(jnp.float32) + 0.5 * mixer_out).astype(jnp.bfloat16)


def solution(mesh):
    return jax.shard_map(
        on_device,
        mesh=mesh,
        in_specs=(
            P(("sp", "tp"), None),
            P("sp", "tp"),
            P("sp", "tp"),
            P("sp", "tp"),
            P("sp", "tp"),
            P("sp", "tp"),
            P("tp"),
            P(),
            P(),
            P(),
            P("sp", "tp"),
            P("sp", "tp"),
            P("tp", "sp"),
        ),
        out_specs=P(("sp", "tp"), None),
        check_vma=False,
    )
```

time: 727 us -> 357 us (0.49)
  matrix products: 214 us -> 29.4 us
  waiting for transfers between devices: 328 us -> 147 us
  blocking collectives: 0 us -> 91.4 us
  local copies, waits for them, and re-layouts: 85.4 us -> 10.2 us
  other arithmetic: 72.1 us -> 0.36 us
  Pallas kernels: 0 us -> 64.2 us
  loops' own time: 10.8 us -> 0 us
    all_gather x6 -> x3, waiting for transfers between devices: 324 us -> 116 us  [the longest x1 92.1 us: on_device(): down_full = lax.all_gather(down_weight.T, 'sp', axis=0, tiled=True)]
    dot_general x33 -> x1, matrix products: 202 us -> 15.7 us  [on_device(): lax.dot_general(hidden, down_full, (((1,), (1,)), ((), ())), preferred_el...]
    all_to_all x0 -> x2, blocking collectives: none -> 91.4 us  [the longest x1 68.3 us: attention(): mine = lax.all_to_all(packed, 'sp', split_axis=1, concat_axis=1, tiled=True)]
    reduce_sum x9 -> x0, other arithmetic: 69.3 us -> none  [the longest x8 69.1 us: update(): totals = totals * rescale + jnp.sum(weights, axis=-1)]
    pallas_call x0 -> x5, Pallas kernels: none -> 64.2 us  [the longest x4 61.3 us: attend(): pl.pallas_call(functools.partial(attend_kernel, kb=kb, hd=hd, first=state...]
    all_gather x3 -> x0, local copies, waits for them, and re-layouts: 45 us -> none  [the longest x1 21.3 us: on_device(): value_rows = lax.all_gather(values, 'sp', axis=0, tiled=True)]
    ppermute x0 -> x3, waiting for transfers between devices: none -> 28.4 us  [attention(): chunks[mask] = lax.ppermute(chunks[mask - low], 'sp', ring)]
    dynamic_slice x16 -> x1, local copies, waits for them, and re-layouts: 18.6 us -> 0.58 us  [attention(): lam = lax.dynamic_slice_in_dim(lambdas, head, 1).reshape(1, 1)]
  transfers between devices with their start and end apart: 6 -> 6, of which waited for: 4 -> 3; matrix products, arithmetic and copies ran while one was open for 41% -> 7% of each run, Pallas kernels for 0% -> 18%
where the time goes in v1:
time: 357 us; the launch traced here: 356 us
  waiting for transfers between devices  147 us (41%)
  blocking collectives  91.4 us (26%)
  Pallas kernels  64.2 us (18%)
  matrix products  29.4 us (8%)
  between operations  13.2 us (4%)
  local copies, waits for them, and re-layouts  10.2 us (3%)
    all_gather x1, waiting for transfers between devices, on_device(): down_full = lax.all_gather(down_weight.T, 'sp', axis=0, tiled=True)  92.1 us
    all_to_all x1, blocking collectives, attention(): mine = lax.all_to_all(packed, 'sp', split_axis=1, concat_axis=1, tiled=True)  68.3 us
    pallas_call x4, Pallas kernels, attend(): pl.pallas_call(functools.partial(attend_kernel, kb=kb, hd=hd, first=state...  61.3 us
    ppermute x3, waiting for transfers between devices, attention(): chunks[mask] = lax.ppermute(chunks[mask - low], 'sp', ring)  28.4 us
    all_gather x1, waiting for transfers between devices, on_device(): up_full = lax.all_gather(up_weight, 'sp', axis=0, tiled=True)  24 us
    all_to_all x1, blocking collectives, attention(): lax.all_to_all(state.reshape(group, part, vd), 'sp', split_axis=0, concat...  23 us
    dot_general x1, matrix products, on_device(): lax.dot_general(hidden, down_full, (((1,), (1,)), ((), ())), preferred_el...  15.7 us
    dot_general x1, matrix products, on_device(): jnp.dot(normed_all, gate_full, preferred_element_type=jnp.float32)  9.25 us
  transfers between devices with their start and end apart: 6, of which 3 were waited for; matrix products, arithmetic and copies ran while one was open for 7% of the time, Pallas kernels for 18%

profile of v1, /device:TPU:0, one launch (start us, length us, event | category | flops | bytes accessed | tf_op | source)
XLA Modules:
  0.0 356.3 jit_solution(16895764541980134754)
XLA Ops:
  6.5 0.7 all-gather.4.cloned.1.call-update
  7.3 0.0 all-gather.6.cloned.1.call-start
  7.3 0.7 all-gather.6.cloned.1.call-update
  8.0 0.0 all-gather.8.cloned.1.call-start
  8.1 0.7 all-gather.8.cloned.1.call-update
  8.7 2.9 shard_map.127
  11.7 1.5 copy.24
  13.2 68.3 %all_to_all.10 = bf16[3,32,64,128]{3,2,0,1:T(8,128)(2,1)S(1)} all-to-all(bf16[3,32,64,128]{3,2,0,1:T(8,128)(2,1)S(1)} %copy.24), channel_id=1, replica_groups=mesh['sp'=32,'tp'=1] {'sp'}, dimensions={1} | all-to-all | bytes 3145728 | tf_op jit(solution)/shard_map/all_to_all | solution.py:167
  81.5 0.1 slice.53
  81.6 1.1 copy.25
  82.7 0.8 collective-permute-start
  83.5 0.1 collective-permute-start.2
  83.6 0.7 copy.26.refs_7_
  84.3 0.6 dynamic_slice.3
  84.9 1.2 fusion.9
  86.1 13.8 %shard_map.128 = (f32[1,4096]{1,0:T(1,128)}, f32[1,4096]{1,0:T(1,128)}, f32[128,4096]{1,0:T(8,128)}) custom-call(bf16[2048,128]{1,0:T(8,128)(2,1)} %bitcast.39, bf16[2048,128]{1,0:T(8,128)(2,1)} %bitcast.44, bf16[2048,128]{1,0:T(8,128)(2,1)} %bitcast.43), custom_call_target="tpu_custom_call" | custom-call | flops 3221225472 | bytes 4194304 | tf_op jit(solution)/shard_map/pallas_call | solution.py:130
  99.9 28.4 %collective-permute-done = bf16[2,2048,128]{2,1,0:T(8,128)(2,1)S(1)} collective-permute-done((bf16[2,2048,128]{2,1,0:T(8,128)(2,1)}, bf16[2,2048,128]{2,1,0:T(8,128)(2,1)S(1)}, u32[]{:S(2)}, u32[]{:S(2)}) %collective-permute-start) | collective-permute-done | bytes 1048608 | tf_op jit(solution)/shard_map/ppermute | solution.py:173
  128.3 2.3 slice_bitcast_fusion
  130.6 15.4 %shard_map.129 = (f32[1,4096]{1,0:T(1,128)}, f32[1,4096]{1,0:T(1,128)}, f32[128,4096]{1,0:T(8,128)}) custom-call(bf16[2048,128]{1,0:T(8,128)(2,1)} %bitcast.40, bf16[2048,128]{1,0:T(8,128)(2,1)} %get-tuple-element.27.refs_1_, bf16[2048,128]{1,0:T(8,128)(2,1)} %get-tuple-element.26.refs_2_, ...), custom_call_target="tpu_custom_call", output_to_operand_aliasing={{0}: (3, {}), {1}: (4, {}), {2}: (5, {})} | custom-call | flops 3221225472 | bytes 4194304 | tf_op jit(solution)/shard_map/pallas_call | solution.py:130
  146.1 1.1 slice_bitcast_fusion.2
  147.1 15.4 %shard_map.130 = (f32[1,4096]{1,0:T(1,128)}, f32[1,4096]{1,0:T(1,128)}, f32[128,4096]{1,0:T(8,128)}) custom-call(bf16[2048,128]{1,0:T(8,128)(2,1)} %bitcast.41, bf16[2048,128]{1,0:T(8,128)(2,1)} %get-tuple-element.29.refs_1_, bf16[2048,128]{1,0:T(8,128)(2,1)} %get-tuple-element.28.refs_2_, ...), custom_call_target="tpu_custom_call", output_to_operand_aliasing={{0}: (3, {}), {1}: (4, {}), {2}: (5, {})} | custom-call | flops 3221225472 | bytes 4194304 | tf_op jit(solution)/shard_map/pallas_call | solution.py:130
  162.6 1.1 slice_bitcast_fusion.4
  163.6 16.6 %shard_map.131 = bf16[2048,128]{1,0:T(8,128)(2,1)} custom-call(bf16[2048,128]{1,0:T(8,128)(2,1)} %bitcast.42, bf16[2048,128]{1,0:T(8,128)(2,1)} %get-tuple-element.31.refs_1_, bf16[2048,128]{1,0:T(8,128)(2,1)} %get-tuple-element.30.refs_2_, f32[1,4096]{1,0:T(1,128)} %get-tuple-element.20.refs_3_, f32[1,4096]{1,0:T(1,128)} %get-tuple-element.21.refs_4_, ...), custom_call_target="tpu_custom_call" | custom-call | flops 3221225472 | bytes 4194304 | tf_op jit(solution)/shard_map/pallas_call | solution.py:130
  180.2 23.0 %all_to_all.11 = bf16[32,64,128]{2,1,0:T(8,128)(2,1)S(1)} all-to-all(bf16[32,64,128]{2,1,0:T(8,128)(2,1)} %bitcast.37), channel_id=1, replica_groups=mesh['sp'=32,'tp'=1] {'sp'}, dimensions={0} | all-to-all | bytes 1048576 | tf_op jit(solution)/shard_map/all_to_all | solution.py:184
  203.3 0.3 copy.27
  203.6 4.5 %fusion.10 = (f32[256]{0:T(256)S(1)}, f32[256,2048]{1,0:T(8,128)S(1)}) fusion(bf16[1024,2048]{1,0:T(8,128)(2,1)} %param.21, bf16[32,8,8,128]{3,2,1,0:T(8,128)(2,1)S(1)} %bitcast.38, bf16[256,2048]{1,0:T(8,128)(2,1)S(1)} %copy-done.1), kind=kOutput, calls=%fused_computation.23 | convolution fusion | flops 1075838720 | bytes 7865344 | tf_op jit(solution)/shard_map/dot_general | solution.py:150
  208.1 0.3 multiply_reduce_fusion
  208.5 0.3 copy-done.2
  208.8 9.2 %fusion.8 = f32[256,2816]{1,0:T(8,128)} fusion(bf16[2048,2816]{1,0:T(8,128)(2,1)} %all-gather.4.cloned.1.call-done, f32[256,2048]{1,0:T(8,128)S(1)} %get-tuple-element.33, f32[2048]{0:T(1024)S(1)} %copy-done.2, f32[256]{0:T(256)S(1)} %add_rsqrt_fusion, f32[256]{0:T(256)S(1)} %broadcast_multiply_fusion), kind=kOutput, calls=%fused_computation.21 | convolution fusion | flops 2954887168 | bytes 16525312 | tf_op jit(solution)/shard_map/dot_general | solution.py:218
  218.0 24.0 %all-gather.6.cloned.1.call-done = bf16[2048,2816]{1,0:T(8,128)(2,1)} async-done(((bf16[64,2816]{1,0:T(8,128)(2,1)}), bf16[2048,2816]{1,0:T(8,128)(2,1)}) %all-gather.6.cloned.1.call-update) | async-done | bytes 11534352 | tf_op jit(solution)/shard_map/all_gather | solution.py:210
  242.0 92.1 %all-gather.8.cloned.1.call-done = bf16[2048,2816]{1,0:T(8,128)(2,1)} async-done(((bf16[64,2816]{1,0:T(8,128)(2,1)}), bf16[2048,2816]{1,0:T(8,128)(2,1)}) %all-gather.8.cloned.1.call-update) | async-done | bytes 11534352 | tf_op jit(solution)/shard_map/all_gather | solution.py:211
  334.1 15.7 %fusion.4 = bf16[256,2048]{1,0:T(8,128)(2,1)} fusion(bf16[2048,2816]{1,0:T(8,128)(2,1)} %all-gather.8.cloned.1.call-done, bf16[2048,2816]{1,0:T(8,128)(2,1)} %all-gather.6.cloned.1.call-done, f32[256,2816]{1,0:T(8,128)} %fusion.8, f32[2048]{0:T(1024)S(1)} %copy-done.2, f32[256]{0:T(256)S(1)} %add_rsqrt_fusion, f32[256,2048]{1,0:T(8,128)S(1)} %get-tuple-element.33, ...), kind=kOutput, calls=%fused_computation.7 | convolution fusion | flops 5917769728 | bytes 29108224 | tf_op jit(solution)/shard_map/dot_general | solution.py:221
  (14 shorter events, 0.1 us)
Async XLA Ops:
  6.5 202.0 %all-gather.4.cloned.1.call-start = ((), (), s32[]{:S(2)}) async-start(), calls=%async_computation.2 | async-start | bytes 11894784 | tf_op jit(solution)/shard_map/all_gather | solution.py:209
  7.3 234.7 %all-gather.6.cloned.1.call-start = ((), (), s32[]{:S(2)}) async-start(), calls=%async_computation.3 | async-start | bytes 11894784 | tf_op jit(solution)/shard_map/all_gather | solution.py:210
  8.0 326.1 %all-gather.8.cloned.1.call-start = ((), (), s32[]{:S(2)}) async-start(), calls=%async_computation.4 | async-start | bytes 11894784 | tf_op jit(solution)/shard_map/all_gather | solution.py:211
  81.5 2.1 copy-start
  81.5 2.8 copy-start.3
  82.7 45.7 %collective-permute-start = (bf16[2,2048,128]{2,1,0:T(8,128)(2,1)}, bf16[2,2048,128]{2,1,0:T(8,128)(2,1)S(1)}, u32[]{:S(2)}, u32[]{:S(2)}) collective-permute-start(bf16[2,2048,128]{2,1,0:T(8,128)(2,1)} %bitcast.2), channel_id=1, source_target_pairs={{0,2},{1,3},{2,0},{3,1},{4,6},{5,7},{6,4},{7,5},{8,10},{9,11},{10,... | collective-permute-start | bytes 3145736 | tf_op jit(solution)/shard_map/ppermute | solution.py:173
  83.5 44.9 %collective-permute-start.2 = (bf16[2,2048,128]{2,1,0:T(8,128)(2,1)}, bf16[2,2048,128]{2,1,0:T(8,128)(2,1)}, u32[]{:S(2)}, u32[]{:S(2)}) collective-permute-start(bf16[2,2048,128]{2,1,0:T(8,128)(2,1)} %bitcast.2), channel_id=1, source_target_pairs={{0,1},{1,0},{2,3},{3,2},{4,5},{5,4},{6,7},{7,6},{8,9},{9,8},{10,11... | collective-permute-start | bytes 3145736 | tf_op jit(solution)/shard_map/ppermute | solution.py:173
  128.3 34.2 %collective-permute-start.1 = (bf16[2,2048,128]{2,1,0:T(8,128)(2,1)S(1)}, bf16[2,2048,128]{2,1,0:T(8,128)(2,1)S(1)}, u32[]{:S(2)}, u32[]{:S(2)}) collective-permute-start(bf16[2,2048,128]{2,1,0:T(8,128)(2,1)S(1)} %collective-permute-done), channel_id=1, source_target_pairs={{0,1},{1,0},{2,3},{3,2},{4,5},{5,4},{6,7},{7,6},{8,9},{9,8},{10,11... | collective-permute-start | bytes 3145736 | tf_op jit(solution)/shard_map/ppermute | solution.py:173
  180.2 23.4 %copy-start.1 = (bf16[256,2048]{1,0:T(8,128)(2,1)S(1)}, bf16[256,2048]{1,0:T(8,128)(2,1)}, u32[]{:S(2)}) copy-start(bf16[256,2048]{1,0:T(8,128)(2,1)} %param.13) | copy-start | bytes 3145732
  208.1 0.7 copy-start.2
Sparse Core Ops, SparseCore 0:
  10.2 132.8 all-gather.3
  145.9 96.0 all-gather.5
  244.9 89.1 all-gather.7

commit v2 on v1

--- a/solution.py
+++ b/solution.py
@@ -17,9 +17,9 @@
 def pack_kernel(q1, q2, k1, k2, v, out, *, heads, hd, vd):
     for h in range(heads):
         cols = slice(h * hd, (h + 1) * hd)
-        out[0, h] = jnp.concatenate([q1[:, cols], q2[:, cols]], axis=1)
-        out[1, h] = jnp.concatenate([k1[:, cols], k2[:, cols]], axis=1)
-        out[2, h] = v[:, h * vd : (h + 1) * vd]
+        out[h, 0] = jnp.concatenate([q1[:, cols], q2[:, cols]], axis=1)
+        out[h, 1] = jnp.concatenate([k1[:, cols], k2[:, cols]], axis=1)
+        out[h, 2] = v[:, h * vd : (h + 1) * vd]
 
 
 def pack(q1, q2, k1, k2, v, heads):
@@ -27,9 +27,108 @@
     hd, vd = q1.shape[1] // heads, v.shape[1] // heads
     return pl.pallas_call(
         functools.partial(pack_kernel, heads=heads, hd=hd, vd=vd),
-        out_shape=jax.ShapeDtypeStruct((3, heads, rows, vd), jnp.bfloat16),
+        out_shape=jax.ShapeDtypeStruct((heads, 3, rows, vd), jnp.bfloat16),
         compiler_params=pltpu.CompilerParams(vmem_limit_bytes=VMEM_LIMIT),
     )(q1, q2, k1, k2, v)
+
+
+def pack_weights_kernel(place, gate, up, down, *outs_and_buf):
+    outs, buf = outs_and_buf[:-1], outs_and_buf[-1]
+    width = gate.shape[1] // len(outs)
+    for p in range(len(outs)):
+        cols = slice(p * width, (p + 1) * width)
+        slot = jnp.bitwise_xor(place[0], p)
+        buf[slot, 0] = gate[:, cols]
+        buf[slot, 1] = up[:, cols]
+        buf[slot, 2] = down[cols, :].T
+    for p, out in enumerate(outs):
+        out[...] = buf[p]
+
+
+def pack_weights(place, gate, up, down, parts):
+    rows, ff = gate.shape
+    piece = (3, rows, ff // parts)
+    return pl.pallas_call(
+        pack_weights_kernel,
+        in_specs=[pl.BlockSpec(memory_space=pltpu.SMEM)] + [pl.BlockSpec()] * 3,
+        out_shape=[jax.ShapeDtypeStruct(piece, jnp.bfloat16)] * parts,
+        scratch_shapes=[pltpu.VMEM((parts,) + piece, jnp.bfloat16)],
+        compiler_params=pltpu.CompilerParams(vmem_limit_bytes=VMEM_LIMIT),
+    )(place, gate, up, down)
+
+
+def assemble_kernel(place, *refs):
+    parts, out = refs[:-1], refs[-1]
+    rows = parts[0].shape[1]
+    for p, part in enumerate(parts):
+        at = pl.multiple_of(jnp.bitwise_xor(place[0], p) * rows, rows)
+        out[:, pl.ds(at, rows), :] = part[...]
+
+
+def assemble(place, parts):
+    kinds, rows, width = parts[0].shape
+    return pl.pallas_call(
+        assemble_kernel,
+        in_specs=[pl.BlockSpec(memory_space=pltpu.SMEM)] + [pl.BlockSpec()] * len(parts),
+        out_shape=jax.ShapeDtypeStruct((kinds, len(parts) * rows, width), jnp.bfloat16),
+        compiler_params=pltpu.CompilerParams(vmem_limit_bytes=VMEM_LIMIT),
+    )(place, *parts)
+
+
+def mixer_kernel(base, *refs, masks, far, rows):
+    weights = refs[: len(masks)]
+    xa, xb, out_a, out_b, buf, sems = refs[len(masks) :]
+    kinds = (slice(0, 2), slice(2, 3))
+
+    def copies(part):
+        for m, mask in enumerate(masks):
+            for n, f in enumerate((0, far)):
+                at = (jnp.bitwise_xor(base[0], mask) + f) * rows
+                at = pl.multiple_of(at, 2 * rows)
+                yield pltpu.make_async_copy(
+                    weights[m].at[kinds[part], pl.ds(n * 2 * rows, 2 * rows)],
+                    buf.at[kinds[part], pl.ds(at, 2 * rows)],
+                    sems.at[part, 2 * m + n],
+                )
+
+    for part in (0, 1):
+        for copy in copies(part):
+            copy.start()
+    for copy in copies(0):
+        copy.wait()
+    hidden = []
+    for x in (xa, xb):
+        gate = jnp.dot(x[...], buf[0], preferred_element_type=jnp.float32)
+        up = jnp.dot(x[...], buf[1], preferred_element_type=jnp.float32)
+        hidden.append((gate / (1.0 + jnp.exp(-gate)) * up).astype(jnp.bfloat16))
+    for copy in copies(1):
+        copy.wait()
+    for h, out in zip(hidden, (out_a, out_b)):
+        out[...] = lax.dot_general(
+            h, buf[2], (((1,), (1,)), ((), ())), preferred_element_type=jnp.float32
+        ).astype(jnp.bfloat16)
+
+
+def mixer(base, xa, xb, weights, masks, far):
+    kinds, block, width = weights[0].shape
+    n, d = xa.shape
+    return pl.pallas_call(
+        functools.partial(mixer_kernel, masks=masks, far=far, rows=block // 4),
+        in_specs=[pl.BlockSpec(memory_space=pltpu.SMEM)]
+        + [pl.BlockSpec(memory_space=pl.ANY)] * len(masks)
+        + [pl.BlockSpec()] * 2,
+        out_shape=[jax.ShapeDtypeStruct((n, d), jnp.bfloat16)] * 2,
+        scratch_shapes=[
+            pltpu.VMEM((kinds, d, width), jnp.bfloat16),
+            pltpu.SemaphoreType.DMA((2, 2 * len(masks))),
+        ],
+        compiler_params=pltpu.CompilerParams(vmem_limit_bytes=VMEM_LIMIT),
+        cost_estimate=pl.CostEstimate(
+            flops=12 * n * d * width,
+            transcendentals=2 * n * width,
+            bytes_accessed=2 * kinds * d * width,
+        ),
+    )(base, *weights, xa, xb)
 
 
 def attend_kernel(*refs, kb, hd, first, last):
@@ -43,14 +142,17 @@
         lam_ref, gain_ref, out_ref, vt_ref = refs
     else:
         m_out, l_out, o_out, vt_ref = refs
-    qb, kc, vd = q_ref.shape[0], k_ref.shape[0], v_ref.shape[1]
+    vd = q_ref.shape[-1]
+    qb = q_ref.shape[0] * q_ref.shape[2]
+    kc = k_ref.shape[0] * k_ref.shape[2]
     c = LOG2E * hd**-0.5
+    keys = k_ref.reshape(kc, vd)
 
     @pl.when(pl.program_id(0) == 0)
     def _():
-        vt_ref[...] = v_ref[...].T
-
-    qt = q_ref[...].T
+        vt_ref[...] = v_ref[...].reshape(kc, vd).T
+
+    qt = q_ref[...].reshape(qb, vd).T
     row = lax.broadcasted_iota(jnp.int32, qt.shape, 0)
     zero = jnp.zeros_like(qt)
     queries = (jnp.where(row < hd, qt, zero), jnp.where(row >= hd, qt, zero))
@@ -71,7 +173,7 @@
     def scores(step):
         j, a = step
         return jnp.dot(
-            k_ref[j * kb : (j + 1) * kb, :], queries[a], preferred_element_type=jnp.float32
+            keys[j * kb : (j + 1) * kb, :], queries[a], preferred_element_type=jnp.float32
         )
 
     steps = [(j, a) for j in range(kc // kb) for a in (0, 1)]
@@ -103,14 +205,22 @@
             m_out[:, cols], l_out[:, cols], o_out[:, cols] = state[a]
 
 
-def attend(q, k, v, state, final, hd):
-    nq, kc, vd = q.shape[0], k.shape[0], v.shape[1]
-    qb = math.gcd(nq, 512)
+def attend(q, kv, state, final, hd):
+    blocks, _, rows, vd = q.shape
+    nq, kc = blocks * rows, kv.shape[0] * kv.shape[2]
+    step = max(1, math.gcd(blocks, 512 // rows))
+    qb = step * rows
     kb = math.gcd(kc, 1024)
     wide = lambda r: pl.BlockSpec((r, 2 * qb), lambda i: (0, i))
     whole = lambda a: pl.BlockSpec(a.shape, lambda i: (0, 0))
-    args = [q, k, v]
-    in_specs = [pl.BlockSpec((qb, q.shape[1]), lambda i: (i, 0)), whole(k), whole(v)]
+    kinds = kv.shape[1]
+    kind = lambda n: pl.BlockSpec((kv.shape[0], 1, rows, vd), lambda i: (0, n, 0, 0))
+    args = [q, kv, kv]
+    in_specs = [
+        pl.BlockSpec((step, 1, rows, vd), lambda i: (i, 0, 0, 0)),
+        kind(kinds - 2),
+        kind(kinds - 1),
+    ]
     aliases = {}
     if state is not None:
         args += list(state)
@@ -155,40 +265,42 @@
     return (centered * lax.rsqrt(row_var + EPSILON) * norm_gain).astype(jnp.bfloat16)
 
 
-def attention(query_one, key_one, query_two, key_two, values, lambdas, head_gain):
-    heads = lambdas.shape[0]
-    tokens = query_one.shape[0]
-    hd, vd = query_one.shape[1] // heads, values.shape[1] // heads
+def swap(x, mask):
     group = lax.axis_size("sp")
-    share = group // heads
-    part = tokens // share
-    packed = pack(query_one, query_two, key_one, key_two, values, heads)
-    packed = packed.reshape(3, group, part, vd)
-    mine = lax.all_to_all(packed, "sp", split_axis=1, concat_axis=1, tiled=True)
-    mine = mine.reshape(3, group * part, vd)
-    chunks = {0: mine[1:]}
-    for mask in range(1, share):
-        low = mask & -mask
-        ring = [(i, i ^ low) for i in range(group)]
-        chunks[mask] = lax.ppermute(chunks[mask - low], "sp", ring)
-    head = lax.axis_index("sp") // share
-    lam = lax.dynamic_slice_in_dim(lambdas, head, 1).reshape(1, 1)
-    final = (lam, head_gain.reshape(vd, 1))
-    order = [0, 1] + list(range(2, share)) if share > 1 else [0]
+    return lax.ppermute(x, "sp", [(i, i ^ mask) for i in range(group)])
+
+
+def subsets(bits):
+    return [sum(b for j, b in enumerate(bits) if n >> j & 1) for n in range(1 << len(bits))]
+
+
+def rank(index, bits):
+    return sum((index // b % 2) << j for j, b in enumerate(bits))
+
+
+def attention(packed, lambdas, head_gain, share_bits, head_bits):
+    heads, _, tokens, vd = packed.shape
+    peers = [[s + h for h in subsets(head_bits)] for s in subsets(share_bits)]
+
+    def exchange(x):
+        return lax.all_to_all(
+            x, "sp", split_axis=0, concat_axis=0, axis_index_groups=peers, tiled=True
+        )
+
+    mine = exchange(packed)
+    chunks = {0: mine[:, 1:]}
+    share = 1 << len(share_bits)
+    for n in range(1, share):
+        low = n & -n
+        chunks[n] = swap(chunks[n - low], share_bits[low.bit_length() - 1])
+    lam = lax.dynamic_slice_in_dim(lambdas, rank(lax.axis_index("sp"), head_bits), 1)
+    final = (lam.reshape(1, 1), head_gain.reshape(vd, 1))
     state = None
-    for n, mask in enumerate(order):
-        kv = chunks[mask]
-        state = attend(
-            mine[0], kv[0], kv[1], state, final if n + 1 == len(order) else None, hd
-        )
-    back = lax.all_to_all(
-        state.reshape(group, part, vd), "sp", split_axis=0, concat_axis=0, tiled=True
-    )
-    return (
-        back.reshape(heads, share, part, vd)
-        .transpose(1, 2, 0, 3)
-        .reshape(tokens, heads * vd)
-    )
+    for n in range(share):
+        kv = mine if n == 0 else chunks[n]
+        state = attend(mine, kv, state, final if n + 1 == share else None, vd // 2)
+    back = exchange(state.reshape(heads, tokens, vd))
+    return back.transpose(1, 0, 2).reshape(tokens, heads * vd)
 
 
 def on_device(
@@ -206,25 +318,56 @@
     up_weight,
     down_weight,
 ):
-    gate_full = lax.all_gather(gate_weight, "sp", axis=0, tiled=True)
-    up_full = lax.all_gather(up_weight, "sp", axis=0, tiled=True)
-    down_full = lax.all_gather(down_weight.T, "sp", axis=0, tiled=True)
-    attended = attention(
-        query_one, key_one, query_two, key_two, values, lambdas, head_gain
-    )
+    heads = lambdas.shape[0]
+    group = lax.axis_size("sp")
+    device = lax.axis_index("sp")
+    far = group // 4
+    others = [1 << n for n in range(1, group.bit_length() - 1) if 1 << n != far]
+    group_bits = [1, far]
+    ordered = group_bits + others
+    n_head_bits = heads.bit_length() - 1
+    share_bits = ordered[: len(ordered) - n_head_bits]
+    head_bits = sorted(ordered[len(ordered) - n_head_bits :])
+    place = rank(device, group_bits).reshape(1)
+    base = (device - device % 2 - (device // far % 2) * far).reshape(1)
+
+    pieces = pack_weights(place, gate_weight, up_weight, down_weight, 4)
+    parts = [pieces[0]]
+    for n, mask in ((1, 1), (2, far), (3, far + 1)):
+        parts.append(swap(pieces[n], mask))
+    block = assemble(place, parts)
+    top, lower = others[-1], subsets(others[:-1])[1:]
+    weights = {0: block, top: swap(block, top)}
+    for mask in lower:
+        weights[mask] = swap(block, mask)
+    for mask in lower:
+        weights[top + mask] = swap(weights[top], mask)
+
+    packed = pack(query_one, query_two, key_one, key_two, values, heads)
+    attended = attention(packed, lambdas, head_gain, share_bits, head_bits)
     by_rows = lax.all_to_all(attended, "tp", split_axis=0, concat_axis=1, tiled=True)
     own_normed = layer_normed(by_rows, stream, out_weight, norm_gain)
-    normed_all = lax.all_gather(own_normed, "tp", axis=0, tiled=True)
-    gate_out = jnp.dot(normed_all, gate_full, preferred_element_type=jnp.float32)
-    upward = jnp.dot(normed_all, up_full, preferred_element_type=jnp.float32)
-    hidden = (jax.nn.silu(gate_out) * upward).astype(jnp.bfloat16)
-    partial_terms = lax.dot_general(
-        hidden, down_full, (((1,), (1,)), ((), ())), preferred_element_type=jnp.float32
+    own = lax.all_gather(own_normed, "tp", axis=0, tiled=True)
+
+    masks = subsets(others)
+    gathered = [weights[mask] for mask in masks]
+    near, away = swap(own, 1), swap(own, far)
+    near_out, own_out = mixer(base, near, own, gathered, masks, far)
+    given = swap(near_out, 1)
+    away, own_out = lax.optimization_barrier((away, own_out))
+    both = swap(away, 1)
+    both_out, away_out = mixer(base, both, away, gathered, masks, far)
+    handed = swap(both_out, 1)
+    summed = away_out.astype(jnp.float32) + handed.astype(jnp.float32)
+    sent = swap(summed.astype(jnp.bfloat16), far)
+    partial_terms = (
+        own_out.astype(jnp.float32) + given.astype(jnp.float32) + sent.astype(jnp.float32)
     )
-    mixer_out = lax.psum_scatter(
-        partial_terms.astype(jnp.bfloat16), "tp", scatter_dimension=0, tiled=True
-    ).astype(jnp.float32)
-    return (ALPHA * own_normed.astype(jnp.float32) + 0.5 * mixer_out).astype(jnp.bfloat16)
+    if lax.axis_size("tp") > 1:
+        partial_terms = lax.psum_scatter(
+            partial_terms.astype(jnp.bfloat16), "tp", scatter_dimension=0, tiled=True
+        ).astype(jnp.float32)
+    return (ALPHA * own_normed.astype(jnp.float32) + 0.5 * partial_terms).astype(jnp.bfloat16)
 
 
 def solution(mesh):

time: 357 us -> 319 us (0.89)
  blocking collectives: 91.4 us -> 45.8 us
  Pallas kernels: 64.2 us -> 91.1 us
  matrix products: 29.4 us -> 3.84 us
  starting transfers between devices: 1.03 us -> 21.1 us
  waiting for transfers between devices: 147 us -> 128 us
  local copies, waits for them, and re-layouts: 10.2 us -> 23.6 us
  between operations: 13.2 us -> 0.2 us
  other arithmetic: 0.36 us -> 5.26 us
    all_gather x3 -> x0, waiting for transfers between devices: 116 us -> none  [the longest x1 92.1 us: on_device(): down_full = lax.all_gather(down_weight.T, 'sp', axis=0, tiled=True)]
    ppermute x3 -> x19, waiting for transfers between devices: 28.4 us -> 118 us  [swap(): return lax.ppermute(x, 'sp', [(i, i ^ mask) for i in range(group)])]
    all_to_all x2 -> x1, blocking collectives: 91.4 us -> 45.8 us  [exchange(): lax.all_to_all(x, 'sp', split_axis=0, concat_axis=0, axis_index_groups=pe...]
    pallas_call x0 -> x4, Pallas kernels: none -> 26.8 us  [the longest x2 21.8 us: mixer(): pl.pallas_call(functools.partial(mixer_kernel, masks=masks, far=far, rows...]
    dot_general x2 -> x0, matrix products: 24.9 us -> none  [the longest x1 15.7 us: on_device(): lax.dot_general(hidden, down_full, (((1,), (1,)), ((), ())), preferred_el...]
    ppermute x3 -> x19, starting transfers between devices: 0.95 us -> 17.7 us  [swap(): return lax.ppermute(x, 'sp', [(i, i ^ mask) for i in range(group)])]
    ppermute x0 -> x7, local copies, waits for them, and re-layouts: none -> 15.8 us  [swap(): return lax.ppermute(x, 'sp', [(i, i ^ mask) for i in range(group)])]
    all_to_all x0 -> x1, waiting for transfers between devices: none -> 9.27 us  [exchange(): lax.all_to_all(x, 'sp', split_axis=0, concat_axis=0, axis_index_groups=pe...]
  transfers between devices with their start and end apart: 6 -> 20, of which waited for: 3 -> 11; matrix products, arithmetic and copies ran while one was open for 7% -> 9% of each run, Pallas kernels for 18% -> 24%
where the time goes in v2:
time: 319 us
  waiting for transfers between devices  128 us (40%)
  Pallas kernels  91.1 us (29%)
  blocking collectives  45.8 us (14%)
  local copies, waits for them, and re-layouts  23.6 us (7%)
  starting transfers between devices  21.1 us (7%)
  other arithmetic  5.26 us (2%)
  matrix products  3.84 us (1%)
    ppermute x19, waiting for transfers between devices, swap(): return lax.ppermute(x, 'sp', [(i, i ^ mask) for i in range(group)])  118 us
    pallas_call x4, Pallas kernels, attend(): pl.pallas_call(functools.partial(attend_kernel, kb=kb, hd=hd, first=state...  61.3 us
    all_to_all x1, blocking collectives, exchange(): lax.all_to_all(x, 'sp', split_axis=0, concat_axis=0, axis_index_groups=pe...  45.8 us
    pallas_call x2, Pallas kernels, mixer(): pl.pallas_call(functools.partial(mixer_kernel, masks=masks, far=far, rows...  21.8 us
    ppermute x19, starting transfers between devices, swap(): return lax.ppermute(x, 'sp', [(i, i ^ mask) for i in range(group)])  17.7 us
    ppermute x7, local copies, waits for them, and re-layouts, swap(): return lax.ppermute(x, 'sp', [(i, i ^ mask) for i in range(group)])  15.8 us
    all_to_all x1, waiting for transfers between devices, exchange(): lax.all_to_all(x, 'sp', split_axis=0, concat_axis=0, axis_index_groups=pe...  9.27 us
  transfers between devices with their start and end apart: 20, of which 11 were waited for; matrix products, arithmetic and copies ran while one was open for 9% of the time, Pallas kernels for 24%

profile of v2, /device:TPU:0, one launch (start us, length us, event | category | flops | bytes accessed | tf_op | source)
XLA Modules:
  0.0 318.6 jit_solution(16359173195168013894)
XLA Ops:
  0.0 2.9 shard_map.127
  2.9 45.8 %all_to_all.10.refs_0_.refs_1_.refs_2_ = bf16[8,3,256,128]{3,2,1,0:T(8,128)(2,1)S(1)} all-to-all(bf16[8,3,256,128]{3,2,1,0:T(8,128)(2,1)} %shard_map.127), channel_id=1, replica_groups={{0,2,4,6,16,18,20,22},{1,3,5,7,17,19,21,23},{8,10,12,14,24,26,28,30},{9..., dimensions={0} | all-to-all | bytes 3145728 | tf_op jit(solution)/shard_map/all_to_all | solution.py:286
  50.2 2.8 shard_map.132
  55.3 19.7 %collective-permute-done.refs_1_.refs_2_ = bf16[8,2,256,128]{3,2,1,0:T(8,128)(2,1)} collective-permute-done((bf16[8,2,256,128]{3,2,1,0:T(8,128)(2,1)S(1)}, bf16[8,2,256,128]{3,2,1,0:T(8,128)(2,1)}, u32[]{:S(2)}, u32[]{:S(2)}) %collective-permute-start) | collective-permute-done | bytes 1048608 | tf_op jit(solution)/shard_map/ppermute | solution.py:270
  76.4 4.8 %collective-permute-done.5.refs_2_ = bf16[3,64,704]{2,1,0:T(8,128)(2,1)S(1)} collective-permute-done((bf16[3,64,704]{2,1,0:T(8,128)(2,1)}, bf16[3,64,704]{2,1,0:T(8,128)(2,1)S(1)}, u32[]{:S(2)}, u32[]{:S(2)}) %collective-permute-start.5) | collective-permute-done | bytes 270368 | tf_op jit(solution)/shard_map/ppermute | solution.py:270
  83.6 2.3 shard_map.133.refs_0_
  86.0 2.4 copy.28
  88.4 3.0 collective-permute-start.10
  91.3 13.8 %shard_map.128 = (f32[1,4096]{1,0:T(1,128)}, f32[1,4096]{1,0:T(1,128)}, f32[128,4096]{1,0:T(8,128)}) custom-call(bf16[8,3,256,128]{3,2,1,0:T(8,128)(2,1)} %copy-done, bf16[8,3,256,128]{3,2,1,0:T(8,128)(2,1)} %copy-done, bf16[8,3,256,128]{3,2,1,0:T(8,128)(2,1)} %copy-done), custom_call_target="tpu_custom_call" | custom-call | flops 3221225472 | bytes 4194304 | tf_op jit(solution)/shard_map/pallas_call | solution.py:240
  105.2 15.4 %shard_map.129 = (f32[1,4096]{1,0:T(1,128)}, f32[1,4096]{1,0:T(1,128)}, f32[128,4096]{1,0:T(8,128)}) custom-call(bf16[8,3,256,128]{3,2,1,0:T(8,128)(2,1)} %copy-done, bf16[8,2,256,128]{3,2,1,0:T(8,128)(2,1)} %collective-permute-done.2.refs_1_.refs_2_, ...), custom_call_target="tpu_custom_call", output_to_operand_aliasing={{0}: (3, {}), {1}: (4, {}), {2}: (5, {})} | custom-call | flops 3221225472 | bytes 4194304 | tf_op jit(solution)/shard_map/pallas_call | solution.py:240
  120.6 15.4 %shard_map.130 = (f32[1,4096]{1,0:T(1,128)}, f32[1,4096]{1,0:T(1,128)}, f32[128,4096]{1,0:T(8,128)}) custom-call(bf16[8,3,256,128]{3,2,1,0:T(8,128)(2,1)} %copy-done, bf16[8,2,256,128]{3,2,1,0:T(8,128)(2,1)} %collective-permute-done.refs_1_.refs_2_, ...), custom_call_target="tpu_custom_call", output_to_operand_aliasing={{0}: (3, {}), {1}: (4, {}), {2}: (5, {})} | custom-call | flops 3221225472 | bytes 4194304 | tf_op jit(solution)/shard_map/pallas_call | solution.py:240
  136.0 16.7 %shard_map.131 = bf16[2048,128]{1,0:T(8,128)(2,1)} custom-call(bf16[8,3,256,128]{3,2,1,0:T(8,128)(2,1)} %copy-done, bf16[8,2,256,128]{3,2,1,0:T(8,128)(2,1)} %collective-permute-done.1.refs_1_.refs_2_, bf16[8,2,256,128]{3,2,1,0:T(8,128)(2,1)} %collective-permute-done.1.refs_1_.refs_2_, f32[1,4096]{1,0:T(1,128)} %get-tuple-element.30.refs_3_, ...), custom_call_target="tpu_custom_call" | custom-call | flops 3221225472 | bytes 4194304 | tf_op jit(solution)/shard_map/pallas_call | solution.py:240
  152.7 2.0 copy.26
  154.7 3.5 %all-to-all-start.1 = ((bf16[8,256,128]{1,2,0:T(8,128)(2,1)}), bf16[8,256,128]{1,2,0:T(8,128)(2,1)S(1)}, u32[]{:S(2)}, u32[]{:S(2)}) async-start(bf16[8,256,128]{1,2,0:T(8,128)(2,1)} %copy.26), calls=%async_computation.1 | async-start | bytes 1048576 | tf_op jit(solution)/shard_map/all_to_all | solution.py:286
  165.1 9.3 %all-to-all-done.1 = bf16[8,256,128]{1,2,0:T(8,128)(2,1)S(1)} async-done(((bf16[8,256,128]{1,2,0:T(8,128)(2,1)}), bf16[8,256,128]{1,2,0:T(8,128)(2,1)S(1)}, u32[]{:S(2)}, u32[]{:S(2)}) %all-to-all-start.1) | async-done | bytes 524320 | tf_op jit(solution)/shard_map/all_to_all | solution.py:286
  174.4 3.8 %fusion = (f32[256]{0:T(256)S(1)}, f32[256,2048]{1,0:T(8,128)S(1)}) fusion(bf16[256,1024]{0,1:T(8,128)(2,1)S(1)} %bitcast.10, bf16[1024,2048]{1,0:T(8,128)(2,1)} %param.21, bf16[256,2048]{1,0:T(8,128)(2,1)} %param.13), kind=kOutput, calls=%fused_computation.7 | convolution fusion | flops 1075838720 | bytes 7865344 | tf_op jit(solution)/shard_map/dot_general | solution.py:260
  178.6 12.2 %collective-permute-done.7 = bf16[3,256,704]{1,2,0:T(8,128)(2,1)} collective-permute-done((bf16[3,256,704]{1,2,0:T(8,128)(2,1)}, bf16[3,256,704]{1,2,0:T(8,128)(2,1)}, u32[]{:S(2)}, u32[]{:S(2)}) %collective-permute-start.7) | collective-permute-done | bytes 1081376 | tf_op jit(solution)/shard_map/ppermute | solution.py:270
  193.6 21.3 %collective-permute-done.9 = bf16[3,256,704]{1,2,0:T(8,128)(2,1)} collective-permute-done((bf16[3,256,704]{1,2,0:T(8,128)(2,1)}, bf16[3,256,704]{1,2,0:T(8,128)(2,1)}, u32[]{:S(2)}, u32[]{:S(2)}) %collective-permute-start.9) | collective-permute-done | bytes 1081376 | tf_op jit(solution)/shard_map/ppermute | solution.py:270
  216.2 2.4 copy.35.refs_4_
  218.6 2.4 copy.32.refs_1_
  221.0 2.4 copy.33.refs_2_
  223.4 2.4 copy.34.refs_3_
  225.8 11.4 %collective-permute-done.11 = bf16[3,256,704]{1,2,0:T(8,128)(2,1)} collective-permute-done((bf16[3,256,704]{1,2,0:T(8,128)(2,1)}, bf16[3,256,704]{1,2,0:T(8,128)(2,1)}, u32[]{:S(2)}, u32[]{:S(2)}) %collective-permute-start.11) | collective-permute-done | bytes 1081376 | tf_op jit(solution)/shard_map/ppermute | solution.py:270
  237.2 2.4 copy.36.refs_5_
  239.6 2.4 copy.37.refs_6_
  242.0 18.4 %collective-permute-done.13 = bf16[3,256,704]{1,2,0:T(8,128)(2,1)S(1)} collective-permute-done((bf16[3,256,704]{1,2,0:T(8,128)(2,1)}, bf16[3,256,704]{1,2,0:T(8,128)(2,1)S(1)}, u32[]{:S(2)}, u32[]{:S(2)}) %collective-permute-start.13) | collective-permute-done | bytes 1081376 | tf_op jit(solution)/shard_map/ppermute | solution.py:270
  261.9 10.8 %shard_map.134 = (bf16[256,2048]{1,0:T(8,128)(2,1)}, bf16[256,2048]{1,0:T(8,128)(2,1)}) custom-call(s32[1]{0:T(128)} %bitcast.5.base, bf16[3,256,704]{2,1,0:T(8,128)(2,1)} %shard_map.133.refs_0_, bf16[3,256,704]{2,1,0:T(8,128)(2,1)} %copy.32.refs_1_, bf16[3,256,704]{2,1,0:T(8,128)(2,1)} %copy.33.refs_2_, bf16[3,256,704]{2,1,0:T(8,128)(2,1)} %copy.34.refs_3_, ...), custom_call_target="tpu_custom_call" | custom-call | flops 4429185024 | bytes 8650752 | tf_op jit(solution)/shard_map/pallas_call | solution.py:115
  272.8 3.0 collective-permute-done.16.refs_8_
  275.8 10.9 %shard_map.135 = (bf16[256,2048]{1,0:T(8,128)(2,1)}, bf16[256,2048]{1,0:T(8,128)(2,1)}) custom-call(s32[1]{0:T(128)} %bitcast.5.base, bf16[3,256,704]{2,1,0:T(8,128)(2,1)} %shard_map.133.refs_0_, bf16[3,256,704]{2,1,0:T(8,128)(2,1)} %copy.32.refs_1_, bf16[3,256,704]{2,1,0:T(8,128)(2,1)} %copy.33.refs_2_, bf16[3,256,704]{2,1,0:T(8,128)(2,1)} %copy.34.refs_3_, ...), custom_call_target="tpu_custom_call" | custom-call | flops 4429185024 | bytes 8650752 | tf_op jit(solution)/shard_map/pallas_call | solution.py:115
  287.3 2.4 collective-permute-done.17
  293.1 23.5 %collective-permute-done.18 = bf16[256,2048]{1,0:T(8,128)(2,1)S(1)} collective-permute-done((bf16[256,2048]{1,0:T(8,128)(2,1)S(1)}, bf16[256,2048]{1,0:T(8,128)(2,1)S(1)}, u32[]{:S(2)}, u32[]{:S(2)}) %collective-permute-start.18) | collective-permute-done | bytes 1048608 | tf_op jit(solution)/shard_map/ppermute | solution.py:270
  316.6 2.0 add_convert_fusion
  (58 shorter events, 24.5 us)
Async XLA Ops:
  2.9 46.1 %copy-start.2 = (bf16[2816,64]{0,1:T(8,128)(2,1)S(1)}, bf16[2816,64]{0,1:T(8,128)(2,1)}, u32[]{:S(2)}) copy-start(bf16[2816,64]{0,1:T(8,128)(2,1)} %param.25) | copy-start | bytes 1081348
  48.7 4.2 %copy-start = (bf16[8,3,256,128]{3,2,1,0:T(8,128)(2,1)}, bf16[8,3,256,128]{3,2,1,0:T(8,128)(2,1)S(1)}, u32[]{:S(2)}) copy-start(bf16[8,3,256,128]{3,2,1,0:T(8,128)(2,1)S(1)} %all_to_all.10.refs_0_.refs_1_.refs_2_) | copy-start | bytes 4718596
  48.7 26.3 %copy-start.7 = (f32[128]{0:T(128)S(1)}, f32[128]{0:T(128)}, u32[]{:S(2)}) copy-start(f32[128]{0:T(128)} %param.20) | copy-start | bytes 1540
  48.7 27.0 %copy-start.9 = (f32[8]{0:T(128)S(1)}, f32[8]{0:T(128)}, u32[]{:S(2)}) copy-start(f32[8]{0:T(128)} %param.19) | copy-start | bytes 100
  48.8 26.2 %collective-permute-start = (bf16[8,2,256,128]{3,2,1,0:T(8,128)(2,1)S(1)}, bf16[8,2,256,128]{3,2,1,0:T(8,128)(2,1)}, u32[]{:S(2)}, u32[]{:S(2)}) collective-permute-start(bf16[8,2,256,128]{3,2,1,0:T(8,128)(2,1)S(1)} %slice.4), channel_id=1, source_target_pairs={{0,8},{1,9},{2,10},{3,11},{4,12},{5,13},{6,14},{7,15},{8,0},{9,1},... | collective-permute-start | bytes 3145736 | tf_op jit(solution)/shard_map/ppermute | solution.py:270
  48.9 56.3 %collective-permute-start.2 = (bf16[8,2,256,128]{3,2,1,0:T(8,128)(2,1)S(1)}, bf16[8,2,256,128]{3,2,1,0:T(8,128)(2,1)}, u32[]{:S(2)}, u32[]{:S(2)}) collective-permute-start(bf16[8,2,256,128]{3,2,1,0:T(8,128)(2,1)S(1)} %slice.4), channel_id=1, source_target_pairs={{0,1},{1,0},{2,3},{3,2},{4,5},{5,4},{6,7},{7,6},{8,9},{9,8},{10,11... | collective-permute-start | bytes 3145736 | tf_op jit(solution)/shard_map/ppermute | solution.py:270
  52.9 23.5 %collective-permute-start.4 = (bf16[3,64,704]{2,1,0:T(8,128)(2,1)}, bf16[3,64,704]{2,1,0:T(8,128)(2,1)S(1)}, u32[]{:S(2)}, u32[]{:S(2)}) collective-permute-start(bf16[3,64,704]{2,1,0:T(8,128)(2,1)} %get-tuple-element.34), channel_id=1, source_target_pairs={{0,1},{1,0},{2,3},{3,2},{4,5},{5,4},{6,7},{7,6},{8,9},{9,8},{10,11... | collective-permute-start | bytes 811016 | tf_op jit(solution)/shard_map/ppermute | solution.py:270
  53.4 27.9 %collective-permute-start.5 = (bf16[3,64,704]{2,1,0:T(8,128)(2,1)}, bf16[3,64,704]{2,1,0:T(8,128)(2,1)S(1)}, u32[]{:S(2)}, u32[]{:S(2)}) collective-permute-start(bf16[3,64,704]{2,1,0:T(8,128)(2,1)} %get-tuple-element.35), channel_id=1, source_target_pairs={{0,8},{1,9},{2,10},{3,11},{4,12},{5,13},{6,14},{7,15},{8,0},{9,1},... | collective-permute-start | bytes 811016 | tf_op jit(solution)/shard_map/ppermute | solution.py:270
  55.3 27.6 %collective-permute-start.6 = (bf16[3,64,704]{2,1,0:T(8,128)(2,1)}, bf16[3,64,704]{2,1,0:T(8,128)(2,1)S(1)}, u32[]{:S(2)}, u32[]{:S(2)}) collective-permute-start(bf16[3,64,704]{2,1,0:T(8,128)(2,1)} %get-tuple-element.36), channel_id=1, source_target_pairs={{0,9},{1,8},{2,11},{3,10},{4,13},{5,12},{6,15},{7,14},{8,1},{9,0},... | collective-permute-start | bytes 811016 | tf_op jit(solution)/shard_map/ppermute | solution.py:270
  75.0 61.0 %collective-permute-start.1 = (bf16[8,2,256,128]{3,2,1,0:T(8,128)(2,1)}, bf16[8,2,256,128]{3,2,1,0:T(8,128)(2,1)}, u32[]{:S(2)}, u32[]{:S(2)}) collective-permute-start(bf16[8,2,256,128]{3,2,1,0:T(8,128)(2,1)} %collective-permute-done.refs_1_.refs_2_), channel_id=1, source_target_pairs={{0,1},{1,0},{2,3},{3,2},{4,5},{5,4},{6,7},{7,6},{8,9},{9,8},{10,11... | collective-permute-start | bytes 3145736 | tf_op jit(solution)/shard_map/ppermute | solution.py:270
  76.4 6.5 %copy-start.3 = (bf16[3,64,704]{2,1,0:T(8,128)(2,1)}, bf16[3,64,704]{2,1,0:T(8,128)(2,1)S(1)}, u32[]{:S(2)}) copy-start(bf16[3,64,704]{2,1,0:T(8,128)(2,1)S(1)} %collective-permute-done.4.refs_1_) | copy-start | bytes 811012
  81.2 1.7 copy-start.4
  82.9 0.7 copy-start.5
  88.4 73.4 %collective-permute-start.10 = (bf16[3,256,704]{1,2,0:T(8,128)(2,1)}, bf16[3,256,704]{1,2,0:T(8,128)(2,1)}, u32[]{:S(2)}, u32[]{:S(2)}) collective-permute-start(bf16[3,256,704]{1,2,0:T(8,128)(2,1)} %copy.28), channel_id=1, source_target_pairs={{0,16},{1,17},{2,18},{3,19},{4,20},{5,21},{6,22},{7,23},{8,24},{9,... | collective-permute-start | bytes 3244040 | tf_op jit(solution)/shard_map/ppermute | solution.py:270
  154.7 19.7 %all-to-all-start.1 = ((bf16[8,256,128]{1,2,0:T(8,128)(2,1)}), bf16[8,256,128]{1,2,0:T(8,128)(2,1)S(1)}, u32[]{:S(2)}, u32[]{:S(2)}) async-start(bf16[8,256,128]{1,2,0:T(8,128)(2,1)} %copy.26), calls=%async_computation.1 | async-start | bytes 1048576 | tf_op jit(solution)/shard_map/all_to_all | solution.py:286
  158.2 32.6 %collective-permute-start.7 = (bf16[3,256,704]{1,2,0:T(8,128)(2,1)}, bf16[3,256,704]{1,2,0:T(8,128)(2,1)}, u32[]{:S(2)}, u32[]{:S(2)}) collective-permute-start(bf16[3,256,704]{1,2,0:T(8,128)(2,1)} %copy.28), channel_id=1, source_target_pairs={{0,2},{1,3},{2,0},{3,1},{4,6},{5,7},{6,4},{7,5},{8,10},{9,11},{10,... | collective-permute-start | bytes 3244040 | tf_op jit(solution)/shard_map/ppermute | solution.py:270
  160.2 33.4 %collective-permute-start.8 = (bf16[3,256,704]{1,2,0:T(8,128)(2,1)}, bf16[3,256,704]{1,2,0:T(8,128)(2,1)}, u32[]{:S(2)}, u32[]{:S(2)}) collective-permute-start(bf16[3,256,704]{1,2,0:T(8,128)(2,1)} %copy.28), channel_id=1, source_target_pairs={{0,4},{1,5},{2,6},{3,7},{4,0},{5,1},{6,2},{7,3},{8,12},{9,13},{10,... | collective-permute-start | bytes 3244040 | tf_op jit(solution)/shard_map/ppermute | solution.py:270
  161.6 53.3 %collective-permute-start.9 = (bf16[3,256,704]{1,2,0:T(8,128)(2,1)}, bf16[3,256,704]{1,2,0:T(8,128)(2,1)}, u32[]{:S(2)}, u32[]{:S(2)}) collective-permute-start(bf16[3,256,704]{1,2,0:T(8,128)(2,1)} %copy.28), channel_id=1, source_target_pairs={{0,6},{1,7},{2,4},{3,5},{4,2},{5,3},{6,0},{7,1},{8,14},{9,15},{10,... | collective-permute-start | bytes 3244040 | tf_op jit(solution)/shard_map/ppermute | solution.py:270
  161.8 75.4 %collective-permute-start.11 = (bf16[3,256,704]{1,2,0:T(8,128)(2,1)}, bf16[3,256,704]{1,2,0:T(8,128)(2,1)}, u32[]{:S(2)}, u32[]{:S(2)}) collective-permute-start(bf16[3,256,704]{1,2,0:T(8,128)(2,1)} %collective-permute-done.10), channel_id=1, source_target_pairs={{0,2},{1,3},{2,0},{3,1},{4,6},{5,7},{6,4},{7,5},{8,10},{9,11},{10,... | collective-permute-start | bytes 3244040 | tf_op jit(solution)/shard_map/ppermute | solution.py:270
  163.6 75.9 %collective-permute-start.12 = (bf16[3,256,704]{1,2,0:T(8,128)(2,1)}, bf16[3,256,704]{1,2,0:T(8,128)(2,1)}, u32[]{:S(2)}, u32[]{:S(2)}) collective-permute-start(bf16[3,256,704]{1,2,0:T(8,128)(2,1)} %collective-permute-done.10), channel_id=1, source_target_pairs={{0,4},{1,5},{2,6},{3,7},{4,0},{5,1},{6,2},{7,3},{8,12},{9,13},{10,... | collective-permute-start | bytes 3244040 | tf_op jit(solution)/shard_map/ppermute | solution.py:270
  178.2 14.0 %copy-start.6 = (f32[2048]{0:T(1024)S(1)}, f32[2048]{0:T(1024)}, u32[]{:S(2)}) copy-start(f32[2048]{0:T(1024)} %param.22) | copy-start | bytes 24580
  190.8 69.6 %collective-permute-start.13 = (bf16[3,256,704]{1,2,0:T(8,128)(2,1)}, bf16[3,256,704]{1,2,0:T(8,128)(2,1)S(1)}, u32[]{:S(2)}, u32[]{:S(2)}) collective-permute-start(bf16[3,256,704]{1,2,0:T(8,128)(2,1)} %collective-permute-done.10), channel_id=1, source_target_pairs={{0,6},{1,7},{2,4},{3,5},{4,2},{5,3},{6,0},{7,1},{8,14},{9,15},{10,... | collective-permute-start | bytes 3244040 | tf_op jit(solution)/shard_map/ppermute | solution.py:270
  193.6 68.3 %collective-permute-start.14 = (bf16[256,2048]{1,0:T(8,128)(2,1)}, bf16[256,2048]{1,0:T(8,128)(2,1)}, u32[]{:S(2)}, u32[]{:S(2)}) collective-permute-start(bf16[256,2048]{1,0:T(8,128)(2,1)} %multiply_convert_fusion.refs_9_), channel_id=1, source_target_pairs={{0,1},{1,0},{2,3},{3,2},{4,5},{5,4},{6,7},{7,6},{8,9},{9,8},{10,11... | collective-permute-start | bytes 3145736 | tf_op jit(solution)/shard_map/ppermute | solution.py:270
  214.9 57.8 %collective-permute-start.3 = (bf16[256,2048]{1,0:T(8,128)(2,1)}, bf16[256,2048]{1,0:T(8,128)(2,1)}, u32[]{:S(2)}, u32[]{:S(2)}) collective-permute-start(bf16[256,2048]{1,0:T(8,128)(2,1)} %multiply_convert_fusion.refs_9_), channel_id=1, source_target_pairs={{0,8},{1,9},{2,10},{3,11},{4,12},{5,13},{6,14},{7,15},{8,0},{9,1},... | collective-permute-start | bytes 3145736 | tf_op jit(solution)/shard_map/ppermute | solution.py:270
  272.7 14.2 %copy-start.8 = (bf16[256,2048]{1,0:T(8,128)(2,1)S(1)}, bf16[256,2048]{1,0:T(8,128)(2,1)}, u32[]{:S(2)}) copy-start(bf16[256,2048]{1,0:T(8,128)(2,1)} %get-tuple-element.39) | copy-start | bytes 3145732
  272.8 3.1 collective-permute-start.16
  286.8 29.8 %copy-start.1 = (bf16[256,2048]{1,0:T(8,128)(2,1)S(1)}, bf16[256,2048]{1,0:T(8,128)(2,1)}, u32[]{:S(2)}) copy-start(bf16[256,2048]{1,0:T(8,128)(2,1)} %get-tuple-element.38) | copy-start | bytes 3145732
  286.8 2.9 collective-permute-start.17
  287.0 6.2 %collective-permute-start.15 = (bf16[256,2048]{1,0:T(8,128)(2,1)S(1)}, bf16[256,2048]{1,0:T(8,128)(2,1)S(1)}, u32[]{:S(2)}, u32[]{:S(2)}) collective-permute-start(bf16[256,2048]{1,0:T(8,128)(2,1)S(1)} %copy-done.8), channel_id=1, source_target_pairs={{0,1},{1,0},{2,3},{3,2},{4,5},{5,4},{6,7},{7,6},{8,9},{9,8},{10,11... | collective-permute-start | bytes 3145736 | tf_op jit(solution)/shard_map/ppermute | solution.py:270
  291.3 25.3 %collective-permute-start.18 = (bf16[256,2048]{1,0:T(8,128)(2,1)S(1)}, bf16[256,2048]{1,0:T(8,128)(2,1)S(1)}, u32[]{:S(2)}, u32[]{:S(2)}) collective-permute-start(bf16[256,2048]{1,0:T(8,128)(2,1)S(1)} %add_convert_fusion.1), channel_id=1, source_target_pairs={{0,8},{1,9},{2,10},{3,11},{4,12},{5,13},{6,14},{7,15},{8,0},{9,1},... | collective-permute-start | bytes 3145736 | tf_op jit(solution)/shard_map/ppermute | solution.py:270

commit v3 on v2

--- a/solution.py
+++ b/solution.py
@@ -40,7 +40,7 @@
         slot = jnp.bitwise_xor(place[0], p)
         buf[slot, 0] = gate[:, cols]
         buf[slot, 1] = up[:, cols]
-        buf[slot, 2] = down[cols, :].T
+        buf[slot, 2] = down[:, cols]
     for p, out in enumerate(outs):
         out[...] = buf[p]
 
@@ -58,69 +58,82 @@
 
 
 def assemble_kernel(place, *refs):
-    parts, out = refs[:-1], refs[-1]
+    parts, out, buf = refs[:-2], refs[-2], refs[-1]
     rows = parts[0].shape[1]
     for p, part in enumerate(parts):
         at = pl.multiple_of(jnp.bitwise_xor(place[0], p) * rows, rows)
-        out[:, pl.ds(at, rows), :] = part[...]
+        buf[:, pl.ds(at, rows), :] = part[...]
+    for kind in range(out.shape[0]):
+        out[kind] = buf[kind].T
 
 
 def assemble(place, parts):
     kinds, rows, width = parts[0].shape
+    block = len(parts) * rows
     return pl.pallas_call(
         assemble_kernel,
         in_specs=[pl.BlockSpec(memory_space=pltpu.SMEM)] + [pl.BlockSpec()] * len(parts),
-        out_shape=jax.ShapeDtypeStruct((kinds, len(parts) * rows, width), jnp.bfloat16),
+        out_shape=jax.ShapeDtypeStruct((kinds, width, block), jnp.bfloat16),
+        scratch_shapes=[pltpu.VMEM((kinds, block, width), jnp.bfloat16)],
         compiler_params=pltpu.CompilerParams(vmem_limit_bytes=VMEM_LIMIT),
     )(place, *parts)
 
 
-def mixer_kernel(base, *refs, masks, far, rows):
-    weights = refs[: len(masks)]
-    xa, xb, out_a, out_b, buf, sems = refs[len(masks) :]
-    kinds = (slice(0, 2), slice(2, 3))
+def mixer_kernel(base, *refs, blocks, strips):
+    weights = refs[:blocks]
+    xa, xb, out_a, out_b, buf, sems = refs[blocks:]
+    block = weights[0].shape[2]
 
     def copies(part):
-        for m, mask in enumerate(masks):
-            for n, f in enumerate((0, far)):
-                at = (jnp.bitwise_xor(base[0], mask) + f) * rows
-                at = pl.multiple_of(at, 2 * rows)
-                yield pltpu.make_async_copy(
-                    weights[m].at[kinds[part], pl.ds(n * 2 * rows, 2 * rows)],
-                    buf.at[kinds[part], pl.ds(at, 2 * rows)],
-                    sems.at[part, 2 * m + n],
-                )
-
-    for part in (0, 1):
+        for m in range(blocks):
+            at = pl.multiple_of(jnp.bitwise_xor(base[0], m) * block, block)
+            yield pltpu.make_async_copy(
+                weights[m].at[part],
+                buf.at[part, :, pl.ds(at, block)],
+                sems.at[part, m],
+            )
+
+    for part in range(3):
         for copy in copies(part):
             copy.start()
+    rows = [jnp.concatenate([x[:, lo:hi] for lo, hi in strips], axis=1) for x in (xa, xb)]
+
+    def project(x, kind):
+        return lax.dot_general(
+            x, buf[kind], (((1,), (1,)), ((), ())), preferred_element_type=jnp.float32
+        )
+
     for copy in copies(0):
         copy.wait()
-    hidden = []
-    for x in (xa, xb):
-        gate = jnp.dot(x[...], buf[0], preferred_element_type=jnp.float32)
-        up = jnp.dot(x[...], buf[1], preferred_element_type=jnp.float32)
-        hidden.append((gate / (1.0 + jnp.exp(-gate)) * up).astype(jnp.bfloat16))
+    gates = [project(x, 0) for x in rows]
     for copy in copies(1):
         copy.wait()
+    hidden = [
+        (gate / (1.0 + jnp.exp(-gate)) * project(x, 1)).astype(jnp.bfloat16)
+        for gate, x in zip(gates, rows)
+    ]
+    for copy in copies(2):
+        copy.wait()
     for h, out in zip(hidden, (out_a, out_b)):
-        out[...] = lax.dot_general(
-            h, buf[2], (((1,), (1,)), ((), ())), preferred_element_type=jnp.float32
-        ).astype(jnp.bfloat16)
-
-
-def mixer(base, xa, xb, weights, masks, far):
-    kinds, block, width = weights[0].shape
+        result = jnp.dot(h, buf[2], preferred_element_type=jnp.float32).astype(jnp.bfloat16)
+        at = 0
+        for lo, hi in strips:
+            out[:, lo:hi] = result[:, at : at + hi - lo]
+            at += hi - lo
+
+
+def mixer(base, xa, xb, weights, strips):
+    kinds, width, _ = weights[0].shape
     n, d = xa.shape
     return pl.pallas_call(
-        functools.partial(mixer_kernel, masks=masks, far=far, rows=block // 4),
+        functools.partial(mixer_kernel, blocks=len(weights), strips=strips),
         in_specs=[pl.BlockSpec(memory_space=pltpu.SMEM)]
-        + [pl.BlockSpec(memory_space=pl.ANY)] * len(masks)
+        + [pl.BlockSpec(memory_space=pl.ANY)] * len(weights)
         + [pl.BlockSpec()] * 2,
         out_shape=[jax.ShapeDtypeStruct((n, d), jnp.bfloat16)] * 2,
         scratch_shapes=[
-            pltpu.VMEM((kinds, d, width), jnp.bfloat16),
-            pltpu.SemaphoreType.DMA((2, 2 * len(masks))),
+            pltpu.VMEM((kinds, width, d), jnp.bfloat16),
+            pltpu.SemaphoreType.DMA((3, len(weights))),
         ],
         compiler_params=pltpu.CompilerParams(vmem_limit_bytes=VMEM_LIMIT),
         cost_estimate=pl.CostEstimate(
@@ -329,9 +342,9 @@
     share_bits = ordered[: len(ordered) - n_head_bits]
     head_bits = sorted(ordered[len(ordered) - n_head_bits :])
     place = rank(device, group_bits).reshape(1)
-    base = (device - device % 2 - (device // far % 2) * far).reshape(1)
-
-    pieces = pack_weights(place, gate_weight, up_weight, down_weight, 4)
+    base = rank(device, others).reshape(1)
+
+    pieces = pack_weights(place, gate_weight, up_weight, down_weight.T, 4)
     parts = [pieces[0]]
     for n, mask in ((1, 1), (2, far), (3, far + 1)):
         parts.append(swap(pieces[n], mask))
@@ -349,17 +362,17 @@
     own_normed = layer_normed(by_rows, stream, out_weight, norm_gain)
     own = lax.all_gather(own_normed, "tp", axis=0, tiled=True)
 
-    masks = subsets(others)
-    gathered = [weights[mask] for mask in masks]
+    gathered = [weights[mask] for mask in subsets(others)]
+    rows = gate_weight.shape[0]
+    strips = [((b + f) * rows, (b + f + 2) * rows) for b in subsets(others) for f in (0, far)]
     near, away = swap(own, 1), swap(own, far)
-    near_out, own_out = mixer(base, near, own, gathered, masks, far)
-    given = swap(near_out, 1)
-    away, own_out = lax.optimization_barrier((away, own_out))
     both = swap(away, 1)
-    both_out, away_out = mixer(base, both, away, gathered, masks, far)
+    both_out, away_out = mixer(base, both, away, gathered, strips)
     handed = swap(both_out, 1)
     summed = away_out.astype(jnp.float32) + handed.astype(jnp.float32)
     sent = swap(summed.astype(jnp.bfloat16), far)
+    near_out, own_out = mixer(base, near, own, gathered, strips)
+    given = swap(near_out, 1)
     partial_terms = (
         own_out.astype(jnp.float32) + given.astype(jnp.float32) + sent.astype(jnp.float32)
     )

time: 319 us -> 318 us (level)
  local copies, waits for them, and re-layouts: 23.6 us -> 6.59 us
  waiting for transfers between devices: 128 us -> 145 us
    ppermute x19, waiting for transfers between devices: 118 us -> 145 us  [swap(): return lax.ppermute(x, 'sp', [(i, i ^ mask) for i in range(group)])]
    ppermute x7 -> x0, local copies, waits for them, and re-layouts: 15.8 us -> none  [swap(): return lax.ppermute(x, 'sp', [(i, i ^ mask) for i in range(group)])]
    all_to_all x1, waiting for transfers between devices: 9.27 us -> 0.01 us  [exchange(): lax.all_to_all(x, 'sp', split_axis=0, concat_axis=0, axis_index_groups=pe...]
  transfers between devices with their start and end apart: 20 -> 20, of which waited for: 11 -> 8; matrix products, arithmetic and copies ran while one was open for 9% -> 3% of each run, Pallas kernels for 24% -> 22%
where the time goes in v3:
time: 318 us
  waiting for transfers between devices  145 us (46%)
  Pallas kernels  89.5 us (28%)
  blocking collectives  45.8 us (14%)
  starting transfers between devices  22.1 us (7%)
  local copies, waits for them, and re-layouts  6.59 us (2%)
  other arithmetic  5.26 us (2%)
  matrix products  3.84 us (1%)
    ppermute x19, waiting for transfers between devices, swap(): return lax.ppermute(x, 'sp', [(i, i ^ mask) for i in range(group)])  145 us
    pallas_call x4, Pallas kernels, attend(): pl.pallas_call(functools.partial(attend_kernel, kb=kb, hd=hd, first=state...  61.4 us
    all_to_all x1, blocking collectives, exchange(): lax.all_to_all(x, 'sp', split_axis=0, concat_axis=0, axis_index_groups=pe...  45.8 us
    pallas_call x2, Pallas kernels, mixer(): pl.pallas_call(functools.partial(mixer_kernel, blocks=len(weights), strip...  20 us
    ppermute x19, starting transfers between devices, swap(): return lax.ppermute(x, 'sp', [(i, i ^ mask) for i in range(group)])  18.6 us
  transfers between devices with their start and end apart: 20, of which 8 were waited for; matrix products, arithmetic and copies ran while one was open for 3% of the time, Pallas kernels for 22%

profile of v3, /device:TPU:0, one launch (start us, length us, event | category | flops | bytes accessed | tf_op | source)
XLA Modules:
  0.0 317.9 jit_solution(6011640619708543517)
XLA Ops:
  0.0 2.9 shard_map.127
  2.9 45.8 %all_to_all.10.refs_0_.refs_1_.refs_2_ = bf16[8,3,256,128]{3,2,1,0:T(8,128)(2,1)S(1)} all-to-all(bf16[8,3,256,128]{3,2,1,0:T(8,128)(2,1)} %shard_map.127), channel_id=1, replica_groups={{0,2,4,6,16,18,20,22},{1,3,5,7,17,19,21,23},{8,10,12,14,24,26,28,30},{9..., dimensions={0} | all-to-all | bytes 3145728 | tf_op jit(solution)/shard_map/all_to_all | solution.py:299
  48.9 23.5 %collective-permute-done.refs_1_.refs_2_ = bf16[8,2,256,128]{3,2,1,0:T(8,128)(2,1)} collective-permute-done((bf16[8,2,256,128]{3,2,1,0:T(8,128)(2,1)S(1)}, bf16[8,2,256,128]{3,2,1,0:T(8,128)(2,1)}, u32[]{:S(2)}, u32[]{:S(2)}) %collective-permute-start) | collective-permute-done | bytes 1048608 | tf_op jit(solution)/shard_map/ppermute | solution.py:283
  73.8 13.9 %shard_map.128 = (f32[1,4096]{1,0:T(1,128)}, f32[1,4096]{1,0:T(1,128)}, f32[128,4096]{1,0:T(8,128)}) custom-call(bf16[8,3,256,128]{3,2,1,0:T(8,128)(2,1)} %copy-done, bf16[8,3,256,128]{3,2,1,0:T(8,128)(2,1)} %copy-done, bf16[8,3,256,128]{3,2,1,0:T(8,128)(2,1)} %copy-done), custom_call_target="tpu_custom_call" | custom-call | flops 3221225472 | bytes 4194304 | tf_op jit(solution)/shard_map/pallas_call | solution.py:253
  87.7 15.4 %shard_map.129 = (f32[1,4096]{1,0:T(1,128)}, f32[1,4096]{1,0:T(1,128)}, f32[128,4096]{1,0:T(8,128)}) custom-call(bf16[8,3,256,128]{3,2,1,0:T(8,128)(2,1)} %copy-done, bf16[8,2,256,128]{3,2,1,0:T(8,128)(2,1)} %collective-permute-done.2.refs_1_.refs_2_, ...), custom_call_target="tpu_custom_call", output_to_operand_aliasing={{0}: (3, {}), {1}: (4, {}), {2}: (5, {})} | custom-call | flops 3221225472 | bytes 4194304 | tf_op jit(solution)/shard_map/pallas_call | solution.py:253
  103.1 15.4 %shard_map.130 = (f32[1,4096]{1,0:T(1,128)}, f32[1,4096]{1,0:T(1,128)}, f32[128,4096]{1,0:T(8,128)}) custom-call(bf16[8,3,256,128]{3,2,1,0:T(8,128)(2,1)} %copy-done, bf16[8,2,256,128]{3,2,1,0:T(8,128)(2,1)} %collective-permute-done.refs_1_.refs_2_, ...), custom_call_target="tpu_custom_call", output_to_operand_aliasing={{0}: (3, {}), {1}: (4, {}), {2}: (5, {})} | custom-call | flops 3221225472 | bytes 4194304 | tf_op jit(solution)/shard_map/pallas_call | solution.py:253
  118.6 16.7 %shard_map.131 = bf16[2048,128]{1,0:T(8,128)(2,1)} custom-call(bf16[8,3,256,128]{3,2,1,0:T(8,128)(2,1)} %copy-done, bf16[8,2,256,128]{3,2,1,0:T(8,128)(2,1)} %collective-permute-done.1.refs_1_.refs_2_, bf16[8,2,256,128]{3,2,1,0:T(8,128)(2,1)} %collective-permute-done.1.refs_1_.refs_2_, f32[1,4096]{1,0:T(1,128)} %get-tuple-element.28.refs_3_, ...), custom_call_target="tpu_custom_call" | custom-call | flops 3221225472 | bytes 4194304 | tf_op jit(solution)/shard_map/pallas_call | solution.py:253
  135.3 2.0 copy.22
  137.3 3.5 %all-to-all-start.1 = ((bf16[8,256,128]{1,2,0:T(8,128)(2,1)}), bf16[8,256,128]{1,2,0:T(8,128)(2,1)S(1)}, u32[]{:S(2)}, u32[]{:S(2)}) async-start(bf16[8,256,128]{1,2,0:T(8,128)(2,1)} %copy.22), calls=%async_computation.1 | async-start | bytes 1048576 | tf_op jit(solution)/shard_map/all_to_all | solution.py:299
  140.9 2.5 shard_map.132
  143.8 1.4 collective-permute-start.4
  145.3 13.2 %collective-permute-done.4.refs_2_ = bf16[3,64,704]{2,1,0:T(8,128)(2,1)S(1)} collective-permute-done((bf16[3,64,704]{2,1,0:T(8,128)(2,1)}, bf16[3,64,704]{2,1,0:T(8,128)(2,1)S(1)}, u32[]{:S(2)}, u32[]{:S(2)}) %collective-permute-start.4) | collective-permute-done | bytes 270368 | tf_op jit(solution)/shard_map/ppermute | solution.py:283
  158.5 4.4 %collective-permute-done.5.refs_3_ = bf16[3,64,704]{2,1,0:T(8,128)(2,1)S(1)} collective-permute-done((bf16[3,64,704]{2,1,0:T(8,128)(2,1)}, bf16[3,64,704]{2,1,0:T(8,128)(2,1)S(1)}, u32[]{:S(2)}, u32[]{:S(2)}) %collective-permute-start.5) | collective-permute-done | bytes 270368 | tf_op jit(solution)/shard_map/ppermute | solution.py:283
  163.6 2.6 shard_map.133.refs_0_
  166.2 4.2 %collective-permute-start.9 = (bf16[3,704,256]{2,1,0:T(8,128)(2,1)}, bf16[3,704,256]{2,1,0:T(8,128)(2,1)}, u32[]{:S(2)}, u32[]{:S(2)}) collective-permute-start(bf16[3,704,256]{2,1,0:T(8,128)(2,1)} %shard_map.133.refs_0_), channel_id=1, source_target_pairs={{0,16},{1,17},{2,18},{3,19},{4,20},{5,21},{6,22},{7,23},{8,24},{9,... | collective-permute-start | bytes 3244040 | tf_op jit(solution)/shard_map/ppermute | solution.py:283
  170.4 1.5 collective-permute-start.6
  171.9 1.5 collective-permute-start.7
  173.3 3.8 %fusion = (f32[256]{0:T(256)S(1)}, f32[256,2048]{1,0:T(8,128)S(1)}) fusion(bf16[256,1024]{0,1:T(8,128)(2,1)S(1)} %bitcast.11, bf16[1024,2048]{1,0:T(8,128)(2,1)} %param.21, bf16[256,2048]{1,0:T(8,128)(2,1)} %param.13), kind=kOutput, calls=%fused_computation.7 | convolution fusion | flops 1075838720 | bytes 7865344 | tf_op jit(solution)/shard_map/dot_general | solution.py:273
  177.9 1.3 multiply_convert_fusion.refs_9_
  179.2 1.9 collective-permute-start.15
  181.6 36.0 %collective-permute-done.9.refs_4_ = bf16[3,704,256]{2,1,0:T(8,128)(2,1)} collective-permute-done((bf16[3,704,256]{2,1,0:T(8,128)(2,1)}, bf16[3,704,256]{2,1,0:T(8,128)(2,1)}, u32[]{:S(2)}, u32[]{:S(2)}) %collective-permute-start.9) | collective-permute-done | bytes 1081376 | tf_op jit(solution)/shard_map/ppermute | solution.py:283
  217.6 1.6 collective-permute-start.10
  219.2 1.5 collective-permute-start.11
  221.7 3.5 %collective-permute-done.15.refs_9_ = bf16[256,2048]{1,0:T(8,128)(2,1)S(1)} collective-permute-done((bf16[256,2048]{1,0:T(8,128)(2,1)}, bf16[256,2048]{1,0:T(8,128)(2,1)S(1)}, u32[]{:S(2)}, u32[]{:S(2)}) %collective-permute-start.15) | collective-permute-done | bytes 1048608 | tf_op jit(solution)/shard_map/ppermute | solution.py:283
  226.7 17.9 %collective-permute-done.10.refs_5_ = bf16[3,704,256]{2,1,0:T(8,128)(2,1)} collective-permute-done((bf16[3,704,256]{2,1,0:T(8,128)(2,1)}, bf16[3,704,256]{2,1,0:T(8,128)(2,1)}, u32[]{:S(2)}, u32[]{:S(2)}) %collective-permute-start.10) | collective-permute-done | bytes 1081376 | tf_op jit(solution)/shard_map/ppermute | solution.py:283
  244.7 22.7 %collective-permute-done.11.refs_6_ = bf16[3,704,256]{2,1,0:T(8,128)(2,1)} collective-permute-done((bf16[3,704,256]{2,1,0:T(8,128)(2,1)}, bf16[3,704,256]{2,1,0:T(8,128)(2,1)}, u32[]{:S(2)}, u32[]{:S(2)}) %collective-permute-start.11) | collective-permute-done | bytes 1081376 | tf_op jit(solution)/shard_map/ppermute | solution.py:283
  268.3 10.0 %shard_map.135 = (bf16[256,2048]{1,0:T(8,128)(2,1)}, bf16[256,2048]{1,0:T(8,128)(2,1)}) custom-call(s32[1]{0:T(128)} %bitcast.5.base, bf16[3,704,256]{2,1,0:T(8,128)(2,1)} %shard_map.133.refs_0_, bf16[3,704,256]{2,1,0:T(8,128)(2,1)} %collective-permute-done.6.refs_1_, bf16[3,704,256]{2,1,0:T(8,128)(2,1)} %collective-permute-done.7.refs_2_, ...), custom_call_target="tpu_custom_call" | custom-call | flops 4429185024 | bytes 8650752 | tf_op jit(solution)/shard_map/pallas_call | solution.py:128
  278.4 10.0 %shard_map.134 = (bf16[256,2048]{1,0:T(8,128)(2,1)}, bf16[256,2048]{1,0:T(8,128)(2,1)}) custom-call(s32[1]{0:T(128)} %bitcast.5.base, bf16[3,704,256]{2,1,0:T(8,128)(2,1)} %shard_map.133.refs_0_, bf16[3,704,256]{2,1,0:T(8,128)(2,1)} %collective-permute-done.6.refs_1_, bf16[3,704,256]{2,1,0:T(8,128)(2,1)} %collective-permute-done.7.refs_2_, ...), custom_call_target="tpu_custom_call" | custom-call | flops 4429185024 | bytes 8650752 | tf_op jit(solution)/shard_map/pallas_call | solution.py:128
  288.9 1.6 add_convert_fusion.1
  290.5 1.8 collective-permute-start.18
  292.4 23.5 %collective-permute-done.18 = bf16[256,2048]{1,0:T(8,128)(2,1)S(1)} collective-permute-done((bf16[256,2048]{1,0:T(8,128)(2,1)S(1)}, bf16[256,2048]{1,0:T(8,128)(2,1)S(1)}, u32[]{:S(2)}, u32[]{:S(2)}) %collective-permute-start.18) | collective-permute-done | bytes 1048608 | tf_op jit(solution)/shard_map/ppermute | solution.py:283
  315.9 2.0 add_convert_fusion
  (55 shorter events, 8.1 us)
Async XLA Ops:
  2.9 69.5 %copy-start.8 = (f32[128]{0:T(128)S(1)}, f32[128]{0:T(128)}, u32[]{:S(2)}) copy-start(f32[128]{0:T(128)} %param.20) | copy-start | bytes 1540
  2.9 70.3 %copy-start.12 = (f32[8]{0:T(128)S(1)}, f32[8]{0:T(128)}, u32[]{:S(2)}) copy-start(f32[8]{0:T(128)} %param.19) | copy-start | bytes 100
  48.7 25.1 %copy-start = (bf16[8,3,256,128]{3,2,1,0:T(8,128)(2,1)}, bf16[8,3,256,128]{3,2,1,0:T(8,128)(2,1)S(1)}, u32[]{:S(2)}) copy-start(bf16[8,3,256,128]{3,2,1,0:T(8,128)(2,1)S(1)} %all_to_all.10.refs_0_.refs_1_.refs_2_) | copy-start | bytes 4718596
  48.8 23.7 %collective-permute-start = (bf16[8,2,256,128]{3,2,1,0:T(8,128)(2,1)S(1)}, bf16[8,2,256,128]{3,2,1,0:T(8,128)(2,1)}, u32[]{:S(2)}, u32[]{:S(2)}) collective-permute-start(bf16[8,2,256,128]{3,2,1,0:T(8,128)(2,1)S(1)} %slice.4), channel_id=1, source_target_pairs={{0,8},{1,9},{2,10},{3,11},{4,12},{5,13},{6,14},{7,15},{8,0},{9,1},... | collective-permute-start | bytes 3145736 | tf_op jit(solution)/shard_map/ppermute | solution.py:283
  48.9 38.8 %collective-permute-start.2 = (bf16[8,2,256,128]{3,2,1,0:T(8,128)(2,1)S(1)}, bf16[8,2,256,128]{3,2,1,0:T(8,128)(2,1)}, u32[]{:S(2)}, u32[]{:S(2)}) collective-permute-start(bf16[8,2,256,128]{3,2,1,0:T(8,128)(2,1)S(1)} %slice.4), channel_id=1, source_target_pairs={{0,1},{1,0},{2,3},{3,2},{4,5},{5,4},{6,7},{7,6},{8,9},{9,8},{10,11... | collective-permute-start | bytes 3145736 | tf_op jit(solution)/shard_map/ppermute | solution.py:283
  72.4 46.1 %collective-permute-start.1 = (bf16[8,2,256,128]{3,2,1,0:T(8,128)(2,1)}, bf16[8,2,256,128]{3,2,1,0:T(8,128)(2,1)}, u32[]{:S(2)}, u32[]{:S(2)}) collective-permute-start(bf16[8,2,256,128]{3,2,1,0:T(8,128)(2,1)} %collective-permute-done.refs_1_.refs_2_), channel_id=1, source_target_pairs={{0,1},{1,0},{2,3},{3,2},{4,5},{5,4},{6,7},{7,6},{8,9},{9,8},{10,11... | collective-permute-start | bytes 3145736 | tf_op jit(solution)/shard_map/ppermute | solution.py:283
  137.3 36.0 %all-to-all-start.1 = ((bf16[8,256,128]{1,2,0:T(8,128)(2,1)}), bf16[8,256,128]{1,2,0:T(8,128)(2,1)S(1)}, u32[]{:S(2)}, u32[]{:S(2)}) async-start(bf16[8,256,128]{1,2,0:T(8,128)(2,1)} %copy.22), calls=%async_computation.1 | async-start | bytes 1048576 | tf_op jit(solution)/shard_map/all_to_all | solution.py:299
  143.3 1.9 collective-permute-start.3
  143.8 14.6 %collective-permute-start.4 = (bf16[3,64,704]{2,1,0:T(8,128)(2,1)}, bf16[3,64,704]{2,1,0:T(8,128)(2,1)S(1)}, u32[]{:S(2)}, u32[]{:S(2)}) collective-permute-start(bf16[3,64,704]{2,1,0:T(8,128)(2,1)} %get-tuple-element.33), channel_id=1, source_target_pairs={{0,8},{1,9},{2,10},{3,11},{4,12},{5,13},{6,14},{7,15},{8,0},{9,1},... | collective-permute-start | bytes 811016 | tf_op jit(solution)/shard_map/ppermute | solution.py:283
  145.3 17.6 %collective-permute-start.5 = (bf16[3,64,704]{2,1,0:T(8,128)(2,1)}, bf16[3,64,704]{2,1,0:T(8,128)(2,1)S(1)}, u32[]{:S(2)}, u32[]{:S(2)}) collective-permute-start(bf16[3,64,704]{2,1,0:T(8,128)(2,1)} %get-tuple-element.34), channel_id=1, source_target_pairs={{0,9},{1,8},{2,11},{3,10},{4,13},{5,12},{6,15},{7,14},{8,1},{9,0},... | collective-permute-start | bytes 811016 | tf_op jit(solution)/shard_map/ppermute | solution.py:283
  145.3 17.6 %copy-start.4 = (bf16[3,64,704]{2,1,0:T(8,128)(2,1)}, bf16[3,64,704]{2,1,0:T(8,128)(2,1)S(1)}, u32[]{:S(2)}) copy-start(bf16[3,64,704]{2,1,0:T(8,128)(2,1)S(1)} %collective-permute-done.3.refs_1_) | copy-start | bytes 811012
  158.5 4.4 %copy-start.5 = (bf16[3,64,704]{2,1,0:T(8,128)(2,1)}, bf16[3,64,704]{2,1,0:T(8,128)(2,1)S(1)}, u32[]{:S(2)}) copy-start(bf16[3,64,704]{2,1,0:T(8,128)(2,1)S(1)} %collective-permute-done.4.refs_2_) | copy-start | bytes 811012
  162.8 0.7 copy-start.6
  166.2 51.4 %collective-permute-start.9 = (bf16[3,704,256]{2,1,0:T(8,128)(2,1)}, bf16[3,704,256]{2,1,0:T(8,128)(2,1)}, u32[]{:S(2)}, u32[]{:S(2)}) collective-permute-start(bf16[3,704,256]{2,1,0:T(8,128)(2,1)} %shard_map.133.refs_0_), channel_id=1, source_target_pairs={{0,16},{1,17},{2,18},{3,19},{4,20},{5,21},{6,22},{7,23},{8,24},{9,... | collective-permute-start | bytes 3244040 | tf_op jit(solution)/shard_map/ppermute | solution.py:283
  170.4 48.9 %collective-permute-start.6 = (bf16[3,704,256]{2,1,0:T(8,128)(2,1)}, bf16[3,704,256]{2,1,0:T(8,128)(2,1)}, u32[]{:S(2)}, u32[]{:S(2)}) collective-permute-start(bf16[3,704,256]{2,1,0:T(8,128)(2,1)} %shard_map.133.refs_0_), channel_id=1, source_target_pairs={{0,2},{1,3},{2,0},{3,1},{4,6},{5,7},{6,4},{7,5},{8,10},{9,11},{10,... | collective-permute-start | bytes 3244040 | tf_op jit(solution)/shard_map/ppermute | solution.py:283
  171.9 48.9 %collective-permute-start.7 = (bf16[3,704,256]{2,1,0:T(8,128)(2,1)}, bf16[3,704,256]{2,1,0:T(8,128)(2,1)}, u32[]{:S(2)}, u32[]{:S(2)}) collective-permute-start(bf16[3,704,256]{2,1,0:T(8,128)(2,1)} %shard_map.133.refs_0_), channel_id=1, source_target_pairs={{0,4},{1,5},{2,6},{3,7},{4,0},{5,1},{6,2},{7,3},{8,12},{9,13},{10,... | collective-permute-start | bytes 3244040 | tf_op jit(solution)/shard_map/ppermute | solution.py:283
  177.6 3.6 %copy-start.1 = (bf16[3,704,256]{2,1,0:T(8,128)(2,1)S(1)}, bf16[3,704,256]{2,1,0:T(8,128)(2,1)}, u32[]{:S(2)}) copy-start(bf16[3,704,256]{2,1,0:T(8,128)(2,1)} %shard_map.133.refs_0_) | copy-start | bytes 3244036
  179.2 46.0 %collective-permute-start.15 = (bf16[256,2048]{1,0:T(8,128)(2,1)}, bf16[256,2048]{1,0:T(8,128)(2,1)S(1)}, u32[]{:S(2)}, u32[]{:S(2)}) collective-permute-start(bf16[256,2048]{1,0:T(8,128)(2,1)} %multiply_convert_fusion.refs_9_), channel_id=1, source_target_pairs={{0,8},{1,9},{2,10},{3,11},{4,12},{5,13},{6,14},{7,15},{8,0},{9,1},... | collective-permute-start | bytes 3145736 | tf_op jit(solution)/shard_map/ppermute | solution.py:283
  181.1 44.1 %collective-permute-start.8 = (bf16[3,704,256]{2,1,0:T(8,128)(2,1)S(1)}, bf16[3,704,256]{2,1,0:T(8,128)(2,1)S(1)}, u32[]{:S(2)}, u32[]{:S(2)}) collective-permute-start(bf16[3,704,256]{2,1,0:T(8,128)(2,1)S(1)} %copy-done.1), channel_id=1, source_target_pairs={{0,6},{1,7},{2,4},{3,5},{4,2},{5,3},{6,0},{7,1},{8,14},{9,15},{10,... | collective-permute-start | bytes 3244040 | tf_op jit(solution)/shard_map/ppermute | solution.py:283
  217.6 27.0 %collective-permute-start.10 = (bf16[3,704,256]{2,1,0:T(8,128)(2,1)}, bf16[3,704,256]{2,1,0:T(8,128)(2,1)}, u32[]{:S(2)}, u32[]{:S(2)}) collective-permute-start(bf16[3,704,256]{2,1,0:T(8,128)(2,1)} %collective-permute-done.9.refs_4_), channel_id=1, source_target_pairs={{0,2},{1,3},{2,0},{3,1},{4,6},{5,7},{6,4},{7,5},{8,10},{9,11},{10,... | collective-permute-start | bytes 3244040 | tf_op jit(solution)/shard_map/ppermute | solution.py:283
  219.2 48.1 %collective-permute-start.11 = (bf16[3,704,256]{2,1,0:T(8,128)(2,1)}, bf16[3,704,256]{2,1,0:T(8,128)(2,1)}, u32[]{:S(2)}, u32[]{:S(2)}) collective-permute-start(bf16[3,704,256]{2,1,0:T(8,128)(2,1)} %collective-permute-done.9.refs_4_), channel_id=1, source_target_pairs={{0,4},{1,5},{2,6},{3,7},{4,0},{5,1},{6,2},{7,3},{8,12},{9,13},{10,... | collective-permute-start | bytes 3244040 | tf_op jit(solution)/shard_map/ppermute | solution.py:283
  220.7 46.6 %collective-permute-start.12 = (bf16[3,704,256]{2,1,0:T(8,128)(2,1)}, bf16[3,704,256]{2,1,0:T(8,128)(2,1)}, u32[]{:S(2)}, u32[]{:S(2)}) collective-permute-start(bf16[3,704,256]{2,1,0:T(8,128)(2,1)} %collective-permute-done.9.refs_4_), channel_id=1, source_target_pairs={{0,6},{1,7},{2,4},{3,5},{4,2},{5,3},{6,0},{7,1},{8,14},{9,15},{10,... | collective-permute-start | bytes 3244040 | tf_op jit(solution)/shard_map/ppermute | solution.py:283
  225.2 43.1 %copy-start.10 = (bf16[256,2048]{1,0:T(8,128)(2,1)}, bf16[256,2048]{1,0:T(8,128)(2,1)S(1)}, u32[]{:S(2)}) copy-start(bf16[256,2048]{1,0:T(8,128)(2,1)S(1)} %collective-permute-done.15.refs_9_) | copy-start | bytes 3145732
  225.2 42.1 %collective-permute-start.16 = (bf16[256,2048]{1,0:T(8,128)(2,1)S(1)}, bf16[256,2048]{1,0:T(8,128)(2,1)S(1)}, u32[]{:S(2)}, u32[]{:S(2)}) collective-permute-start(bf16[256,2048]{1,0:T(8,128)(2,1)S(1)} %collective-permute-done.15.refs_9_), channel_id=1, source_target_pairs={{0,1},{1,0},{2,3},{3,2},{4,5},{5,4},{6,7},{7,6},{8,9},{9,8},{10,11... | collective-permute-start | bytes 3145736 | tf_op jit(solution)/shard_map/ppermute | solution.py:283
  225.2 1.1 copy-start.9
  226.3 52.1 %collective-permute-start.13 = (bf16[256,2048]{1,0:T(8,128)(2,1)}, bf16[256,2048]{1,0:T(8,128)(2,1)}, u32[]{:S(2)}, u32[]{:S(2)}) collective-permute-start(bf16[256,2048]{1,0:T(8,128)(2,1)} %multiply_convert_fusion.refs_9_), channel_id=1, source_target_pairs={{0,1},{1,0},{2,3},{3,2},{4,5},{5,4},{6,7},{7,6},{8,9},{9,8},{10,11... | collective-permute-start | bytes 3145736 | tf_op jit(solution)/shard_map/ppermute | solution.py:283
  267.3 1.0 copy-start.11
  278.3 10.6 %copy-start.2 = (bf16[256,2048]{1,0:T(8,128)(2,1)S(1)}, bf16[256,2048]{1,0:T(8,128)(2,1)}, u32[]{:S(2)}) copy-start(bf16[256,2048]{1,0:T(8,128)(2,1)} %get-tuple-element.37) | copy-start | bytes 3145732
  278.3 10.6 %collective-permute-start.17 = (bf16[256,2048]{1,0:T(8,128)(2,1)}, bf16[256,2048]{1,0:T(8,128)(2,1)}, u32[]{:S(2)}, u32[]{:S(2)}) collective-permute-start(bf16[256,2048]{1,0:T(8,128)(2,1)} %get-tuple-element.38), channel_id=1, source_target_pairs={{0,1},{1,0},{2,3},{3,2},{4,5},{5,4},{6,7},{7,6},{8,9},{9,8},{10,11... | collective-permute-start | bytes 3145736 | tf_op jit(solution)/shard_map/ppermute | solution.py:283
  288.4 27.5 %copy-start.3 = (bf16[256,2048]{1,0:T(8,128)(2,1)S(1)}, bf16[256,2048]{1,0:T(8,128)(2,1)}, u32[]{:S(2)}) copy-start(bf16[256,2048]{1,0:T(8,128)(2,1)} %get-tuple-element.35) | copy-start | bytes 3145732
  288.4 4.0 %collective-permute-start.14 = (bf16[256,2048]{1,0:T(8,128)(2,1)}, bf16[256,2048]{1,0:T(8,128)(2,1)S(1)}, u32[]{:S(2)}, u32[]{:S(2)}) collective-permute-start(bf16[256,2048]{1,0:T(8,128)(2,1)} %get-tuple-element.36), channel_id=1, source_target_pairs={{0,1},{1,0},{2,3},{3,2},{4,5},{5,4},{6,7},{7,6},{8,9},{9,8},{10,11... | collective-permute-start | bytes 3145736 | tf_op jit(solution)/shard_map/ppermute | solution.py:283
  290.5 25.4 %collective-permute-start.18 = (bf16[256,2048]{1,0:T(8,128)(2,1)S(1)}, bf16[256,2048]{1,0:T(8,128)(2,1)S(1)}, u32[]{:S(2)}, u32[]{:S(2)}) collective-permute-start(bf16[256,2048]{1,0:T(8,128)(2,1)S(1)} %add_convert_fusion.1), channel_id=1, source_target_pairs={{0,8},{1,9},{2,10},{3,11},{4,12},{5,13},{6,14},{7,15},{8,0},{9,1},... | collective-permute-start | bytes 3145736 | tf_op jit(solution)/shard_map/ppermute | solution.py:283
  (1 other events, 0.7 us)

commit v4 on v3

--- a/solution.py
+++ b/solution.py
@@ -152,23 +152,32 @@
         m_in, l_in, o_in = refs[:3]
         refs = refs[3:]
     if last:
-        lam_ref, gain_ref, out_ref, vt_ref = refs
+        lam_ref, gain_ref, out_ref, vt_ref, keys_one, keys_two = refs
     else:
-        m_out, l_out, o_out, vt_ref = refs
+        m_out, l_out, o_out, vt_ref, keys_one, keys_two = refs
+    tripled = (keys_one, keys_two)
     vd = q_ref.shape[-1]
     qb = q_ref.shape[0] * q_ref.shape[2]
     kc = k_ref.shape[0] * k_ref.shape[2]
     c = LOG2E * hd**-0.5
-    keys = k_ref.reshape(kc, vd)
 
     @pl.when(pl.program_id(0) == 0)
     def _():
         vt_ref[...] = v_ref[...].reshape(kc, vd).T
+        keys = k_ref[...].reshape(kc, vd)
+        for a, ref in enumerate(tripled):
+            own = keys[:, a * hd : (a + 1) * hd]
+            ref[...] = jnp.concatenate([own, own, own, jnp.zeros_like(own)], axis=1)
 
     qt = q_ref[...].reshape(qb, vd).T
-    row = lax.broadcasted_iota(jnp.int32, qt.shape, 0)
-    zero = jnp.zeros_like(qt)
-    queries = (jnp.where(row < hd, qt, zero), jnp.where(row >= hd, qt, zero))
+    queries = []
+    for a in (0, 1):
+        exact = qt[a * hd : (a + 1) * hd].astype(jnp.float32) * c
+        high = exact.astype(jnp.bfloat16)
+        rest = exact - high.astype(jnp.float32)
+        middle = rest.astype(jnp.bfloat16)
+        low = (rest - middle.astype(jnp.float32)).astype(jnp.bfloat16)
+        queries.append(jnp.concatenate([high, middle, low, jnp.zeros_like(high)], axis=0))
     state = []
     for a in (0, 1):
         cols = slice(a * qb, (a + 1) * qb)
@@ -186,7 +195,7 @@
     def scores(step):
         j, a = step
         return jnp.dot(
-            keys[j * kb : (j + 1) * kb, :], queries[a], preferred_element_type=jnp.float32
+            tripled[a][j * kb : (j + 1) * kb, :], queries[a], preferred_element_type=jnp.float32
         )
 
     steps = [(j, a) for j in range(kc // kb) for a in (0, 1)]
@@ -195,8 +204,8 @@
         s_next = scores(steps[t + 1]) if t + 1 < len(steps) else None
         m, l, o = state[a]
         m_new = jnp.maximum(m, jnp.max(s, axis=0, keepdims=True))
-        p = jnp.exp2((s - m_new) * c)
-        scale = jnp.exp2((m - m_new) * c)
+        p = jnp.exp2(s - m_new)
+        scale = jnp.exp2(m - m_new)
         l = l * scale + jnp.sum(p, axis=0, keepdims=True)
         o = o * scale + jnp.dot(
             vt_ref[:, j * kb : (j + 1) * kb],
@@ -259,7 +268,8 @@
         out_specs=out_specs,
         out_shape=out_shape,
         input_output_aliases=aliases,
-        scratch_shapes=[pltpu.VMEM((vd, kc), jnp.bfloat16)],
+        scratch_shapes=[pltpu.VMEM((vd, kc), jnp.bfloat16)]
+        + [pltpu.VMEM((kc, 4 * hd), jnp.bfloat16)] * 2,
         compiler_params=pltpu.CompilerParams(
             dimension_semantics=("arbitrary",), vmem_limit_bytes=VMEM_LIMIT
         ),
@@ -359,14 +369,24 @@
     packed = pack(query_one, query_two, key_one, key_two, values, heads)
     attended = attention(packed, lambdas, head_gain, share_bits, head_bits)
     by_rows = lax.all_to_all(attended, "tp", split_axis=0, concat_axis=1, tiled=True)
-    own_normed = layer_normed(by_rows, stream, out_weight, norm_gain)
-    own = lax.all_gather(own_normed, "tp", axis=0, tiled=True)
-
+    stream_far = swap(stream, far)
+    stream_near = swap(stream, 1)
+    stream_both = swap(stream_far, 1)
+    rows_far = swap(by_rows, far)
+    rows_near = swap(by_rows, 1)
+    rows_both = swap(rows_far, 1)
+
+    def normed(heads_rows, residual_rows):
+        own = layer_normed(heads_rows, residual_rows, out_weight, norm_gain)
+        return own, lax.all_gather(own, "tp", axis=0, tiled=True)
+
+    own_normed, own = normed(by_rows, stream)
+    near = normed(rows_near, stream_near)[1]
+    away = normed(rows_far, stream_far)[1]
+    both = normed(rows_both, stream_both)[1]
     gathered = [weights[mask] for mask in subsets(others)]
     rows = gate_weight.shape[0]
     strips = [((b + f) * rows, (b + f + 2) * rows) for b in subsets(others) for f in (0, far)]
-    near, away = swap(own, 1), swap(own, far)
-    both = swap(away, 1)
     both_out, away_out = mixer(base, both, away, gathered, strips)
     handed = swap(both_out, 1)
     summed = away_out.astype(jnp.float32) + handed.astype(jnp.float32)

time: 318 us -> 344 us (1.082)
  waiting for transfers between devices: 145 us -> 165 us
  Pallas kernels: 89.5 us -> 84.9 us
  matrix products: 3.84 us -> 8.09 us
    ppermute x19 -> x22, waiting for transfers between devices: 145 us -> 165 us  [swap(): return lax.ppermute(x, 'sp', [(i, i ^ mask) for i in range(group)])]
    pallas_call x4, Pallas kernels: 61.4 us -> 56.8 us  [attend(): pl.pallas_call(functools.partial(attend_kernel, kb=kb, hd=hd, first=state...]
    dot_general x1 -> x4, matrix products: 3.84 us -> 8.09 us  [layer_normed(): branch = jnp.dot(heads_rows, out_weight, preferred_element_type=jnp.float32)]
    ppermute x19 -> x22, starting transfers between devices: 18.6 us -> 20.9 us  [swap(): return lax.ppermute(x, 'sp', [(i, i ^ mask) for i in range(group)])]
  transfers between devices with their start and end apart: 20 -> 23, of which waited for: 8 -> 10; matrix products, arithmetic and copies ran while one was open for 3% -> 4% of each run, Pallas kernels for 22% -> 16%
where the time goes in v4:
time: 344 us; the launch traced here: 343 us
  waiting for transfers between devices  165 us (48%)
  Pallas kernels  84.9 us (25%)
  blocking collectives  45.8 us (13%)
  starting transfers between devices  24.4 us (7%)
  matrix products  8.09 us (2%)
  local copies, waits for them, and re-layouts  7.41 us (2%)
  other arithmetic  7.39 us (2%)
    ppermute x22, waiting for transfers between devices, swap(): return lax.ppermute(x, 'sp', [(i, i ^ mask) for i in range(group)])  165 us
    pallas_call x4, Pallas kernels, attend(): pl.pallas_call(functools.partial(attend_kernel, kb=kb, hd=hd, first=state...  56.8 us
    all_to_all x1, blocking collectives, exchange(): lax.all_to_all(x, 'sp', split_axis=0, concat_axis=0, axis_index_groups=pe...  45.8 us
    ppermute x22, starting transfers between devices, swap(): return lax.ppermute(x, 'sp', [(i, i ^ mask) for i in range(group)])  20.9 us
    pallas_call x2, Pallas kernels, mixer(): pl.pallas_call(functools.partial(mixer_kernel, blocks=len(weights), strip...  20 us
    dot_general x4, matrix products, layer_normed(): branch = jnp.dot(heads_rows, out_weight, preferred_element_type=jnp.float32)  8.09 us
  transfers between devices with their start and end apart: 23, of which 10 were waited for; matrix products, arithmetic and copies ran while one was open for 4% of the time, Pallas kernels for 16%

profile of v4, /device:TPU:0, one launch (start us, length us, event | category | flops | bytes accessed | tf_op | source)
XLA Modules:
  0.0 343.5 jit_solution(14544049229722901734)
XLA Ops:
  0.0 2.9 shard_map.127
  2.9 45.8 %all_to_all.10.refs_0_.refs_1_.refs_2_ = bf16[8,3,256,128]{3,2,1,0:T(8,128)(2,1)S(1)} all-to-all(bf16[8,3,256,128]{3,2,1,0:T(8,128)(2,1)} %shard_map.127), channel_id=1, replica_groups={{0,2,4,6,16,18,20,22},{1,3,5,7,17,19,21,23},{8,10,12,14,24,26,28,30},{9..., dimensions={0} | all-to-all | bytes 3145728 | tf_op jit(solution)/shard_map/all_to_all | solution.py:309
  48.9 23.5 %collective-permute-done.refs_1_.refs_2_ = bf16[8,2,256,128]{3,2,1,0:T(8,128)(2,1)} collective-permute-done((bf16[8,2,256,128]{3,2,1,0:T(8,128)(2,1)S(1)}, bf16[8,2,256,128]{3,2,1,0:T(8,128)(2,1)}, u32[]{:S(2)}, u32[]{:S(2)}) %collective-permute-start) | collective-permute-done | bytes 1048608 | tf_op jit(solution)/shard_map/ppermute | solution.py:293
  73.9 13.5 %shard_map.128 = (f32[1,4096]{1,0:T(1,128)}, f32[1,4096]{1,0:T(1,128)}, f32[128,4096]{1,0:T(8,128)}) custom-call(bf16[8,3,256,128]{3,2,1,0:T(8,128)(2,1)} %copy-done.1, bf16[8,3,256,128]{3,2,1,0:T(8,128)(2,1)} %copy-done.1, bf16[8,3,256,128]{3,2,1,0:T(8,128)(2,1)} %copy-done.1), custom_call_target="tpu_custom_call" | custom-call | flops 3221225472 | bytes 4194304 | tf_op jit(solution)/shard_map/pallas_call | solution.py:262
  87.4 13.7 %shard_map.129 = (f32[1,4096]{1,0:T(1,128)}, f32[1,4096]{1,0:T(1,128)}, f32[128,4096]{1,0:T(8,128)}) custom-call(bf16[8,3,256,128]{3,2,1,0:T(8,128)(2,1)} %copy-done.1, bf16[8,2,256,128]{3,2,1,0:T(8,128)(2,1)} %collective-permute-done.2.refs_1_.refs_2_, ...), custom_call_target="tpu_custom_call", output_to_operand_aliasing={{0}: (3, {}), {1}: (4, {}), {2}: (5, {})} | custom-call | flops 3221225472 | bytes 4194304 | tf_op jit(solution)/shard_map/pallas_call | solution.py:262
  101.1 13.7 %shard_map.130 = (f32[1,4096]{1,0:T(1,128)}, f32[1,4096]{1,0:T(1,128)}, f32[128,4096]{1,0:T(8,128)}) custom-call(bf16[8,3,256,128]{3,2,1,0:T(8,128)(2,1)} %copy-done.1, bf16[8,2,256,128]{3,2,1,0:T(8,128)(2,1)} %collective-permute-done.refs_1_.refs_2_, ...), custom_call_target="tpu_custom_call", output_to_operand_aliasing={{0}: (3, {}), {1}: (4, {}), {2}: (5, {})} | custom-call | flops 3221225472 | bytes 4194304 | tf_op jit(solution)/shard_map/pallas_call | solution.py:262
  114.8 15.8 %shard_map.131 = bf16[2048,128]{1,0:T(8,128)(2,1)} custom-call(bf16[8,3,256,128]{3,2,1,0:T(8,128)(2,1)} %copy-done.1, bf16[8,2,256,128]{3,2,1,0:T(8,128)(2,1)} %collective-permute-done.1.refs_1_.refs_2_, bf16[8,2,256,128]{3,2,1,0:T(8,128)(2,1)} %collective-permute-done.1.refs_1_.refs_2_, f32[1,4096]{1,0:T(1,128)} %get-tuple-element.28.refs_3_, ...), custom_call_target="tpu_custom_call" | custom-call | flops 3221225472 | bytes 4194304 | tf_op jit(solution)/shard_map/pallas_call | solution.py:262
  130.6 2.0 copy.22
  132.7 3.5 %all-to-all-start.1 = ((bf16[8,256,128]{1,2,0:T(8,128)(2,1)}), bf16[8,256,128]{1,2,0:T(8,128)(2,1)S(1)}, u32[]{:S(2)}, u32[]{:S(2)}) async-start(bf16[8,256,128]{1,2,0:T(8,128)(2,1)} %copy.22), calls=%async_computation.1 | async-start | bytes 1048576 | tf_op jit(solution)/shard_map/all_to_all | solution.py:309
  136.2 2.5 shard_map.132
  140.6 1.6 collective-permute-start.16
  142.5 11.3 %collective-permute-done.4.refs_2_ = bf16[3,64,704]{2,1,0:T(8,128)(2,1)S(1)} collective-permute-done((bf16[3,64,704]{2,1,0:T(8,128)(2,1)}, bf16[3,64,704]{2,1,0:T(8,128)(2,1)S(1)}, u32[]{:S(2)}, u32[]{:S(2)}) %collective-permute-start.4) | collective-permute-done | bytes 270368 | tf_op jit(solution)/shard_map/ppermute | solution.py:293
  153.8 4.4 %collective-permute-done.5.refs_3_ = bf16[3,64,704]{2,1,0:T(8,128)(2,1)S(1)} collective-permute-done((bf16[3,64,704]{2,1,0:T(8,128)(2,1)}, bf16[3,64,704]{2,1,0:T(8,128)(2,1)S(1)}, u32[]{:S(2)}, u32[]{:S(2)}) %collective-permute-start.5) | collective-permute-done | bytes 270368 | tf_op jit(solution)/shard_map/ppermute | solution.py:293
  159.0 2.7 shard_map.133.refs_0_
  161.6 4.6 %collective-permute-start.9 = (bf16[3,704,256]{2,1,0:T(8,128)(2,1)}, bf16[3,704,256]{2,1,0:T(8,128)(2,1)}, u32[]{:S(2)}, u32[]{:S(2)}) collective-permute-start(bf16[3,704,256]{2,1,0:T(8,128)(2,1)} %shard_map.133.refs_0_), channel_id=1, source_target_pairs={{0,16},{1,17},{2,18},{3,19},{4,20},{5,21},{6,22},{7,23},{8,24},{9,... | collective-permute-start | bytes 3244040 | tf_op jit(solution)/shard_map/ppermute | solution.py:293
  166.3 1.5 collective-permute-start.6
  167.7 1.4 collective-permute-start.18
  169.2 4.0 %fusion.3 = (f32[256]{0:T(256)S(1)}, f32[256,2048]{1,0:T(8,128)S(1)}) fusion(bf16[256,1024]{0,1:T(8,128)(2,1)S(1)} %bitcast.18, bf16[1024,2048]{1,0:T(8,128)(2,1)} %param.21, bf16[256,2048]{1,0:T(8,128)(2,1)} %param.13), kind=kOutput, calls=%fused_computation.25 | convolution fusion | flops 1075838720 | bytes 7865344 | tf_op jit(solution)/shard_map/dot_general | solution.py:283
  173.6 24.0 %collective-permute-done.16 = bf16[256,2048]{1,0:T(8,128)(2,1)S(1)} collective-permute-done((bf16[256,2048]{1,0:T(8,128)(2,1)}, bf16[256,2048]{1,0:T(8,128)(2,1)S(1)}, u32[]{:S(2)}, u32[]{:S(2)}) %collective-permute-start.16) | collective-permute-done | bytes 1048608 | tf_op jit(solution)/shard_map/ppermute | solution.py:293
  197.6 1.5 collective-permute-start.7
  199.1 17.0 %collective-permute-done.18 = bf16[256,1024]{0,1:T(8,128)(2,1)S(1)} collective-permute-done((bf16[256,1024]{0,1:T(8,128)(2,1)S(1)}, bf16[256,1024]{0,1:T(8,128)(2,1)S(1)}, u32[]{:S(2)}, u32[]{:S(2)}) %collective-permute-start.18) | collective-permute-done | bytes 524320 | tf_op jit(solution)/shard_map/ppermute | solution.py:293
  220.6 3.0 collective-permute-start.8
  225.6 2.9 collective-permute-start.12
  229.0 3.4 multiply_convert_fusion.3
  232.4 15.9 %collective-permute-done.8.refs_3_ = bf16[3,704,256]{2,1,0:T(8,128)(2,1)S(1)} collective-permute-done((bf16[3,704,256]{2,1,0:T(8,128)(2,1)S(1)}, bf16[3,704,256]{2,1,0:T(8,128)(2,1)S(1)}, u32[]{:S(2)}, u32[]{:S(2)}) %collective-permute-start.8) | collective-permute-done | bytes 1081376 | tf_op jit(solution)/shard_map/ppermute | solution.py:293
  248.3 23.7 %collective-permute-done.10.refs_5_ = bf16[3,704,256]{2,1,0:T(8,128)(2,1)S(1)} collective-permute-done((bf16[3,704,256]{2,1,0:T(8,128)(2,1)}, bf16[3,704,256]{2,1,0:T(8,128)(2,1)S(1)}, u32[]{:S(2)}, u32[]{:S(2)}) %collective-permute-start.10) | collective-permute-done | bytes 1081376 | tf_op jit(solution)/shard_map/ppermute | solution.py:293
  274.0 20.4 %collective-permute-done.12.refs_7_ = bf16[3,704,256]{2,1,0:T(8,128)(2,1)S(1)} collective-permute-done((bf16[3,704,256]{2,1,0:T(8,128)(2,1)}, bf16[3,704,256]{2,1,0:T(8,128)(2,1)S(1)}, u32[]{:S(2)}, u32[]{:S(2)}) %collective-permute-start.12) | collective-permute-done | bytes 1081376 | tf_op jit(solution)/shard_map/ppermute | solution.py:293
  295.5 10.0 %shard_map.135 = (bf16[256,2048]{1,0:T(8,128)(2,1)}, bf16[256,2048]{1,0:T(8,128)(2,1)}) custom-call(s32[1]{0:T(128)} %bitcast.5.base, bf16[3,704,256]{2,1,0:T(8,128)(2,1)} %shard_map.133.refs_0_, bf16[3,704,256]{2,1,0:T(8,128)(2,1)} %collective-permute-done.6.refs_1_, bf16[3,704,256]{2,1,0:T(8,128)(2,1)} %copy-done.11, bf16[3,704,256]{2,1,0:T(8,128)(2,1)} %copy-done.12, ...), custom_call_target="tpu_custom_call" | custom-call | flops 4429185024 | bytes 8650752 | tf_op jit(solution)/shard_map/pallas_call | solution.py:128
  305.5 10.1 %shard_map.134 = (bf16[256,2048]{1,0:T(8,128)(2,1)}, bf16[256,2048]{1,0:T(8,128)(2,1)}) custom-call(s32[1]{0:T(128)} %bitcast.5.base, bf16[3,704,256]{2,1,0:T(8,128)(2,1)} %shard_map.133.refs_0_, bf16[3,704,256]{2,1,0:T(8,128)(2,1)} %collective-permute-done.6.refs_1_, bf16[3,704,256]{2,1,0:T(8,128)(2,1)} %copy-done.11, bf16[3,704,256]{2,1,0:T(8,128)(2,1)} %copy-done.12, ...), custom_call_target="tpu_custom_call" | custom-call | flops 4429185024 | bytes 8650752 | tf_op jit(solution)/shard_map/pallas_call | solution.py:128
  316.6 2.0 collective-permute-done.15
  318.7 23.1 %collective-permute-done.21 = bf16[256,2048]{1,0:T(8,128)(2,1)S(1)} collective-permute-done((bf16[256,2048]{1,0:T(8,128)(2,1)S(1)}, bf16[256,2048]{1,0:T(8,128)(2,1)S(1)}, u32[]{:S(2)}, u32[]{:S(2)}) %collective-permute-start.21) | collective-permute-done | bytes 1048608 | tf_op jit(solution)/shard_map/ppermute | solution.py:293
  341.7 1.8 add_convert_fusion
  (81 shorter events, 16.1 us)
Async XLA Ops:
  2.9 69.5 %copy-start.10 = (f32[128]{0:T(128)S(1)}, f32[128]{0:T(128)}, u32[]{:S(2)}) copy-start(f32[128]{0:T(128)} %param.20) | copy-start | bytes 1540
  2.9 70.3 %copy-start.16 = (f32[8]{0:T(128)S(1)}, f32[8]{0:T(128)}, u32[]{:S(2)}) copy-start(f32[8]{0:T(128)} %param.19) | copy-start | bytes 100
  48.7 25.2 %copy-start.1 = (bf16[8,3,256,128]{3,2,1,0:T(8,128)(2,1)}, bf16[8,3,256,128]{3,2,1,0:T(8,128)(2,1)S(1)}, u32[]{:S(2)}) copy-start(bf16[8,3,256,128]{3,2,1,0:T(8,128)(2,1)S(1)} %all_to_all.10.refs_0_.refs_1_.refs_2_) | copy-start | bytes 4718596
  48.8 23.7 %collective-permute-start = (bf16[8,2,256,128]{3,2,1,0:T(8,128)(2,1)S(1)}, bf16[8,2,256,128]{3,2,1,0:T(8,128)(2,1)}, u32[]{:S(2)}, u32[]{:S(2)}) collective-permute-start(bf16[8,2,256,128]{3,2,1,0:T(8,128)(2,1)S(1)} %slice.4), channel_id=1, source_target_pairs={{0,8},{1,9},{2,10},{3,11},{4,12},{5,13},{6,14},{7,15},{8,0},{9,1},... | collective-permute-start | bytes 3145736 | tf_op jit(solution)/shard_map/ppermute | solution.py:293
  48.9 38.5 %collective-permute-start.2 = (bf16[8,2,256,128]{3,2,1,0:T(8,128)(2,1)S(1)}, bf16[8,2,256,128]{3,2,1,0:T(8,128)(2,1)}, u32[]{:S(2)}, u32[]{:S(2)}) collective-permute-start(bf16[8,2,256,128]{3,2,1,0:T(8,128)(2,1)S(1)} %slice.4), channel_id=1, source_target_pairs={{0,1},{1,0},{2,3},{3,2},{4,5},{5,4},{6,7},{7,6},{8,9},{9,8},{10,11... | collective-permute-start | bytes 3145736 | tf_op jit(solution)/shard_map/ppermute | solution.py:293
  72.4 42.4 %collective-permute-start.1 = (bf16[8,2,256,128]{3,2,1,0:T(8,128)(2,1)}, bf16[8,2,256,128]{3,2,1,0:T(8,128)(2,1)}, u32[]{:S(2)}, u32[]{:S(2)}) collective-permute-start(bf16[8,2,256,128]{3,2,1,0:T(8,128)(2,1)} %collective-permute-done.refs_1_.refs_2_), channel_id=1, source_target_pairs={{0,1},{1,0},{2,3},{3,2},{4,5},{5,4},{6,7},{7,6},{8,9},{9,8},{10,11... | collective-permute-start | bytes 3145736 | tf_op jit(solution)/shard_map/ppermute | solution.py:293
  132.7 35.1 %all-to-all-start.1 = ((bf16[8,256,128]{1,2,0:T(8,128)(2,1)}), bf16[8,256,128]{1,2,0:T(8,128)(2,1)S(1)}, u32[]{:S(2)}, u32[]{:S(2)}) async-start(bf16[8,256,128]{1,2,0:T(8,128)(2,1)} %copy.22), calls=%async_computation.1 | async-start | bytes 1048576 | tf_op jit(solution)/shard_map/all_to_all | solution.py:309
  138.7 3.8 %collective-permute-start.3 = (bf16[3,64,704]{2,1,0:T(8,128)(2,1)}, bf16[3,64,704]{2,1,0:T(8,128)(2,1)S(1)}, u32[]{:S(2)}, u32[]{:S(2)}) collective-permute-start(bf16[3,64,704]{2,1,0:T(8,128)(2,1)} %get-tuple-element.32), channel_id=1, source_target_pairs={{0,1},{1,0},{2,3},{3,2},{4,5},{5,4},{6,7},{7,6},{8,9},{9,8},{10,11... | collective-permute-start | bytes 811016 | tf_op jit(solution)/shard_map/ppermute | solution.py:293
  139.2 14.6 %collective-permute-start.4 = (bf16[3,64,704]{2,1,0:T(8,128)(2,1)}, bf16[3,64,704]{2,1,0:T(8,128)(2,1)S(1)}, u32[]{:S(2)}, u32[]{:S(2)}) collective-permute-start(bf16[3,64,704]{2,1,0:T(8,128)(2,1)} %get-tuple-element.33), channel_id=1, source_target_pairs={{0,8},{1,9},{2,10},{3,11},{4,12},{5,13},{6,14},{7,15},{8,0},{9,1},... | collective-permute-start | bytes 811016 | tf_op jit(solution)/shard_map/ppermute | solution.py:293
  140.6 17.6 %collective-permute-start.5 = (bf16[3,64,704]{2,1,0:T(8,128)(2,1)}, bf16[3,64,704]{2,1,0:T(8,128)(2,1)S(1)}, u32[]{:S(2)}, u32[]{:S(2)}) collective-permute-start(bf16[3,64,704]{2,1,0:T(8,128)(2,1)} %get-tuple-element.34), channel_id=1, source_target_pairs={{0,9},{1,8},{2,11},{3,10},{4,13},{5,12},{6,15},{7,14},{8,1},{9,0},... | collective-permute-start | bytes 811016 | tf_op jit(solution)/shard_map/ppermute | solution.py:293
  140.6 57.0 %collective-permute-start.16 = (bf16[256,2048]{1,0:T(8,128)(2,1)}, bf16[256,2048]{1,0:T(8,128)(2,1)S(1)}, u32[]{:S(2)}, u32[]{:S(2)}) collective-permute-start(bf16[256,2048]{1,0:T(8,128)(2,1)} %param.13), channel_id=1, source_target_pairs={{0,8},{1,9},{2,10},{3,11},{4,12},{5,13},{6,14},{7,15},{8,0},{9,1},... | collective-permute-start | bytes 3145736 | tf_op jit(solution)/shard_map/ppermute | solution.py:293
  142.2 75.2 %collective-permute-start.13 = (bf16[256,2048]{1,0:T(8,128)(2,1)}, bf16[256,2048]{1,0:T(8,128)(2,1)S(1)}, u32[]{:S(2)}, u32[]{:S(2)}) collective-permute-start(bf16[256,2048]{1,0:T(8,128)(2,1)} %param.13), channel_id=1, source_target_pairs={{0,1},{1,0},{2,3},{3,2},{4,5},{5,4},{6,7},{7,6},{8,9},{9,8},{10,11... | collective-permute-start | bytes 3145736 | tf_op jit(solution)/shard_map/ppermute | solution.py:293
  161.6 58.9 %collective-permute-start.9 = (bf16[3,704,256]{2,1,0:T(8,128)(2,1)}, bf16[3,704,256]{2,1,0:T(8,128)(2,1)}, u32[]{:S(2)}, u32[]{:S(2)}) collective-permute-start(bf16[3,704,256]{2,1,0:T(8,128)(2,1)} %shard_map.133.refs_0_), channel_id=1, source_target_pairs={{0,16},{1,17},{2,18},{3,19},{4,20},{5,21},{6,22},{7,23},{8,24},{9,... | collective-permute-start | bytes 3244040 | tf_op jit(solution)/shard_map/ppermute | solution.py:293
  166.3 59.3 %collective-permute-start.6 = (bf16[3,704,256]{2,1,0:T(8,128)(2,1)}, bf16[3,704,256]{2,1,0:T(8,128)(2,1)}, u32[]{:S(2)}, u32[]{:S(2)}) collective-permute-start(bf16[3,704,256]{2,1,0:T(8,128)(2,1)} %shard_map.133.refs_0_), channel_id=1, source_target_pairs={{0,2},{1,3},{2,0},{3,1},{4,6},{5,7},{6,4},{7,5},{8,10},{9,11},{10,... | collective-permute-start | bytes 3244040 | tf_op jit(solution)/shard_map/ppermute | solution.py:293
  167.7 48.3 %collective-permute-start.18 = (bf16[256,1024]{0,1:T(8,128)(2,1)S(1)}, bf16[256,1024]{0,1:T(8,128)(2,1)S(1)}, u32[]{:S(2)}, u32[]{:S(2)}) collective-permute-start(bf16[256,1024]{0,1:T(8,128)(2,1)S(1)} %bitcast.17), channel_id=1, source_target_pairs={{0,8},{1,9},{2,10},{3,11},{4,12},{5,13},{6,14},{7,15},{8,0},{9,1},... | collective-permute-start | bytes 1572872 | tf_op jit(solution)/shard_map/ppermute | solution.py:293
  169.2 46.9 %copy-start = (bf16[1024,2048]{1,0:T(8,128)(2,1)S(1)}, bf16[1024,2048]{1,0:T(8,128)(2,1)}, u32[]{:S(2)}) copy-start(bf16[1024,2048]{1,0:T(8,128)(2,1)} %param.21) | copy-start | bytes 12582916
  173.2 24.4 %copy-start.3 = (bf16[3,704,256]{2,1,0:T(8,128)(2,1)S(1)}, bf16[3,704,256]{2,1,0:T(8,128)(2,1)}, u32[]{:S(2)}) copy-start(bf16[3,704,256]{2,1,0:T(8,128)(2,1)} %shard_map.133.refs_0_) | copy-start | bytes 3244036
  197.6 34.7 %collective-permute-start.7 = (bf16[3,704,256]{2,1,0:T(8,128)(2,1)S(1)}, bf16[3,704,256]{2,1,0:T(8,128)(2,1)S(1)}, u32[]{:S(2)}, u32[]{:S(2)}) collective-permute-start(bf16[3,704,256]{2,1,0:T(8,128)(2,1)S(1)} %copy-done.3), channel_id=1, source_target_pairs={{0,4},{1,5},{2,6},{3,7},{4,0},{5,1},{6,2},{7,3},{8,12},{9,13},{10,... | collective-permute-start | bytes 3244040 | tf_op jit(solution)/shard_map/ppermute | solution.py:293
  216.0 2.0 collective-permute-start.14
  217.4 6.1 %collective-permute-start.17 = (bf16[256,2048]{1,0:T(8,128)(2,1)S(1)}, bf16[256,2048]{1,0:T(8,128)(2,1)S(1)}, u32[]{:S(2)}, u32[]{:S(2)}) collective-permute-start(bf16[256,2048]{1,0:T(8,128)(2,1)S(1)} %collective-permute-done.16), channel_id=1, source_target_pairs={{0,1},{1,0},{2,3},{3,2},{4,5},{5,4},{6,7},{7,6},{8,9},{9,8},{10,11... | collective-permute-start | bytes 3145736 | tf_op jit(solution)/shard_map/ppermute | solution.py:293
  219.4 4.7 %collective-permute-start.19 = (bf16[256,1024]{0,1:T(8,128)(2,1)S(1)}, bf16[256,1024]{0,1:T(8,128)(2,1)S(1)}, u32[]{:S(2)}, u32[]{:S(2)}) collective-permute-start(bf16[256,1024]{0,1:T(8,128)(2,1)S(1)} %collective-permute-done.18), channel_id=1, source_target_pairs={{0,1},{1,0},{2,3},{3,2},{4,5},{5,4},{6,7},{7,6},{8,9},{9,8},{10,11... | collective-permute-start | bytes 1572872 | tf_op jit(solution)/shard_map/ppermute | solution.py:293
  220.6 27.7 %collective-permute-start.8 = (bf16[3,704,256]{2,1,0:T(8,128)(2,1)S(1)}, bf16[3,704,256]{2,1,0:T(8,128)(2,1)S(1)}, u32[]{:S(2)}, u32[]{:S(2)}) collective-permute-start(bf16[3,704,256]{2,1,0:T(8,128)(2,1)S(1)} %copy-done.3), channel_id=1, source_target_pairs={{0,6},{1,7},{2,4},{3,5},{4,2},{5,3},{6,0},{7,1},{8,14},{9,15},{10,... | collective-permute-start | bytes 3244040 | tf_op jit(solution)/shard_map/ppermute | solution.py:293
  223.5 48.5 %collective-permute-start.10 = (bf16[3,704,256]{2,1,0:T(8,128)(2,1)}, bf16[3,704,256]{2,1,0:T(8,128)(2,1)S(1)}, u32[]{:S(2)}, u32[]{:S(2)}) collective-permute-start(bf16[3,704,256]{2,1,0:T(8,128)(2,1)} %collective-permute-done.9.refs_4_), channel_id=1, source_target_pairs={{0,2},{1,3},{2,0},{3,1},{4,6},{5,7},{6,4},{7,5},{8,10},{9,11},{10,... | collective-permute-start | bytes 3244040 | tf_op jit(solution)/shard_map/ppermute | solution.py:293
  224.1 48.9 %collective-permute-start.11 = (bf16[3,704,256]{2,1,0:T(8,128)(2,1)}, bf16[3,704,256]{2,1,0:T(8,128)(2,1)S(1)}, u32[]{:S(2)}, u32[]{:S(2)}) collective-permute-start(bf16[3,704,256]{2,1,0:T(8,128)(2,1)} %collective-permute-done.9.refs_4_), channel_id=1, source_target_pairs={{0,4},{1,5},{2,6},{3,7},{4,0},{5,1},{6,2},{7,3},{8,12},{9,13},{10,... | collective-permute-start | bytes 3244040 | tf_op jit(solution)/shard_map/ppermute | solution.py:293
  225.6 68.8 %collective-permute-start.12 = (bf16[3,704,256]{2,1,0:T(8,128)(2,1)}, bf16[3,704,256]{2,1,0:T(8,128)(2,1)S(1)}, u32[]{:S(2)}, u32[]{:S(2)}) collective-permute-start(bf16[3,704,256]{2,1,0:T(8,128)(2,1)} %collective-permute-done.9.refs_4_), channel_id=1, source_target_pairs={{0,6},{1,7},{2,4},{3,5},{4,2},{5,3},{6,0},{7,1},{8,14},{9,15},{10,... | collective-permute-start | bytes 3244040 | tf_op jit(solution)/shard_map/ppermute | solution.py:293
  232.4 15.9 %copy-start.11 = (bf16[3,704,256]{2,1,0:T(8,128)(2,1)}, bf16[3,704,256]{2,1,0:T(8,128)(2,1)S(1)}, u32[]{:S(2)}) copy-start(bf16[3,704,256]{2,1,0:T(8,128)(2,1)S(1)} %collective-permute-done.7.refs_2_) | copy-start | bytes 3244036
  248.3 47.2 %copy-start.12 = (bf16[3,704,256]{2,1,0:T(8,128)(2,1)}, bf16[3,704,256]{2,1,0:T(8,128)(2,1)S(1)}, u32[]{:S(2)}) copy-start(bf16[3,704,256]{2,1,0:T(8,128)(2,1)S(1)} %collective-permute-done.8.refs_3_) | copy-start | bytes 3244036
  305.4 10.7 %collective-permute-start.20 = (bf16[256,2048]{1,0:T(8,128)(2,1)}, bf16[256,2048]{1,0:T(8,128)(2,1)S(1)}, u32[]{:S(2)}, u32[]{:S(2)}) collective-permute-start(bf16[256,2048]{1,0:T(8,128)(2,1)} %get-tuple-element.38), channel_id=1, source_target_pairs={{0,1},{1,0},{2,3},{3,2},{4,5},{5,4},{6,7},{7,6},{8,9},{9,8},{10,11... | collective-permute-start | bytes 3145736 | tf_op jit(solution)/shard_map/ppermute | solution.py:293
  315.6 26.1 %copy-start.2 = (bf16[256,2048]{1,0:T(8,128)(2,1)S(1)}, bf16[256,2048]{1,0:T(8,128)(2,1)}, u32[]{:S(2)}) copy-start(bf16[256,2048]{1,0:T(8,128)(2,1)} %get-tuple-element.39.refs_9_) | copy-start | bytes 3145732
  315.6 26.1 %copy-start.4 = (bf16[256,2048]{1,0:T(8,128)(2,1)S(1)}, bf16[256,2048]{1,0:T(8,128)(2,1)}, u32[]{:S(2)}) copy-start(bf16[256,2048]{1,0:T(8,128)(2,1)} %get-tuple-element.35) | copy-start | bytes 3145732
  315.6 3.0 collective-permute-start.15
  316.6 25.2 %collective-permute-start.21 = (bf16[256,2048]{1,0:T(8,128)(2,1)S(1)}, bf16[256,2048]{1,0:T(8,128)(2,1)S(1)}, u32[]{:S(2)}, u32[]{:S(2)}) collective-permute-start(bf16[256,2048]{1,0:T(8,128)(2,1)S(1)} %add_convert_fusion.1), channel_id=1, source_target_pairs={{0,8},{1,9},{2,10},{3,11},{4,12},{5,13},{6,14},{7,15},{8,0},{9,1},... | collective-permute-start | bytes 3145736 | tf_op jit(solution)/shard_map/ppermute | solution.py:293
  (8 other events, 38.1 us)

commit v5 on v4

--- a/solution.py
+++ b/solution.py
@@ -377,13 +377,17 @@
     rows_both = swap(rows_far, 1)
 
     def normed(heads_rows, residual_rows):
-        own = layer_normed(heads_rows, residual_rows, out_weight, norm_gain)
-        return own, lax.all_gather(own, "tp", axis=0, tiled=True)
-
-    own_normed, own = normed(by_rows, stream)
-    near = normed(rows_near, stream_near)[1]
-    away = normed(rows_far, stream_far)[1]
-    both = normed(rows_both, stream_both)[1]
+        return layer_normed(heads_rows, residual_rows, out_weight, norm_gain)
+
+    def whole(rows):
+        return lax.all_gather(rows, "tp", axis=0, tiled=True)
+
+    own_normed = normed(by_rows, stream)
+    own, near = whole(own_normed), whole(normed(rows_near, stream_near))
+    pair = normed(
+        jnp.concatenate([rows_far, rows_both]), jnp.concatenate([stream_far, stream_both])
+    )
+    away, both = whole(pair[: pair.shape[0] // 2]), whole(pair[pair.shape[0] // 2 :])
     gathered = [weights[mask] for mask in subsets(others)]
     rows = gate_weight.shape[0]
     strips = [((b + f) * rows, (b + f + 2) * rows) for b in subsets(others) for f in (0, far)]

time: 344 us -> 359 us (1.044)
  waiting for transfers between devices: 165 us -> 181 us
  starting transfers between devices: 24.4 us -> 19.8 us
    ppermute x22, waiting for transfers between devices: 165 us -> 181 us  [swap(): return lax.ppermute(x, 'sp', [(i, i ^ mask) for i in range(group)])]
    ppermute x22, starting transfers between devices: 20.9 us -> 15.6 us  [swap(): return lax.ppermute(x, 'sp', [(i, i ^ mask) for i in range(group)])]
    dot_general x4 -> x3, matrix products: 8.09 us -> 9.47 us  [layer_normed(): branch = jnp.dot(heads_rows, out_weight, preferred_element_type=jnp.float32)]
  transfers between devices with their start and end apart: 23 -> 23, of which waited for: 10 -> 12; matrix products, arithmetic and copies ran while one was open for 4% -> 5% of each run, Pallas kernels for 16% -> 16%
where the time goes in v5:
time: 359 us
  waiting for transfers between devices  181 us (50%)
  Pallas kernels  85 us (24%)
  blocking collectives  45.8 us (13%)
  starting transfers between devices  19.8 us (6%)
  matrix products  9.47 us (3%)
  other arithmetic  9.16 us (3%)
  local copies, waits for them, and re-layouts  8.04 us (2%)
    ppermute x22, waiting for transfers between devices, swap(): return lax.ppermute(x, 'sp', [(i, i ^ mask) for i in range(group)])  181 us
    pallas_call x4, Pallas kernels, attend(): pl.pallas_call(functools.partial(attend_kernel, kb=kb, hd=hd, first=state...  56.6 us
    all_to_all x1, blocking collectives, exchange(): lax.all_to_all(x, 'sp', split_axis=0, concat_axis=0, axis_index_groups=pe...  45.8 us
    pallas_call x2, Pallas kernels, mixer(): pl.pallas_call(functools.partial(mixer_kernel, blocks=len(weights), strip...  20.3 us
    ppermute x22, starting transfers between devices, swap(): return lax.ppermute(x, 'sp', [(i, i ^ mask) for i in range(group)])  15.6 us
    dot_general x3, matrix products, layer_normed(): branch = jnp.dot(heads_rows, out_weight, preferred_element_type=jnp.float32)  9.47 us
  transfers between devices with their start and end apart: 23, of which 12 were waited for; matrix products, arithmetic and copies ran while one was open for 5% of the time, Pallas kernels for 16%

profile of v5, /device:TPU:0, one launch (start us, length us, event | category | flops | bytes accessed | tf_op | source)
XLA Modules:
  0.0 358.8 jit_solution(5991133701147427974)
XLA Ops:
  0.0 2.9 shard_map.127
  2.9 45.8 %all_to_all.10.refs_0_.refs_1_.refs_2_ = bf16[8,3,256,128]{3,2,1,0:T(8,128)(2,1)S(1)} all-to-all(bf16[8,3,256,128]{3,2,1,0:T(8,128)(2,1)} %shard_map.127), channel_id=1, replica_groups={{0,2,4,6,16,18,20,22},{1,3,5,7,17,19,21,23},{8,10,12,14,24,26,28,30},{9..., dimensions={0} | all-to-all | bytes 3145728 | tf_op jit(solution)/shard_map/all_to_all | solution.py:309
  48.9 23.5 %collective-permute-done.refs_1_.refs_2_ = bf16[8,2,256,128]{3,2,1,0:T(8,128)(2,1)} collective-permute-done((bf16[8,2,256,128]{3,2,1,0:T(8,128)(2,1)S(1)}, bf16[8,2,256,128]{3,2,1,0:T(8,128)(2,1)}, u32[]{:S(2)}, u32[]{:S(2)}) %collective-permute-start) | collective-permute-done | bytes 1048608 | tf_op jit(solution)/shard_map/ppermute | solution.py:293
  73.8 13.5 %shard_map.128 = (f32[1,4096]{1,0:T(1,128)}, f32[1,4096]{1,0:T(1,128)}, f32[128,4096]{1,0:T(8,128)}) custom-call(bf16[8,3,256,128]{3,2,1,0:T(8,128)(2,1)} %copy-done.2, bf16[8,3,256,128]{3,2,1,0:T(8,128)(2,1)} %copy-done.2, bf16[8,3,256,128]{3,2,1,0:T(8,128)(2,1)} %copy-done.2), custom_call_target="tpu_custom_call" | custom-call | flops 3221225472 | bytes 4194304 | tf_op jit(solution)/shard_map/pallas_call | solution.py:262
  87.3 13.7 %shard_map.129 = (f32[1,4096]{1,0:T(1,128)}, f32[1,4096]{1,0:T(1,128)}, f32[128,4096]{1,0:T(8,128)}) custom-call(bf16[8,3,256,128]{3,2,1,0:T(8,128)(2,1)} %copy-done.2, bf16[8,2,256,128]{3,2,1,0:T(8,128)(2,1)} %collective-permute-done.2.refs_1_.refs_2_, ...), custom_call_target="tpu_custom_call", output_to_operand_aliasing={{0}: (3, {}), {1}: (4, {}), {2}: (5, {})} | custom-call | flops 3221225472 | bytes 4194304 | tf_op jit(solution)/shard_map/pallas_call | solution.py:262
  101.0 13.7 %shard_map.130 = (f32[1,4096]{1,0:T(1,128)}, f32[1,4096]{1,0:T(1,128)}, f32[128,4096]{1,0:T(8,128)}) custom-call(bf16[8,3,256,128]{3,2,1,0:T(8,128)(2,1)} %copy-done.2, bf16[8,2,256,128]{3,2,1,0:T(8,128)(2,1)} %collective-permute-done.refs_1_.refs_2_, ...), custom_call_target="tpu_custom_call", output_to_operand_aliasing={{0}: (3, {}), {1}: (4, {}), {2}: (5, {})} | custom-call | flops 3221225472 | bytes 4194304 | tf_op jit(solution)/shard_map/pallas_call | solution.py:262
  114.7 15.7 %shard_map.131 = bf16[2048,128]{1,0:T(8,128)(2,1)} custom-call(bf16[8,3,256,128]{3,2,1,0:T(8,128)(2,1)} %copy-done.2, bf16[8,2,256,128]{3,2,1,0:T(8,128)(2,1)} %collective-permute-done.1.refs_1_.refs_2_, bf16[8,2,256,128]{3,2,1,0:T(8,128)(2,1)} %collective-permute-done.1.refs_1_.refs_2_, f32[1,4096]{1,0:T(1,128)} %get-tuple-element.28.refs_3_, ...), custom_call_target="tpu_custom_call" | custom-call | flops 3221225472 | bytes 4194304 | tf_op jit(solution)/shard_map/pallas_call | solution.py:262
  130.4 2.1 copy.22
  132.5 4.1 %all-to-all-start.1 = ((bf16[8,256,128]{1,2,0:T(8,128)(2,1)}), bf16[8,256,128]{1,2,0:T(8,128)(2,1)}, u32[]{:S(2)}, u32[]{:S(2)}) async-start(bf16[8,256,128]{1,2,0:T(8,128)(2,1)} %copy.22), calls=%async_computation.1 | async-start | bytes 1048576 | tf_op jit(solution)/shard_map/all_to_all | solution.py:309
  136.7 2.5 shard_map.132
  142.3 12.6 %collective-permute-done.4.refs_2_ = bf16[3,64,704]{2,1,0:T(8,128)(2,1)S(1)} collective-permute-done((bf16[3,64,704]{2,1,0:T(8,128)(2,1)}, bf16[3,64,704]{2,1,0:T(8,128)(2,1)S(1)}, u32[]{:S(2)}, u32[]{:S(2)}) %collective-permute-start.4) | collective-permute-done | bytes 270368 | tf_op jit(solution)/shard_map/ppermute | solution.py:293
  154.9 4.4 %collective-permute-done.5.refs_3_ = bf16[3,64,704]{2,1,0:T(8,128)(2,1)S(1)} collective-permute-done((bf16[3,64,704]{2,1,0:T(8,128)(2,1)}, bf16[3,64,704]{2,1,0:T(8,128)(2,1)S(1)}, u32[]{:S(2)}, u32[]{:S(2)}) %collective-permute-start.5) | collective-permute-done | bytes 270368 | tf_op jit(solution)/shard_map/ppermute | solution.py:293
  160.0 2.7 shard_map.133.refs_0_
  162.7 2.1 collective-permute-start.6
  165.8 4.2 %fusion.10 = (f32[256]{0:T(256)S(1)}, f32[256,2048]{1,0:T(8,128)S(1)}) fusion(bf16[256,1024]{0,1:T(8,128)(2,1)} %bitcast.4, bf16[1024,2048]{1,0:T(8,128)(2,1)} %param.21, bf16[256,2048]{1,0:T(8,128)(2,1)} %param.13), kind=kOutput, calls=%fused_computation.25 | convolution fusion | flops 1075838720 | bytes 7865344 | tf_op jit(solution)/shard_map/dot_general | solution.py:283
  170.4 13.4 %collective-permute-done.16 = bf16[256,2048]{1,0:T(8,128)(2,1)} collective-permute-done((bf16[256,2048]{1,0:T(8,128)(2,1)}, bf16[256,2048]{1,0:T(8,128)(2,1)}, u32[]{:S(2)}, u32[]{:S(2)}) %collective-permute-start.16) | collective-permute-done | bytes 1048608 | tf_op jit(solution)/shard_map/ppermute | solution.py:293
  183.8 1.6 collective-permute-start.7
  186.1 13.7 %collective-permute-done.18 = bf16[256,1024]{0,1:T(8,128)(2,1)S(1)} collective-permute-done((bf16[256,1024]{0,1:T(8,128)(2,1)}, bf16[256,1024]{0,1:T(8,128)(2,1)S(1)}, u32[]{:S(2)}, u32[]{:S(2)}) %collective-permute-start.18) | collective-permute-done | bytes 524320 | tf_op jit(solution)/shard_map/ppermute | solution.py:293
  203.6 30.2 %collective-permute-done.9.refs_4_ = bf16[3,704,256]{2,1,0:T(8,128)(2,1)S(1)} collective-permute-done((bf16[3,704,256]{2,1,0:T(8,128)(2,1)S(1)}, bf16[3,704,256]{2,1,0:T(8,128)(2,1)S(1)}, u32[]{:S(2)}, u32[]{:S(2)}) %collective-permute-start.9) | collective-permute-done | bytes 1081376 | tf_op jit(solution)/shard_map/ppermute | solution.py:293
  235.6 1.7 collective-permute-start.11
  237.3 4.0 %fusion.9 = (f32[512]{0:T(512)S(1)}, f32[512,2048]{1,0:T(8,128)S(1)}) fusion(bf16[1024,2048]{1,0:T(8,128)(2,1)S(1)} %copy-done, bf16[256,1024]{0,1:T(8,128)(2,1)S(1)} %collective-permute-done.19, bf16[256,1024]{0,1:T(8,128)(2,1)S(1)} %collective-permute-done.18, bf16[256,2048]{1,0:T(8,128)(2,1)S(1)} %collective-permute-done.17, ...), kind=kOutput, calls=%fused_computation.24 | convolution fusion | flops 2156920320 | bytes 11536384 | tf_op jit(solution)/shard_map/dot_general | solution.py:283
  241.8 1.5 collective-permute-start.12
  244.0 1.5 fusion.8
  245.4 16.0 %collective-permute-done.8.refs_3_ = bf16[3,704,256]{2,1,0:T(8,128)(2,1)S(1)} collective-permute-done((bf16[3,704,256]{2,1,0:T(8,128)(2,1)S(1)}, bf16[3,704,256]{2,1,0:T(8,128)(2,1)S(1)}, u32[]{:S(2)}, u32[]{:S(2)}) %collective-permute-start.8) | collective-permute-done | bytes 1081376 | tf_op jit(solution)/shard_map/ppermute | solution.py:293
  261.4 22.1 %collective-permute-done.10.refs_5_ = bf16[3,704,256]{2,1,0:T(8,128)(2,1)S(1)} collective-permute-done((bf16[3,704,256]{2,1,0:T(8,128)(2,1)S(1)}, bf16[3,704,256]{2,1,0:T(8,128)(2,1)S(1)}, u32[]{:S(2)}, u32[]{:S(2)}) %collective-permute-start.10) | collective-permute-done | bytes 1081376 | tf_op jit(solution)/shard_map/ppermute | solution.py:293
  284.5 20.0 %collective-permute-done.12.refs_7_ = bf16[3,704,256]{2,1,0:T(8,128)(2,1)S(1)} collective-permute-done((bf16[3,704,256]{2,1,0:T(8,128)(2,1)S(1)}, bf16[3,704,256]{2,1,0:T(8,128)(2,1)S(1)}, u32[]{:S(2)}, u32[]{:S(2)}) %collective-permute-start.12) | collective-permute-done | bytes 1081376 | tf_op jit(solution)/shard_map/ppermute | solution.py:293
  305.5 10.3 %shard_map.135 = (bf16[256,2048]{1,0:T(8,128)(2,1)}, bf16[256,2048]{1,0:T(8,128)(2,1)}) custom-call(s32[1]{0:T(128)} %bitcast.5.base, bf16[3,704,256]{2,1,0:T(8,128)(2,1)} %shard_map.133.refs_0_, bf16[3,704,256]{2,1,0:T(8,128)(2,1)} %collective-permute-done.6.refs_1_, bf16[3,704,256]{2,1,0:T(8,128)(2,1)} %copy-done.12, bf16[3,704,256]{2,1,0:T(8,128)(2,1)} %copy-done.14, ...), custom_call_target="tpu_custom_call" | custom-call | flops 4429185024 | bytes 8650752 | tf_op jit(solution)/shard_map/pallas_call | solution.py:128
  315.8 3.7 %multiply_convert_fusion.2 = (bf16[256,2048]{1,0:T(8,128)(2,1)}, bf16[256,2048]{1,0:T(8,128)(2,1)}) fusion(f32[256,2048]{1,0:T(8,128)S(1)} %get-tuple-element.46, f32[2048]{0:T(1024)S(1)} %copy-done.10, f32[256]{0:T(256)S(1)} %add_rsqrt_fusion.2, f32[256]{0:T(256)S(1)} %broadcast_multiply_fusion.2, f32[256]{0:T(256)S(1)} %add_rsqrt_fusion.1, ...), kind=kLoop, calls=%fused_computation.9 | loop fusion | flops 5767168 | bytes 7352320 | tf_op jit(solution)/shard_map/convert_element_type | solution.py:288
  319.5 10.0 %shard_map.134 = (bf16[256,2048]{1,0:T(8,128)(2,1)}, bf16[256,2048]{1,0:T(8,128)(2,1)}) custom-call(s32[1]{0:T(128)} %bitcast.5.base, bf16[3,704,256]{2,1,0:T(8,128)(2,1)} %shard_map.133.refs_0_, bf16[3,704,256]{2,1,0:T(8,128)(2,1)} %collective-permute-done.6.refs_1_, bf16[3,704,256]{2,1,0:T(8,128)(2,1)} %copy-done.12, bf16[3,704,256]{2,1,0:T(8,128)(2,1)} %copy-done.14, ...), custom_call_target="tpu_custom_call" | custom-call | flops 4429185024 | bytes 8650752 | tf_op jit(solution)/shard_map/pallas_call | solution.py:128
  330.1 1.7 add_convert_fusion.1
  332.6 24.4 %collective-permute-done.21 = bf16[256,2048]{1,0:T(8,128)(2,1)S(1)} collective-permute-done((bf16[256,2048]{1,0:T(8,128)(2,1)S(1)}, bf16[256,2048]{1,0:T(8,128)(2,1)S(1)}, u32[]{:S(2)}, u32[]{:S(2)}) %collective-permute-start.21) | collective-permute-done | bytes 1048608 | tf_op jit(solution)/shard_map/ppermute | solution.py:293
  357.0 1.8 add_convert_fusion
  (83 shorter events, 17.7 us)
Async XLA Ops:
  2.9 69.5 %copy-start.11 = (f32[128]{0:T(128)S(1)}, f32[128]{0:T(128)}, u32[]{:S(2)}) copy-start(f32[128]{0:T(128)} %param.20) | copy-start | bytes 1540
  2.9 70.3 %copy-start.18 = (f32[8]{0:T(128)S(1)}, f32[8]{0:T(128)}, u32[]{:S(2)}) copy-start(f32[8]{0:T(128)} %param.19) | copy-start | bytes 100
  48.7 25.1 %copy-start.2 = (bf16[8,3,256,128]{3,2,1,0:T(8,128)(2,1)}, bf16[8,3,256,128]{3,2,1,0:T(8,128)(2,1)S(1)}, u32[]{:S(2)}) copy-start(bf16[8,3,256,128]{3,2,1,0:T(8,128)(2,1)S(1)} %all_to_all.10.refs_0_.refs_1_.refs_2_) | copy-start | bytes 4718596
  48.8 23.7 %collective-permute-start = (bf16[8,2,256,128]{3,2,1,0:T(8,128)(2,1)S(1)}, bf16[8,2,256,128]{3,2,1,0:T(8,128)(2,1)}, u32[]{:S(2)}, u32[]{:S(2)}) collective-permute-start(bf16[8,2,256,128]{3,2,1,0:T(8,128)(2,1)S(1)} %slice.12), channel_id=1, source_target_pairs={{0,8},{1,9},{2,10},{3,11},{4,12},{5,13},{6,14},{7,15},{8,0},{9,1},... | collective-permute-start | bytes 3145736 | tf_op jit(solution)/shard_map/ppermute | solution.py:293
  48.9 38.4 %collective-permute-start.2 = (bf16[8,2,256,128]{3,2,1,0:T(8,128)(2,1)S(1)}, bf16[8,2,256,128]{3,2,1,0:T(8,128)(2,1)}, u32[]{:S(2)}, u32[]{:S(2)}) collective-permute-start(bf16[8,2,256,128]{3,2,1,0:T(8,128)(2,1)S(1)} %slice.12), channel_id=1, source_target_pairs={{0,1},{1,0},{2,3},{3,2},{4,5},{5,4},{6,7},{7,6},{8,9},{9,8},{10,11... | collective-permute-start | bytes 3145736 | tf_op jit(solution)/shard_map/ppermute | solution.py:293
  72.4 42.3 %collective-permute-start.1 = (bf16[8,2,256,128]{3,2,1,0:T(8,128)(2,1)}, bf16[8,2,256,128]{3,2,1,0:T(8,128)(2,1)}, u32[]{:S(2)}, u32[]{:S(2)}) collective-permute-start(bf16[8,2,256,128]{3,2,1,0:T(8,128)(2,1)} %collective-permute-done.refs_1_.refs_2_), channel_id=1, source_target_pairs={{0,1},{1,0},{2,3},{3,2},{4,5},{5,4},{6,7},{7,6},{8,9},{9,8},{10,11... | collective-permute-start | bytes 3145736 | tf_op jit(solution)/shard_map/ppermute | solution.py:293
  132.5 32.3 %all-to-all-start.1 = ((bf16[8,256,128]{1,2,0:T(8,128)(2,1)}), bf16[8,256,128]{1,2,0:T(8,128)(2,1)}, u32[]{:S(2)}, u32[]{:S(2)}) async-start(bf16[8,256,128]{1,2,0:T(8,128)(2,1)} %copy.22), calls=%async_computation.1 | async-start | bytes 1048576 | tf_op jit(solution)/shard_map/all_to_all | solution.py:309
  139.2 3.1 collective-permute-start.3
  139.7 15.2 %collective-permute-start.4 = (bf16[3,64,704]{2,1,0:T(8,128)(2,1)}, bf16[3,64,704]{2,1,0:T(8,128)(2,1)S(1)}, u32[]{:S(2)}, u32[]{:S(2)}) collective-permute-start(bf16[3,64,704]{2,1,0:T(8,128)(2,1)} %get-tuple-element.33), channel_id=1, source_target_pairs={{0,8},{1,9},{2,10},{3,11},{4,12},{5,13},{6,14},{7,15},{8,0},{9,1},... | collective-permute-start | bytes 811016 | tf_op jit(solution)/shard_map/ppermute | solution.py:293
  140.4 18.9 %collective-permute-start.5 = (bf16[3,64,704]{2,1,0:T(8,128)(2,1)}, bf16[3,64,704]{2,1,0:T(8,128)(2,1)S(1)}, u32[]{:S(2)}, u32[]{:S(2)}) collective-permute-start(bf16[3,64,704]{2,1,0:T(8,128)(2,1)} %get-tuple-element.34), channel_id=1, source_target_pairs={{0,9},{1,8},{2,11},{3,10},{4,13},{5,12},{6,15},{7,14},{8,1},{9,0},... | collective-permute-start | bytes 811016 | tf_op jit(solution)/shard_map/ppermute | solution.py:293
  141.0 42.8 %collective-permute-start.16 = (bf16[256,2048]{1,0:T(8,128)(2,1)}, bf16[256,2048]{1,0:T(8,128)(2,1)}, u32[]{:S(2)}, u32[]{:S(2)}) collective-permute-start(bf16[256,2048]{1,0:T(8,128)(2,1)} %param.13), channel_id=1, source_target_pairs={{0,8},{1,9},{2,10},{3,11},{4,12},{5,13},{6,14},{7,15},{8,0},{9,1},... | collective-permute-start | bytes 3145736 | tf_op jit(solution)/shard_map/ppermute | solution.py:293
  142.1 43.3 %collective-permute-start.13 = (bf16[256,2048]{1,0:T(8,128)(2,1)}, bf16[256,2048]{1,0:T(8,128)(2,1)S(1)}, u32[]{:S(2)}, u32[]{:S(2)}) collective-permute-start(bf16[256,2048]{1,0:T(8,128)(2,1)} %param.13), channel_id=1, source_target_pairs={{0,1},{1,0},{2,3},{3,2},{4,5},{5,4},{6,7},{7,6},{8,9},{9,8},{10,11... | collective-permute-start | bytes 3145736 | tf_op jit(solution)/shard_map/ppermute | solution.py:293
  162.7 79.1 %collective-permute-start.6 = (bf16[3,704,256]{2,1,0:T(8,128)(2,1)}, bf16[3,704,256]{2,1,0:T(8,128)(2,1)}, u32[]{:S(2)}, u32[]{:S(2)}) collective-permute-start(bf16[3,704,256]{2,1,0:T(8,128)(2,1)} %shard_map.133.refs_0_), channel_id=1, source_target_pairs={{0,2},{1,3},{2,0},{3,1},{4,6},{5,7},{6,4},{7,5},{8,10},{9,11},{10,... | collective-permute-start | bytes 3244040 | tf_op jit(solution)/shard_map/ppermute | solution.py:293
  164.8 35.0 %collective-permute-start.18 = (bf16[256,1024]{0,1:T(8,128)(2,1)}, bf16[256,1024]{0,1:T(8,128)(2,1)S(1)}, u32[]{:S(2)}, u32[]{:S(2)}) collective-permute-start(bf16[256,1024]{0,1:T(8,128)(2,1)} %bitcast.4), channel_id=1, source_target_pairs={{0,8},{1,9},{2,10},{3,11},{4,12},{5,13},{6,14},{7,15},{8,0},{9,1},... | collective-permute-start | bytes 1572872 | tf_op jit(solution)/shard_map/ppermute | solution.py:293
  165.8 34.0 %collective-permute-start.14 = (bf16[256,1024]{0,1:T(8,128)(2,1)}, bf16[256,1024]{0,1:T(8,128)(2,1)S(1)}, u32[]{:S(2)}, u32[]{:S(2)}) collective-permute-start(bf16[256,1024]{0,1:T(8,128)(2,1)} %bitcast.4), channel_id=1, source_target_pairs={{0,1},{1,0},{2,3},{3,2},{4,5},{5,4},{6,7},{7,6},{8,9},{9,8},{10,11... | collective-permute-start | bytes 1572872 | tf_op jit(solution)/shard_map/ppermute | solution.py:293
  165.8 34.5 %copy-start = (bf16[1024,2048]{1,0:T(8,128)(2,1)S(1)}, bf16[1024,2048]{1,0:T(8,128)(2,1)}, u32[]{:S(2)}) copy-start(bf16[1024,2048]{1,0:T(8,128)(2,1)} %param.21) | copy-start | bytes 12582916
  183.8 61.6 %collective-permute-start.7 = (bf16[3,704,256]{2,1,0:T(8,128)(2,1)S(1)}, bf16[3,704,256]{2,1,0:T(8,128)(2,1)S(1)}, u32[]{:S(2)}, u32[]{:S(2)}) collective-permute-start(bf16[3,704,256]{2,1,0:T(8,128)(2,1)S(1)} %copy-done.4), channel_id=1, source_target_pairs={{0,4},{1,5},{2,6},{3,7},{4,0},{5,1},{6,2},{7,3},{8,12},{9,13},{10,... | collective-permute-start | bytes 3244040 | tf_op jit(solution)/shard_map/ppermute | solution.py:293
  185.4 48.4 %collective-permute-start.9 = (bf16[3,704,256]{2,1,0:T(8,128)(2,1)S(1)}, bf16[3,704,256]{2,1,0:T(8,128)(2,1)S(1)}, u32[]{:S(2)}, u32[]{:S(2)}) collective-permute-start(bf16[3,704,256]{2,1,0:T(8,128)(2,1)S(1)} %copy-done.4), channel_id=1, source_target_pairs={{0,16},{1,17},{2,18},{3,19},{4,20},{5,21},{6,22},{7,23},{8,24},{9,... | collective-permute-start | bytes 3244040 | tf_op jit(solution)/shard_map/ppermute | solution.py:293
  199.8 35.4 %collective-permute-start.17 = (bf16[256,2048]{1,0:T(8,128)(2,1)}, bf16[256,2048]{1,0:T(8,128)(2,1)S(1)}, u32[]{:S(2)}, u32[]{:S(2)}) collective-permute-start(bf16[256,2048]{1,0:T(8,128)(2,1)} %collective-permute-done.16), channel_id=1, source_target_pairs={{0,1},{1,0},{2,3},{3,2},{4,5},{5,4},{6,7},{7,6},{8,9},{9,8},{10,11... | collective-permute-start | bytes 3145736 | tf_op jit(solution)/shard_map/ppermute | solution.py:293
  199.8 35.8 %collective-permute-start.19 = (bf16[256,1024]{0,1:T(8,128)(2,1)S(1)}, bf16[256,1024]{0,1:T(8,128)(2,1)S(1)}, u32[]{:S(2)}, u32[]{:S(2)}) collective-permute-start(bf16[256,1024]{0,1:T(8,128)(2,1)S(1)} %collective-permute-done.18), channel_id=1, source_target_pairs={{0,1},{1,0},{2,3},{3,2},{4,5},{5,4},{6,7},{7,6},{8,9},{9,8},{10,11... | collective-permute-start | bytes 1572872 | tf_op jit(solution)/shard_map/ppermute | solution.py:293
  233.8 27.6 %collective-permute-start.8 = (bf16[3,704,256]{2,1,0:T(8,128)(2,1)S(1)}, bf16[3,704,256]{2,1,0:T(8,128)(2,1)S(1)}, u32[]{:S(2)}, u32[]{:S(2)}) collective-permute-start(bf16[3,704,256]{2,1,0:T(8,128)(2,1)S(1)} %copy-done.4), channel_id=1, source_target_pairs={{0,6},{1,7},{2,4},{3,5},{4,2},{5,3},{6,0},{7,1},{8,14},{9,15},{10,... | collective-permute-start | bytes 3244040 | tf_op jit(solution)/shard_map/ppermute | solution.py:293
  235.2 48.3 %collective-permute-start.10 = (bf16[3,704,256]{2,1,0:T(8,128)(2,1)S(1)}, bf16[3,704,256]{2,1,0:T(8,128)(2,1)S(1)}, u32[]{:S(2)}, u32[]{:S(2)}) collective-permute-start(bf16[3,704,256]{2,1,0:T(8,128)(2,1)S(1)} %collective-permute-done.9.refs_4_), channel_id=1, source_target_pairs={{0,2},{1,3},{2,0},{3,1},{4,6},{5,7},{6,4},{7,5},{8,10},{9,11},{10,... | collective-permute-start | bytes 3244040 | tf_op jit(solution)/shard_map/ppermute | solution.py:293
  235.6 48.9 %collective-permute-start.11 = (bf16[3,704,256]{2,1,0:T(8,128)(2,1)S(1)}, bf16[3,704,256]{2,1,0:T(8,128)(2,1)S(1)}, u32[]{:S(2)}, u32[]{:S(2)}) collective-permute-start(bf16[3,704,256]{2,1,0:T(8,128)(2,1)S(1)} %collective-permute-done.9.refs_4_), channel_id=1, source_target_pairs={{0,4},{1,5},{2,6},{3,7},{4,0},{5,1},{6,2},{7,3},{8,12},{9,13},{10,... | collective-permute-start | bytes 3244040 | tf_op jit(solution)/shard_map/ppermute | solution.py:293
  241.8 62.7 %collective-permute-start.12 = (bf16[3,704,256]{2,1,0:T(8,128)(2,1)S(1)}, bf16[3,704,256]{2,1,0:T(8,128)(2,1)S(1)}, u32[]{:S(2)}, u32[]{:S(2)}) collective-permute-start(bf16[3,704,256]{2,1,0:T(8,128)(2,1)S(1)} %collective-permute-done.9.refs_4_), channel_id=1, source_target_pairs={{0,6},{1,7},{2,4},{3,5},{4,2},{5,3},{6,0},{7,1},{8,14},{9,15},{10,... | collective-permute-start | bytes 3244040 | tf_op jit(solution)/shard_map/ppermute | solution.py:293
  261.4 43.1 %copy-start.14 = (bf16[3,704,256]{2,1,0:T(8,128)(2,1)}, bf16[3,704,256]{2,1,0:T(8,128)(2,1)S(1)}, u32[]{:S(2)}) copy-start(bf16[3,704,256]{2,1,0:T(8,128)(2,1)S(1)} %collective-permute-done.8.refs_3_) | copy-start | bytes 3244036
  283.5 21.0 %copy-start.15 = (bf16[3,704,256]{2,1,0:T(8,128)(2,1)}, bf16[3,704,256]{2,1,0:T(8,128)(2,1)S(1)}, u32[]{:S(2)}) copy-start(bf16[3,704,256]{2,1,0:T(8,128)(2,1)S(1)} %collective-permute-done.10.refs_5_) | copy-start | bytes 3244036
  284.5 20.0 %copy-start.16 = (bf16[3,704,256]{2,1,0:T(8,128)(2,1)}, bf16[3,704,256]{2,1,0:T(8,128)(2,1)S(1)}, u32[]{:S(2)}) copy-start(bf16[3,704,256]{2,1,0:T(8,128)(2,1)S(1)} %collective-permute-done.11.refs_6_) | copy-start | bytes 3244036
  315.7 14.4 %collective-permute-start.20 = (bf16[256,2048]{1,0:T(8,128)(2,1)}, bf16[256,2048]{1,0:T(8,128)(2,1)}, u32[]{:S(2)}, u32[]{:S(2)}) collective-permute-start(bf16[256,2048]{1,0:T(8,128)(2,1)} %get-tuple-element.38), channel_id=1, source_target_pairs={{0,1},{1,0},{2,3},{3,2},{4,5},{5,4},{6,7},{7,6},{8,9},{9,8},{10,11... | collective-permute-start | bytes 3145736 | tf_op jit(solution)/shard_map/ppermute | solution.py:293
  329.5 27.5 %copy-start.3 = (bf16[256,2048]{1,0:T(8,128)(2,1)S(1)}, bf16[256,2048]{1,0:T(8,128)(2,1)}, u32[]{:S(2)}) copy-start(bf16[256,2048]{1,0:T(8,128)(2,1)} %get-tuple-element.41.refs_9_) | copy-start | bytes 3145732
  329.5 27.5 %copy-start.6 = (bf16[256,2048]{1,0:T(8,128)(2,1)S(1)}, bf16[256,2048]{1,0:T(8,128)(2,1)}, u32[]{:S(2)}) copy-start(bf16[256,2048]{1,0:T(8,128)(2,1)} %get-tuple-element.35) | copy-start | bytes 3145732
  329.5 3.1 collective-permute-start.15
  331.8 25.2 %collective-permute-start.21 = (bf16[256,2048]{1,0:T(8,128)(2,1)S(1)}, bf16[256,2048]{1,0:T(8,128)(2,1)S(1)}, u32[]{:S(2)}, u32[]{:S(2)}) collective-permute-start(bf16[256,2048]{1,0:T(8,128)(2,1)S(1)} %add_convert_fusion.1), channel_id=1, source_target_pairs={{0,8},{1,9},{2,10},{3,11},{4,12},{5,13},{6,14},{7,15},{8,0},{9,1},... | collective-permute-start | bytes 3145736 | tf_op jit(solution)/shard_map/ppermute | solution.py:293
  (10 other events, 75.0 us)
